TPU v7x, 256 devices: a whole 4x4x8 slice. The times are simulated.
256 devices in a mesh: sp: 64 (over z, y, core), tp: 4 (over x).
Axes of the slice: x: 4, y: 4, z: 8, core: 2. Of those that a mesh axis runs over, the one named last changes fastest.
Arguments:
- stream: bfloat16 [8192, 2048], P('sp'), may hold values from -12 to 12
- out_grad: bfloat16 [8192, 2048], P('sp'), may hold values from -16 to 16
- routes: int32 [8192, 2], P('sp'), may hold values from 0 to 63, all different within a row; in each aligned block of 128 rows (0 to 127, 128 to 255, ...) at most 8 rows name the same one
- route_weight: float32 [8192, 2], P('sp'), may hold values from 0.2 to 1
- queries: bfloat16 [8192, 8, 128], P('sp', 'tp'), may hold values from -6 to 6
- key_vectors: bfloat16 [8192, 8, 128], P('sp', 'tp'), may hold values from -6 to 6
- value_vectors: bfloat16 [8192, 8, 256], P('sp', 'tp'), may hold values from -6 to 6
- log_decay: float32 [8192, 8], P('sp', 'tp'), may hold values from -1 to 0
- out_proj: bfloat16 [2048, 2048], P(None, 'tp'), may hold values from -0.125 to 0.125
- gate_weight: bfloat16 [64, 2048, 1024], P('sp', None, 'tp'), may hold values from -0.125 to 0.125
- up_weight: bfloat16 [64, 2048, 1024], P('sp', None, 'tp'), may hold values from -0.125 to 0.125
- down_weight: bfloat16 [64, 1024, 2048], P('sp', 'tp'), may hold values from -0.1875 to 0.1875
Outputs:
- gate_grad: bfloat16 [64, 2048, 1024], P('sp', None, 'tp')
- up_grad: bfloat16 [64, 2048, 1024], P('sp', None, 'tp')
- down_grad: bfloat16 [64, 1024, 2048], P('sp', 'tp')
- proj_grad: float32 [2048, 2048], P('sp', 'tp')
- query_grad: bfloat16 [8192, 8, 128], P('sp', 'tp')
- key_grad: bfloat16 [8192, 8, 128], P('sp', 'tp')
- value_grad: bfloat16 [8192, 8, 256], P('sp', 'tp')
Inputs may be any that keep to these rules, and one draw needn't show every extreme that they name: `routes`: each row names two different experts. In each aligned block of 128 rows no expert is named by more than 8 rows, and in some block an expert is named by exactly 8.
All inputs are finite; a program needn't handle non-finite values.
Results may differ from a plain program's by a relative error of at most 0.025.
Values may be sent and summed in bfloat16 or wider, within the bound.
No kernel may reach another device: no remote copies, remote signals or barrier semaphores. Data moves between devices by JAX's collectives and lax.ppermute only.
A program may use at most 128 MiB of HBM per device.

v0:
```python
import jax
import jax.numpy as jnp
from jax import lax
from jax.sharding import Mesh
from jax.sharding import PartitionSpec as P

SP = ("sp_0", "sp_1", "sp_2")


CLAMP_LIMIT = 7.0
GATE_SLOPE = 1.702
EPSILON = 1e-06
TOP_PRECISION = lax.Precision.HIGHEST


def in_one_piece(arrays, axis, split_dim, concat_dim, along):
    both = jnp.concatenate(arrays, axis=along)
    result, at, finished = (
        lax.all_to_all(both, axis, split_axis=split_dim, concat_axis=concat_dim, tiled=True),
        0,
        [],
    )
    for a in arrays:
        finished.append(lax.slice_in_dim(result, at, at + a.shape[along], axis=along))
        at += a.shape[along]
    return tuple(finished)


def split_up(x, dim, length):
    before, after = (x.shape[:dim], x.shape[dim + 1 :])
    return jnp.moveaxis(x.reshape(*before, length, -1, *after), dim, 0)


def sent_and_summed(x, axis, dim):
    pieces = split_up(x, dim, lax.axis_size(axis))
    arrived = lax.all_to_all(pieces, axis, split_axis=0, concat_axis=0, tiled=True)
    return arrived.astype(jnp.float32).sum(axis=0)


def copy_for_each(x, axis):
    copies = jnp.broadcast_to(x, (lax.axis_size(axis), *x.shape))
    return lax.all_to_all(copies, axis, split_axis=0, concat_axis=0, tiled=True)


def joined_along(pieces, dim):
    lengths = list(pieces.shape[1:])
    lengths[dim] *= pieces.shape[0]
    return jnp.moveaxis(pieces, 0, dim).reshape(lengths)


def collect(x, axis, dim):
    pieces = copy_for_each(x, axis)
    return joined_along(pieces, dim)


def filled_with(x, identity):
    return jax.tree.map(
        lambda a, e: jnp.broadcast_to(jnp.asarray(e, a.dtype), a.shape), x, identity
    )


def prefix_by_axis(x, axes, combine, identity):
    before = start = filled_with(x, identity)
    total = x
    for axis in reversed(axes):
        length, position = (lax.axis_size(axis), lax.axis_index(axis))
        pieces = jax.tree.map(
            lambda part, kind: lax.all_gather(part.astype(kind), axis),
            total,
            (jnp.bfloat16, jnp.bfloat16),
        )
        inside, total = (start, start)
        for k in range(length):
            passed = k < position
            total = combine(
                total, jax.tree.map(lambda part, own: part[k].astype(own.dtype), pieces, x)
            )
            inside = jax.tree.map(lambda new, old: jnp.where(passed, new, old), total, inside)
        before = combine(inside, before)
    return before


def summed_rows(total, axes):
    for axis in axes:
        total = lax.psum_scatter(total, axis, scatter_dimension=0, tiled=True)
    return total


def prefix_by_axis_2(x, axes, combine, identity):
    before = start = filled_with(x, identity)
    total = x
    for axis in reversed(axes):
        length, position = (lax.axis_size(axis), lax.axis_index(axis))
        pieces = jax.tree.map(
            lambda part, kind: lax.all_gather(part.astype(kind), axis),
            total,
            jax.tree.map(lambda a: jnp.bfloat16 if a.dtype == jnp.float32 else a.dtype, x),
        )
        inside, total = (start, start)
        for k in reversed(range(length)):
            passed = k > position
            total = combine(
                total, jax.tree.map(lambda part, own: part[k].astype(own.dtype), pieces, x)
            )
            inside = jax.tree.map(lambda new, old: jnp.where(passed, new, old), total, inside)
        before = combine(inside, before)
    return before


def slot_numbers(route_block, expert_count):
    flat_ids = route_block.reshape(-1)
    onehot = (flat_ids[:, None] == jnp.arange(expert_count, dtype=jnp.int32)[None, :]).astype(
        jnp.int32
    )
    before = jnp.cumsum(onehot, axis=0) - onehot
    return (flat_ids, jnp.sum(before * onehot, axis=1))


def rotation_tables(start, count, key_width):
    frequency = 1.0 / 10000.0 ** jnp.linspace(0.0, 1.0, key_width // 2, dtype=jnp.float32)
    token_position = (start + jnp.arange(count, dtype=jnp.int32)).astype(jnp.float32)
    angles = token_position[:, None] * frequency[None, :]
    return (jnp.cos(angles), jnp.sin(angles))


def turn(field, cosines, sines):
    paired = field.reshape(field.shape[:-1] + (field.shape[-1] // 2, 2))
    even_part = paired[..., 0]
    odd_part = paired[..., 1]
    cos_rows = cosines[:, None, :]
    sin_rows = sines[:, None, :]
    turned = jnp.stack(
        [even_part * cos_rows - odd_part * sin_rows, odd_part * cos_rows + even_part * sin_rows],
        axis=-1,
    )
    return turned.reshape(field.shape)


def decay_combine(earlier, next_rows):
    return (earlier[0] * next_rows[0], next_rows[1] + next_rows[0][:, None, None] * earlier[1])


def expert_local(routed_rows, routed_grads, gate_w, up_w, down_w):
    gate_pre = jnp.dot(routed_rows, gate_w, preferred_element_type=jnp.float32)
    up_pre = jnp.dot(routed_rows, up_w, preferred_element_type=jnp.float32)
    gate_clip = jnp.minimum(gate_pre, CLAMP_LIMIT)
    up_clip = jnp.clip(up_pre, -CLAMP_LIMIT, CLAMP_LIMIT)
    sigmoid_gate = jax.nn.sigmoid(GATE_SLOPE * gate_clip)
    activated = (gate_clip * sigmoid_gate * (up_clip + 1.0)).astype(jnp.bfloat16)
    down_part = lax.dot_general(
        activated, routed_grads, (((0,), (0,)), ((), ())), preferred_element_type=jnp.float32
    )
    act_grad = lax.dot_general(
        routed_grads, down_w, (((1,), (1,)), ((), ())), preferred_element_type=jnp.float32
    )
    slope = sigmoid_gate + GATE_SLOPE * gate_clip * sigmoid_gate * (1.0 - sigmoid_gate)
    gate_pre_grad = jnp.where(
        gate_pre < CLAMP_LIMIT, act_grad * (up_clip + 1.0) * slope, 0.0
    ).astype(jnp.bfloat16)
    up_pre_grad = jnp.where(
        jnp.abs(up_pre) < CLAMP_LIMIT, act_grad * gate_clip * sigmoid_gate, 0.0
    ).astype(jnp.bfloat16)
    gate_part = lax.dot_general(
        routed_rows, gate_pre_grad, (((0,), (0,)), ((), ())), preferred_element_type=jnp.float32
    )
    up_part = lax.dot_general(
        routed_rows, up_pre_grad, (((0,), (0,)), ((), ())), preferred_element_type=jnp.float32
    )
    back_rows = lax.dot_general(
        gate_pre_grad, gate_w, (((1,), (1,)), ((), ())), preferred_element_type=jnp.float32
    )
    back_rows = back_rows + lax.dot_general(
        up_pre_grad, up_w, (((1,), (1,)), ((), ())), preferred_element_type=jnp.float32
    )
    return (
        gate_part.astype(jnp.bfloat16),
        up_part.astype(jnp.bfloat16),
        down_part.astype(jnp.bfloat16),
        back_rows.astype(jnp.bfloat16),
    )


def per_device(
    stream,
    out_grad,
    routes,
    route_weight,
    queries,
    key_vectors,
    value_vectors,
    log_decay,
    out_proj,
    gate_weight,
    up_weight,
    down_weight,
):
    experts = lax.axis_size(SP)
    tokens_here = stream.shape[0]
    model_width = stream.shape[1]
    capacity = 4 * tokens_here // experts
    pair_count = 2 * tokens_here
    flat_ids, slot_ids = slot_numbers(routes, experts)
    destination = flat_ids * capacity + slot_ids
    source = (
        jnp.full((experts * capacity,), -1, jnp.int32)
        .at[destination]
        .set(jnp.arange(pair_count, dtype=jnp.int32))
    )
    present = (source >= 0)[:, None]
    picked = jnp.maximum(source, 0)
    zero_value = jnp.zeros((), jnp.bfloat16)
    pair_grad = (route_weight[:, :, None] * out_grad[:, None, :].astype(jnp.float32)).astype(
        jnp.bfloat16
    )
    pair_grad = pair_grad.reshape(pair_count, model_width)
    send_rows = jnp.where(present, jnp.take(stream, picked // 2, axis=0), zero_value)
    send_rows = send_rows.reshape(experts, capacity, model_width)
    send_grads = jnp.where(present, jnp.take(pair_grad, picked, axis=0), zero_value)
    send_grads = send_grads.reshape(experts, capacity, model_width)
    routed_rows, routed_grads = in_one_piece((send_rows, send_grads), SP, 0, 0, 1)
    routed_rows = routed_rows.reshape(experts * capacity, model_width)
    routed_grads = routed_grads.reshape(experts * capacity, model_width)
    gate_part, up_part, down_part, back_rows = expert_local(
        routed_rows, routed_grads, gate_weight[0], up_weight[0], down_weight[0]
    )
    shares = sent_and_summed(back_rows.reshape(experts, capacity, model_width), "tp", 2)
    shares = lax.all_to_all(
        shares.astype(jnp.bfloat16), SP, split_axis=0, concat_axis=0, tiled=True
    )
    returned = collect(shares, "tp", 2)
    returned = returned.reshape(experts * capacity, model_width)
    per_pair = (
        jnp.take(returned, destination, axis=0)
        .reshape(tokens_here, 2, model_width)
        .astype(jnp.float32)
    )
    resid_grad = (out_grad.astype(jnp.float32) + per_pair[:, 0] + per_pair[:, 1]).astype(
        jnp.bfloat16
    )
    heads_local = queries.shape[1]
    key_width = queries.shape[2]
    value_width = value_vectors.shape[2]
    key_scale = key_width ** (-0.5)
    cosines, sines = rotation_tables(lax.axis_index(SP) * tokens_here, tokens_here, key_width)
    query_rotated = turn(queries.astype(jnp.float32), cosines, sines).transpose(1, 0, 2)
    key_rotated = (turn(key_vectors.astype(jnp.float32), cosines, sines) * key_scale).transpose(
        1, 0, 2
    )
    value_per_head = value_vectors.astype(jnp.float32).transpose(1, 0, 2)
    running_total = jnp.cumsum(log_decay, axis=0).T
    block_total = running_total[:, -1]
    causal = (jnp.arange(tokens_here)[:, None] >= jnp.arange(tokens_here)[None, :])[None]
    difference = running_total[:, :, None] - running_total[:, None, :]
    decay_mask = jnp.where(causal, jnp.exp(jnp.where(causal, difference, 0.0)), 0.0)
    per_head_decay = jnp.exp(running_total)
    remaining_decay = jnp.exp(block_total[:, None] - running_total)
    carried = jnp.exp(block_total)
    inner_state = jnp.einsum(
        "wfs,wfi->wsi",
        key_rotated * remaining_decay[..., None],
        value_per_head,
        precision=TOP_PRECISION,
    )
    identity = (jnp.ones_like(carried), jnp.zeros_like(inner_state))
    incoming_state = prefix_by_axis((carried, inner_state), SP, decay_combine, identity)[1]
    weights = (
        jnp.einsum("hik,hjk->hij", query_rotated, key_rotated, precision=TOP_PRECISION) * decay_mask
    )
    retained_output = jnp.einsum("hij,hjv->hiv", weights, value_per_head, precision=TOP_PRECISION)
    retained_output = retained_output + per_head_decay[..., None] * jnp.einsum(
        "dzr,drs->dzs", query_rotated, incoming_state, precision=TOP_PRECISION
    )
    inverse_rms = lax.rsqrt(
        jnp.mean(retained_output * retained_output, axis=-1, keepdims=True) + EPSILON
    )
    normed = retained_output * inverse_rms
    normed_bf = (
        normed.transpose(1, 0, 2)
        .reshape(tokens_here, heads_local * value_width)
        .astype(jnp.bfloat16)
    )
    proj_grad = summed_rows(
        lax.dot_general(
            resid_grad, normed_bf, (((0,), (0,)), ((), ())), preferred_element_type=jnp.float32
        ),
        SP,
    )
    normed_grad = jnp.dot(resid_grad, out_proj, preferred_element_type=jnp.float32)
    normed_grad = normed_grad.reshape(tokens_here, heads_local, value_width).transpose(1, 0, 2)
    retention_gradient = inverse_rms * (
        normed_grad - normed * jnp.mean(normed_grad * normed, axis=-1, keepdims=True)
    )
    inner_gradient = jnp.einsum(
        "gwn,gwj->gnj",
        query_rotated * per_head_decay[..., None],
        retention_gradient,
        precision=TOP_PRECISION,
    )
    future_gradient = prefix_by_axis_2((carried, inner_gradient), SP, decay_combine, identity)[1]
    score_grad = (
        jnp.einsum("hiv,hjv->hij", retention_gradient, value_per_head, precision=TOP_PRECISION)
        * decay_mask
    )
    query_portion = jnp.einsum("hij,hjk->hik", score_grad, key_rotated, precision=TOP_PRECISION)
    query_portion = query_portion + per_head_decay[..., None] * jnp.einsum(
        "bpl,btl->bpt", retention_gradient, incoming_state, precision=TOP_PRECISION
    )
    key_portion = jnp.einsum("hij,hik->hjk", score_grad, query_rotated, precision=TOP_PRECISION)
    key_portion = key_portion + remaining_decay[..., None] * jnp.einsum(
        "uxn,ubn->uxb", value_per_head, future_gradient, precision=TOP_PRECISION
    )
    value_portion = jnp.einsum("hij,hiv->hjv", weights, retention_gradient, precision=TOP_PRECISION)
    value_portion = value_portion + remaining_decay[..., None] * jnp.einsum(
        "bui,bim->bum", key_rotated, future_gradient, precision=TOP_PRECISION
    )
    query_grad = turn(query_portion.transpose(1, 0, 2), cosines, -sines).astype(jnp.bfloat16)
    key_grad = (turn(key_portion.transpose(1, 0, 2), cosines, -sines) * key_scale).astype(
        jnp.bfloat16
    )
    value_grad = value_portion.transpose(1, 0, 2).astype(jnp.bfloat16)
    return (
        gate_part[None],
        up_part[None],
        down_part[None],
        proj_grad,
        query_grad,
        key_grad,
        value_grad,
    )


def solution(mesh):
    split = Mesh(mesh.devices.reshape(8, 4, 2, mesh.shape["tp"]), ("sp_0", "sp_1", "sp_2", "tp"))
    placed = (
        P(SP, None),
        P(SP, None),
        P(SP, None),
        P(SP, None),
        P(SP, "tp", None),
        P(SP, "tp", None),
        P(SP, "tp", None),
        P(SP, "tp"),
        P(None, "tp"),
        P(SP, None, "tp"),
        P(SP, None, "tp"),
        P(SP, "tp", None),
    )
    return jax.shard_map(
        per_device,
        mesh=split,
        in_specs=placed,
        out_specs=(
            P(SP, None, "tp"),
            P(SP, None, "tp"),
            P(SP, "tp", None),
            P(SP, "tp"),
            P(SP, "tp", None),
            P(SP, "tp", None),
            P(SP, "tp", None),
        ),
        check_vma=False,
    )
```

profile of v0, /device:TPU:1, one launch (start us, length us, event | category | flops | bytes accessed | tf_op | source)
XLA Modules:
  0.0 402.8 jit_solution(11609621116955901032)
XLA Ops:
  10.3 1.4 scatter_custom_fusion
  12.0 3.4 mul.753
  15.4 3.7 mul.754
  19.5 3.3 gather_fusion
  22.8 1.8 multiply_convert_fusion
  24.6 3.3 gather_fusion.1
  27.9 2.5 fusion.4
  30.4 2.3 pad_maximum_fusion
  32.7 13.5 %all-to-all-start = ((bf16[64,16,2048]{2,1,0:T(8,128)(2,1)}), bf16[64,16,2048]{2,1,0:T(8,128)(2,1)}, u32[]{:S(2)}, u32[]{:S(2)}) async-start(bf16[64,16,2048]{2,1,0:T(8,128)(2,1)} %pad_maximum_fusion), calls=%async_computation | async-start | bytes 8388608 | tf_op jit(solution)/shard_map/all_to_all | solution.py:19
  48.3 2.6 all-reduce
  51.0 8.8 %all-gather.3 = bf16[4,1,2]{2,1,0:T(2,128)(2,1)S(1)} all-gather(bf16[1,1,2]{2,1,0:T(2,128)(2,1)S(1)} %convert_bitcast_fusion.12), channel_id=1, replica_groups=mesh['sp_0'=8,'sp_1'=4,'sp_2'=2,'tp'=4] {'sp_1'}, dimensions={0}, use_global_device_ids=true | all-gather | bytes 20 | tf_op jit(solution)/shard_map/all_gather | solution.py:68
  63.7 7.8 %all-gather = bf16[4,128,256]{2,1,0:T(8,128)(2,1)S(1)} all-gather(bf16[2,128,256]{2,1,0:T(8,128)(2,1)S(1)} %convolution_convert_fusion.4), channel_id=2, replica_groups=mesh['sp_0'=8,'sp_1'=4,'sp_2'=2,'tp'=4] {'sp_2'}, dimensions={0}, use_global_device_ids=true | all-gather | bytes 393216 | tf_op jit(solution)/shard_map/all_gather | solution.py:68
  71.5 69.4 %all-to-all-done = bf16[64,16,2048]{2,1,0:T(8,128)(2,1)} async-done(((bf16[64,16,2048]{2,1,0:T(8,128)(2,1)}), bf16[64,16,2048]{2,1,0:T(8,128)(2,1)}, u32[]{:S(2)}, u32[]{:S(2)}) %all-to-all-start) | async-done | bytes 4194336 | tf_op jit(solution)/shard_map/all_to_all | solution.py:19
  140.9 2.7 fusion.6
  143.6 2.5 fusion.7
  146.2 2.8 select_convert_fusion
  151.2 1.5 copy.218
  152.8 4.4 %all-to-all-start.1 = ((bf16[4,64,8,512]{3,2,1,0:T(8,128)(2,1)}), bf16[4,64,8,512]{3,2,1,0:T(8,128)(2,1)}, u32[]{:S(2)}, u32[]{:S(2)}) async-start(bf16[4,64,8,512]{3,2,1,0:T(8,128)(2,1)} %bitcast.511), calls=%async_computation.1 | async-start | bytes 4194304 | tf_op jit(solution)/shard_map/all_to_all | solution.py:36
  158.6 11.2 %all_gather.51 = bf16[4,2,128,256]{3,2,1,0:T(8,128)(2,1)S(1)} all-gather(bf16[1,2,128,256]{3,2,1,0:T(8,128)(2,1)S(1)} %fusion.64), channel_id=1, replica_groups=mesh['sp_0'=8,'sp_1'=4,'sp_2'=2,'tp'=4] {'sp_1'}, dimensions={0}, use_global_device_ids=true | all-gather | bytes 655360 | tf_op jit(solution)/shard_map/all_gather | solution.py:68
  171.7 13.2 %all-gather.4 = bf16[8,1,2]{2,1,0:T(2,128)(2,1)S(1)} all-gather(bf16[1,1,2]{2,1,0:T(2,128)(2,1)S(1)} %get-tuple-element.85), channel_id=1, replica_groups=mesh['sp_0'=8,'sp_1'=4,'sp_2'=2,'tp'=4] {'sp_0'}, dimensions={0}, use_global_device_ids=true | all-gather | bytes 36 | tf_op jit(solution)/shard_map/all_gather | solution.py:68
  185.1 2.9 reduce_sum.46
  188.0 10.8 %all-to-all-start.2 = ((bf16[64,8,512]{2,1,0:T(8,128)(2,1)}), bf16[64,8,512]{2,1,0:T(8,128)(2,1)S(1)}, u32[]{:S(2)}, u32[]{:S(2)}) async-start(bf16[64,8,512]{2,1,0:T(8,128)(2,1)} %reduce_sum.46), calls=%async_computation.2 | async-start | bytes 1048576 | tf_op jit(solution)/shard_map/all_to_all | solution.py:227
  200.1 1.2 compare_and_fusion
  201.9 1.5 subtract_exponential_fusion
  203.4 14.6 %all-to-all-done.2 = bf16[64,8,512]{2,1,0:T(8,128)(2,1)S(1)} async-done(((bf16[64,8,512]{2,1,0:T(8,128)(2,1)}), bf16[64,8,512]{2,1,0:T(8,128)(2,1)S(1)}, u32[]{:S(2)}, u32[]{:S(2)}) %all-to-all-start.2) | async-done | bytes 524320 | tf_op jit(solution)/shard_map/all_to_all | solution.py:227
  218.0 1.5 broadcast_in_dim.177
  219.6 4.6 %all-to-all-start.3 = ((bf16[4,64,8,512]{3,2,1,0:T(8,128)(2,1)}), bf16[4,64,8,512]{3,2,1,0:T(8,128)(2,1)}, u32[]{:S(2)}, u32[]{:S(2)}) async-start(bf16[4,64,8,512]{3,2,1,0:T(8,128)(2,1)} %broadcast_in_dim.177), calls=%async_computation.3 | async-start | bytes 4194304 | tf_op jit(solution)/shard_map/all_to_all | solution.py:42
  226.9 2.0 fusion.34
  229.2 1.6 multiply_reduce_fusion
  233.0 17.1 %all-to-all-done.3 = bf16[4,64,8,512]{3,2,1,0:T(8,128)(2,1)} async-done(((bf16[4,64,8,512]{3,2,1,0:T(8,128)(2,1)}), bf16[4,64,8,512]{3,2,1,0:T(8,128)(2,1)}, u32[]{:S(2)}, u32[]{:S(2)}) %all-to-all-start.3) | async-done | bytes 2097184 | tf_op jit(solution)/shard_map/all_to_all | solution.py:42
  250.1 3.3 copy.165
  253.4 4.4 %gather_fusion.2 = bf16[256,2048]{1,0:T(8,128)(2,1)S(1)} fusion(bf16[512,2048]{1,0:T(8,128)(2,1)} %bitcast.510, s32[1024]{0:T(1024)} %pad_clamp_fusion), kind=kCustom, calls=%fused_computation.2 | custom fusion | bytes 2098176 | tf_op jit(solution)/shard_map/jit(_take)/gather | solution.py:233
  257.8 1.5 gather.23
  259.3 2.0 fusion.24
  262.1 2.7 fusion.162
  265.5 12.7 %all-gather.5 = bf16[8,1,2]{2,1,0:T(2,128)(2,1)S(1)} all-gather(bf16[1,1,2]{2,1,0:T(2,128)(2,1)S(1)} %copy-done.49), channel_id=1, replica_groups=mesh['sp_0'=8,'sp_1'=4,'sp_2'=2,'tp'=4] {'sp_0'}, dimensions={0}, use_global_device_ids=true | all-gather | bytes 36 | tf_op jit(solution)/shard_map/all_gather | solution.py:95
  280.0 1.6 fusion.163
  283.6 6.2 %all-gather.2 = bf16[4,128,256]{2,1,0:T(8,128)(2,1)S(1)} all-gather(bf16[2,128,256]{2,1,0:T(8,128)(2,1)S(1)} %convolution_convert_fusion.3), channel_id=4, replica_groups=mesh['sp_0'=8,'sp_1'=4,'sp_2'=2,'tp'=4] {'sp_2'}, dimensions={0}, use_global_device_ids=true | all-gather | bytes 393216 | tf_op jit(solution)/shard_map/all_gather | solution.py:95
  290.5 11.1 %all_gather.57 = bf16[4,2,128,256]{3,2,1,0:T(8,128)(2,1)S(1)} all-gather(bf16[1,2,128,256]{3,2,1,0:T(8,128)(2,1)S(1)} %fusion.68), channel_id=1, replica_groups=mesh['sp_0'=8,'sp_1'=4,'sp_2'=2,'tp'=4] {'sp_1'}, dimensions={0}, use_global_device_ids=true | all-gather | bytes 655360 | tf_op jit(solution)/shard_map/all_gather | solution.py:95
  301.6 1.5 fusion.52
  303.2 3.4 fusion
  306.5 3.4 fusion.1
  310.0 3.5 fusion.2
  317.4 1.9 convolution_bitcast_fusion.4
  319.2 30.7 %all-gather.11.cloned.1.call-done = bf16[8,2,128,256]{3,2,1,0:T(8,128)(2,1)} async-done(((bf16[1,2,128,256]{3,2,1,0:T(8,128)(2,1)}), bf16[8,2,128,256]{3,2,1,0:T(8,128)(2,1)}) %all-gather.11.cloned.1.call-update) | async-done | bytes 1048592 | tf_op jit(solution)/shard_map/all_gather | solution.py:95
  350.0 2.0 fusion.31
  354.5 23.2 %reduce-scatter.6.cloned.1.call-done = f32[64,512]{1,0:T(8,128)} async-done(((f32[256,512]{1,0:T(8,128)}), f32[64,512]{1,0:T(8,128)}) %reduce-scatter.6.cloned.1.call-update) | async-done | bytes 131088 | tf_op jit(solution)/shard_map/reduce_scatter | solution.py:85
  380.5 15.8 %reduce-scatter.8.cloned.1.call-done = f32[32,512]{1,0:T(8,128)} async-done(((f32[64,512]{1,0:T(8,128)}), f32[32,512]{1,0:T(8,128)}) %reduce-scatter.8.cloned.1.call-update) | async-done | bytes 65552 | tf_op jit(solution)/shard_map/reduce_scatter | solution.py:85
  (218 shorter events, 36.6 us)
Async XLA Ops:
  7.2 272.8 %copy-start = (bf16[2048,512]{1,0:T(8,128)(2,1)S(1)}, bf16[2048,512]{1,0:T(8,128)(2,1)}, u32[]{:S(2)}) copy-start(bf16[2048,512]{1,0:T(8,128)(2,1)} %param.20) | copy-start | bytes 6291460
  15.4 3.7 copy-start.50
  15.4 4.1 %copy-start.1 = (bf16[128,2048]{1,0:T(8,128)(2,1)S(1)}, bf16[128,2048]{1,0:T(8,128)(2,1)}, u32[]{:S(2)}) copy-start(bf16[128,2048]{1,0:T(8,128)(2,1)} %param.12) | copy-start | bytes 1572868
  32.7 13.5 %copy-start.51 = (f32[128,2]{0,1:T(2,128)S(1)}, f32[128,2]{0,1:T(2,128)}, u32[]{:S(2)}) copy-start(f32[128,2]{0,1:T(2,128)} %param.19) | copy-start | bytes 3076
  32.7 13.9 %copy-start.53 = (u32[256]{0:T(256)S(1)}, u32[256]{0:T(256)}, u32[]{:S(2)}) copy-start(u32[256]{0:T(256)} %constant.149) | copy-start | bytes 3076
  32.7 27.1 %copy-start.28 = (bf16[128,2,128]{2,1,0:T(2,128)(2,1)S(1)}, bf16[128,2,128]{2,1,0:T(2,128)(2,1)}, u32[]{:S(2)}) copy-start(bf16[128,2,128]{2,1,0:T(2,128)(2,1)} %param.16) | copy-start | bytes 196612
  32.7 27.3 %copy-start.29 = (bf16[128,2,128]{2,1,0:T(2,128)(2,1)S(1)}, bf16[128,2,128]{2,1,0:T(2,128)(2,1)}, u32[]{:S(2)}) copy-start(bf16[128,2,128]{2,1,0:T(2,128)(2,1)} %param.17) | copy-start | bytes 196612
  32.7 108.2 %all-to-all-start = ((bf16[64,16,2048]{2,1,0:T(8,128)(2,1)}), bf16[64,16,2048]{2,1,0:T(8,128)(2,1)}, u32[]{:S(2)}, u32[]{:S(2)}) async-start(bf16[64,16,2048]{2,1,0:T(8,128)(2,1)} %pad_maximum_fusion), calls=%async_computation | async-start | bytes 8388608 | tf_op jit(solution)/shard_map/all_to_all | solution.py:19
  46.2 17.1 %copy-start.6 = (bf16[128,2,256]{2,1,0:T(2,128)(2,1)S(1)}, bf16[128,2,256]{2,1,0:T(2,128)(2,1)}, u32[]{:S(2)}) copy-start(bf16[128,2,256]{2,1,0:T(2,128)(2,1)} %param.18) | copy-start | bytes 393220
  46.5 14.9 %copy-start.18 = (f32[128,2]{1,0:T(8,128)}, f32[128,2]{1,0:T(8,128)S(1)}, u32[]{:S(2)}) copy-start(f32[128,2]{1,0:T(8,128)S(1)} %reduce_window_sum.28) | copy-start | bytes 3076
  46.6 16.7 %copy-start.30 = (f32[128,2]{0,1:T(2,128)}, f32[128,2]{0,1:T(2,128)S(1)}, u32[]{:S(2)}) copy-start(f32[128,2]{0,1:T(2,128)S(1)} %copy.172) | copy-start | bytes 3076
  62.4 81.2 %copy-start.11 = (f32[128,2,64,2]{0,3,2,1:T(2,128)}, f32[128,2,64,2]{0,3,2,1:T(2,128)S(1)}, u32[]{:S(2)}) copy-start(f32[128,2,64,2]{0,3,2,1:T(2,128)S(1)} %get-tuple-element.105) | copy-start | bytes 393220
  152.8 32.3 %all-to-all-start.1 = ((bf16[4,64,8,512]{3,2,1,0:T(8,128)(2,1)}), bf16[4,64,8,512]{3,2,1,0:T(8,128)(2,1)}, u32[]{:S(2)}, u32[]{:S(2)}) async-start(bf16[4,64,8,512]{3,2,1,0:T(8,128)(2,1)} %bitcast.511), calls=%async_computation.1 | async-start | bytes 4194304 | tf_op jit(solution)/shard_map/all_to_all | solution.py:36
  157.2 69.6 %all-gather.9.cloned.1.call-start = ((), (), s32[]{:S(2)}) async-start(), calls=%async_computation.7 | async-start | bytes 1179648 | tf_op jit(solution)/shard_map/all_gather | solution.py:68
  157.8 30.2 %copy-start.44 = (f32[2]{0:T(128)}, f32[2]{0:T(128)S(1)}, u32[]{:S(2)}) copy-start(f32[2]{0:T(128)S(1)} %get-tuple-element.102) | copy-start | bytes 28
  158.5 13.2 %copy-start.42 = (f32[2]{0:T(128)}, f32[2]{0:T(128)S(1)}, u32[]{:S(2)}) copy-start(f32[2]{0:T(128)S(1)} %get-tuple-element.83) | copy-start | bytes 28
  158.5 29.5 %copy-start.43 = (f32[2]{0:T(128)}, f32[2]{0:T(128)S(1)}, u32[]{:S(2)}) copy-start(f32[2]{0:T(128)S(1)} %get-tuple-element.99) | copy-start | bytes 28
  188.0 30.0 %all-to-all-start.2 = ((bf16[64,8,512]{2,1,0:T(8,128)(2,1)}), bf16[64,8,512]{2,1,0:T(8,128)(2,1)S(1)}, u32[]{:S(2)}, u32[]{:S(2)}) async-start(bf16[64,8,512]{2,1,0:T(8,128)(2,1)} %reduce_sum.46), calls=%async_computation.2 | async-start | bytes 1048576 | tf_op jit(solution)/shard_map/all_to_all | solution.py:227
  219.6 4.9 %copy-start.47 = (s32[256,1]{0,1:T(1,128)S(1)}, s32[256,1]{0,1:T(1,128)}, u32[]{:S(2)}) copy-start(s32[256,1]{0,1:T(1,128)} %copy-done.46) | copy-start | bytes 3076
  219.6 5.5 %copy-start.10 = (f32[128,2,64,2]{0,3,2,1:T(2,128)S(1)}, f32[128,2,64,2]{0,3,2,1:T(2,128)}, u32[]{:S(2)}) copy-start(f32[128,2,64,2]{0,3,2,1:T(2,128)} %get-tuple-element.104) | copy-start | bytes 393220
  219.6 5.6 %copy-start.24 = (f32[128,2]{1,0:T(8,128)S(1)}, f32[128,2]{1,0:T(8,128)}, u32[]{:S(2)}) copy-start(f32[128,2]{1,0:T(8,128)} %get-tuple-element.63) | copy-start | bytes 3076
  219.6 6.2 %copy-start.31 = (f32[128,2]{0,1:T(2,128)S(1)}, f32[128,2]{0,1:T(2,128)}, u32[]{:S(2)}) copy-start(f32[128,2]{0,1:T(2,128)} %copy-done.30) | copy-start | bytes 3076
  219.6 30.5 %all-to-all-start.3 = ((bf16[4,64,8,512]{3,2,1,0:T(8,128)(2,1)}), bf16[4,64,8,512]{3,2,1,0:T(8,128)(2,1)}, u32[]{:S(2)}, u32[]{:S(2)}) async-start(bf16[4,64,8,512]{3,2,1,0:T(8,128)(2,1)} %broadcast_in_dim.177), calls=%async_computation.3 | async-start | bytes 4194304 | tf_op jit(solution)/shard_map/all_to_all | solution.py:42
  224.2 5.1 %copy-start.7 = (bf16[128,2,256]{2,1,0:T(2,128)(2,1)S(1)}, bf16[128,2,256]{2,1,0:T(2,128)(2,1)}, u32[]{:S(2)}) copy-start(bf16[128,2,256]{2,1,0:T(2,128)(2,1)} %param.18) | copy-start | bytes 393220
  224.2 92.8 %reduce-scatter.4.cloned.1.call-start = ((), (), s32[]{:S(2)}) async-start(), calls=%async_computation.8 | async-start | bytes 4718592 | tf_op jit(solution)/shard_map/reduce_scatter | solution.py:85
  225.2 5.7 %copy-start.3 = (f32[128,2,128]{2,0,1:T(8,128)}, f32[128,2,128]{2,0,1:T(8,128)S(1)}, u32[]{:S(2)}) copy-start(f32[128,2,128]{2,0,1:T(8,128)S(1)} %copy.168) | copy-start | bytes 393220
  264.9 13.3 %copy-start.23 = (f32[128,2]{1,0:T(8,128)S(1)}, f32[128,2]{1,0:T(8,128)}, u32[]{:S(2)}) copy-start(f32[128,2]{1,0:T(8,128)} %get-tuple-element.62) | copy-start | bytes 3076
  264.9 17.8 %copy-start.2 = (f32[2,128,256]{2,1,0:T(8,128)S(1)}, f32[2,128,256]{2,1,0:T(8,128)}, u32[]{:S(2)}) copy-start(f32[2,128,256]{2,1,0:T(8,128)} %get-tuple-element.45) | copy-start | bytes 786436
  264.9 17.8 %copy-start.39 = (f32[2,128]{1,0:T(2,128)S(1)}, f32[2,128]{1,0:T(2,128)}, u32[]{:S(2)}) copy-start(f32[2,128]{1,0:T(2,128)} %get-tuple-element.95) | copy-start | bytes 3076
  264.9 85.0 %all-gather.11.cloned.1.call-start = ((), (), s32[]{:S(2)}) async-start(), calls=%async_computation.11 | async-start | bytes 1179648 | tf_op jit(solution)/shard_map/all_gather | solution.py:95
  280.0 3.1 copy-start.4
  280.0 3.1 copy-start.40
  303.1 74.6 %reduce-scatter.6.cloned.1.call-start = ((), (), s32[]{:S(2)}) async-start(), calls=%async_computation.9 | async-start | bytes 655360 | tf_op jit(solution)/shard_map/reduce_scatter | solution.py:85
  303.1 3.4 copy-start.27
  306.5 3.4 copy-start.55
  306.5 3.4 copy-start.57
  310.0 3.5 copy-start.8
  310.0 3.5 copy-start.32
  310.0 4.4 %copy-start.12 = (f32[128,2,64,2]{0,3,2,1:T(2,128)S(1)}, f32[128,2,64,2]{0,3,2,1:T(2,128)}, u32[]{:S(2)}) copy-start(f32[128,2,64,2]{0,3,2,1:T(2,128)} %copy-done.11) | copy-start | bytes 393220
  310.0 4.8 %copy-start.14 = (f32[2,128,128]{2,1,0:T(8,128)S(1)}, f32[2,128,128]{2,1,0:T(8,128)}, u32[]{:S(2)}) copy-start(f32[2,128,128]{2,1,0:T(8,128)} %convolution_multiply_fusion.1) | copy-start | bytes 393220
  310.0 5.9 %copy-start.37 = (f32[128,2]{0,1:T(2,128)S(1)}, f32[128,2]{0,1:T(2,128)}, u32[]{:S(2)}) copy-start(f32[128,2]{0,1:T(2,128)} %copy.174) | copy-start | bytes 3076
  313.8 36.2 %copy-start.34 = (f32[2]{0:T(128)S(1)}, f32[2]{0:T(128)}, u32[]{:S(2)}) copy-start(f32[2]{0:T(128)} %copy-done.33) | copy-start | bytes 28
  313.8 36.2 %copy-start.36 = (f32[2]{0:T(128)S(1)}, f32[2]{0:T(128)}, u32[]{:S(2)}) copy-start(f32[2]{0:T(128)} %copy-done.35) | copy-start | bytes 28
  313.8 36.2 %copy-start.41 = (f32[2]{0:T(128)S(1)}, f32[2]{0:T(128)}, u32[]{:S(2)}) copy-start(f32[2]{0:T(128)} %get-tuple-element.82) | copy-start | bytes 28
  314.8 37.2 %copy-start.38 = (f32[128,2]{0,1:T(2,128)S(1)}, f32[128,2]{0,1:T(2,128)}, u32[]{:S(2)}) copy-start(f32[128,2]{0,1:T(2,128)} %copy.184) | copy-start | bytes 3076
  317.0 79.3 %reduce-scatter.8.cloned.1.call-start = ((), (), s32[]{:S(2)}) async-start(), calls=%async_computation.10 | async-start | bytes 196608 | tf_op jit(solution)/shard_map/reduce_scatter | solution.py:85
  319.2 60.1 %copy-start.15 = (f32[128,2,256]{2,0,1:T(8,128)S(1)}, f32[128,2,256]{2,0,1:T(8,128)}, u32[]{:S(2)}) copy-start(f32[128,2,256]{2,0,1:T(8,128)} %convolution_bitcast_fusion.1) | copy-start | bytes 786436
  350.0 3.2 copy-start.21
  (19 other events, 29.9 us)
Sparse Core Ops, SparseCore 0:
  171.3 35.3 all-gather.8
  265.0 50.9 reduce-scatter.3
  317.9 32.0 all-gather.10
  352.4 25.2 reduce-scatter.5
  380.6 15.6 reduce-scatter.7
where the time goes:
time: 404 us; the launch traced here: 403 us
  waiting for transfers between devices  171 us (42%)
  blocking collectives  73.6 us (18%)
  local copies, waits for them, and re-layouts  39.3 us (10%)
  other arithmetic  35.3 us (9%)
  matrix products  34.4 us (9%)
  starting transfers between devices  34 us (8%)
  between operations  15.3 us (4%)
    all_to_all x1, waiting for transfers between devices, in_one_piece(): lax.all_to_all(both, axis, split_axis=split_dim, concat_axis=concat_dim,...  69.4 us
    all_gather x4, blocking collectives, prefix_by_axis(): lax.all_gather(part.astype(kind), axis)  41 us
    reduce_scatter x3, waiting for transfers between devices, summed_rows(): total = lax.psum_scatter(total, axis, scatter_dimension=0, tiled=True)  39 us
    all_gather x1, waiting for transfers between devices, prefix_by_axis_2(): lax.all_gather(part.astype(kind), axis)  30.7 us
    all_gather x3, blocking collectives, prefix_by_axis_2(): lax.all_gather(part.astype(kind), axis)  29.9 us
    all_to_all x1, waiting for transfers between devices, copy_for_each(): return lax.all_to_all(copies, axis, split_axis=0, concat_axis=0, tiled=True)  17.1 us
    all_to_all x1, waiting for transfers between devices, per_device(): lax.all_to_all(shares.astype(jnp.bfloat16), SP, split_axis=0, concat_axis...  14.6 us
    all_to_all x1, starting transfers between devices, in_one_piece(): lax.all_to_all(both, axis, split_axis=split_dim, concat_axis=concat_dim,...  13.5 us
  transfers between devices with their start and end apart: 9, of which 6 were waited for; matrix products, arithmetic and copies ran while one was open for 14% of the time, Pallas kernels for 0%

commit v1 on v0

v1 whole, which is shorter than its diff:
```python
import functools

import jax
import jax.numpy as jnp
import numpy as np
from jax import lax
from jax.experimental import pallas as pl
from jax.experimental.pallas import tpu as pltpu
from jax.sharding import Mesh
from jax.sharding import PartitionSpec as P

SP = ("sp_0", "sp_1", "sp_2")
YC = ("sp_1", "sp_2")
ZAX = "sp_0"
TP = "tp"

CLAMP_LIMIT = 7.0
GATE_SLOPE = 1.702
EPSILON = 1e-06
HI = lax.Precision.HIGHEST
F32 = jnp.float32
BF = jnp.bfloat16

NN = (((1,), (0,)), ((), ()))
NT = (((1,), (1,)), ((), ()))
TN = (((0,), (0,)), ((), ()))


def mm(a, b, dims=NN):
    return lax.dot_general(a, b, dims, preferred_element_type=F32)


def mmh(a, b, dims=NN):
    return lax.dot_general(a, b, dims, precision=HI, preferred_element_type=F32)


def iota(shape, dim):
    return lax.broadcasted_iota(jnp.int32, shape, dim)


def whole(shape):
    return pl.BlockSpec(shape, lambda i, q: (0,) * len(shape))


def call(name, body, q, args, outs, in_specs=None, out_specs=None, grid=1, flops=0):
    in_specs = in_specs or {}
    out_specs = out_specs or {}
    return pl.pallas_call(
        body,
        out_shape=[jax.ShapeDtypeStruct(s, d) for s, d in outs],
        grid_spec=pltpu.PrefetchScalarGridSpec(
            num_scalar_prefetch=1,
            grid=(grid,),
            in_specs=[in_specs.get(i, whole(a.shape)) for i, a in enumerate(args)],
            out_specs=[out_specs.get(i, whole(s)) for i, (s, _) in enumerate(outs)],
        ),
        cost_estimate=pl.CostEstimate(flops=flops, bytes_accessed=0, transcendentals=0) if flops else None,
        name=name,
    )(q, *args)


def dispatch_body(q, routes, rw, stream, og, rows, grads, qt):
    n = routes.shape[0]
    slots = rows.shape[0]
    r = routes[...].astype(F32)
    w = rw[...]
    ti, tj = iota((n, n), 0), iota((n, n), 1)
    eye = ti == tj
    before = ti < tj

    def row(c):
        return jnp.sum(jnp.where(eye, c, 0.0), axis=0, keepdims=True)

    def col(c):
        return jnp.sum(jnp.where(eye, c, 0.0), axis=1, keepdims=True)

    e0, e1 = r[:, 0:1], r[:, 1:2]
    e0r, e1r = row(e0), row(e1)
    w0r, w1r = row(w[:, 0:1]), row(w[:, 1:2])

    def earlier(er):
        same = (e0 == er).astype(F32) + (e1 == er).astype(F32)
        return jnp.sum(jnp.where(before, same, 0.0), axis=0, keepdims=True)

    cap = slots // 64
    d0 = e0r * cap + earlier(e0r)
    d1 = e1r * cap + earlier(e1r) + (e0r == e1r).astype(F32)
    di = iota((slots, n), 0).astype(F32)
    q0, q1 = di == d0, di == d1
    weight = jnp.sum(jnp.where(q0, w0r, 0.0) + jnp.where(q1, w1r, 0.0), axis=1, keepdims=True)
    pick = (jnp.where(q0, 1.0, 0.0) + jnp.where(q1, 1.0, 0.0)).astype(BF)
    rows[...] = mm(pick, stream[...]).astype(BF)
    grads[...] = (mm(pick, og[...]) * weight).astype(BF)
    dl = iota((n, slots), 1).astype(F32)
    qt[0:n, :] = jnp.where(dl == col(d0), 1.0, 0.0).astype(BF)
    qt[n : 2 * n, :] = jnp.where(dl == col(d1), 1.0, 0.0).astype(BF)


def combine_body(q, ret, qt, og, resid):
    n = og.shape[0]
    back = mm(qt[...], ret[...])
    resid[...] = ((og[...].astype(F32) + back[0:n]) + back[n : 2 * n]).astype(BF)


def gate_up_body(q, r0, r1, r2, r3, g0, g1, g2, g3, u0, u1, u2, u3, act, ga, ua):
    rows = (r0, r1, r2, r3)
    gate = mm(r0[...], g0[...])
    up = mm(r0[...], u0[...])
    for r, g, u in zip(rows[1:], (g1, g2, g3), (u1, u2, u3)):
        x = r[...]
        gate = gate + mm(x, g[...])
        up = up + mm(x, u[...])
    gc = jnp.minimum(gate, CLAMP_LIMIT)
    uc = jnp.clip(up, -CLAMP_LIMIT, CLAMP_LIMIT)
    sig = 1.0 / (1.0 + jnp.exp(-GATE_SLOPE * gc))
    gs = gc * sig
    act[...] = (gs * (uc + 1.0)).astype(BF)
    slope = sig + GATE_SLOPE * gs * (1.0 - sig)
    ga[...] = jnp.where(gate < CLAMP_LIMIT, (uc + 1.0) * slope, 0.0)
    ua[...] = jnp.where(jnp.abs(up) < CLAMP_LIMIT, gs, 0.0)


def expert_back_body(
    q, x0, x1, x2, x3, d0, d1, d2, d3, g0, g1, g2, g3, u0, u1, u2, u3, ga, ua, gp, up, b0, b1, b2, b3
):
    act_grad = mm(x0[...], d0[...], NT)
    for x, d in zip((x1, x2, x3), (d1, d2, d3)):
        act_grad = act_grad + mm(x[...], d[...], NT)
    gpg = (act_grad * ga[...]).astype(BF)
    upg = (act_grad * ua[...]).astype(BF)
    gp[...] = gpg
    up[...] = upg
    for b, g, u in zip((b0, b1, b2, b3), (g0, g1, g2, g3), (u0, u1, u2, u3)):
        b[...] = (mm(gpg, g[...], NT) + mm(upg, u[...], NT)).astype(BF)


def weight_grads_body(q, r0, r1, r2, r3, x0, x1, x2, x3, gp, up, act, gw, uw, dw):
    step = pl.program_id(0)
    for k, (r, x) in enumerate(zip((r0, r1, r2, r3), (x0, x1, x2, x3))):

        @pl.when(step == k)
        def _(r=r, x=x):
            rt = r[...]
            gw[...] = mm(rt, gp[...], TN).astype(BF)
            uw[...] = mm(rt, up[...], TN).astype(BF)
            dw[...] = mm(act[...], x[...], TN).astype(BF)


def turned(x, c, s):
    even = (iota(x.shape, 1) % 2) == 0
    n = x.shape[1]
    other = jnp.where(even, -pltpu.roll(x, n - 1, 1), pltpu.roll(x, 1, 1))
    return x * c + other * s


def prepare_body(
    q, qv, kv, vv, ld, cb, sb, cr, sr, send, qr, kr, qdt, wts, dm, dec, rem, intra, cs, sn
):
    heads, n, kd = qv.shape
    vd = vv.shape[2]
    ti, tj = iota((n, n), 0), iota((n, n), 1)
    eye, causal = ti == tj, ti >= tj
    c = cb[...] * cr[...] - sb[...] * sr[...]
    s = sb[...] * cr[...] + cb[...] * sr[...]
    cs[...] = c
    sn[...] = s
    pieces = []
    extra = []
    for h in range(heads):
        col = ld[:, h : h + 1]
        rt_r = jnp.sum(jnp.where(ti <= tj, col, 0.0), axis=0, keepdims=True)
        rt_c = jnp.sum(jnp.where(eye, rt_r, 0.0), axis=1, keepdims=True)
        total = rt_r[:, n - 1 : n]
        mask = jnp.where(causal, jnp.exp(jnp.where(causal, rt_c - rt_r, 0.0)), 0.0)
        grow = jnp.exp(rt_c)
        left = jnp.exp(total - rt_c)
        qh = turned(qv[h].astype(F32), c, s)
        kh = turned(kv[h].astype(F32), c, s) * (kd**-0.5)
        vh = vv[h].astype(F32)
        inner = mmh((kh * left).T, vh)
        for u in range(vd // 128):
            pieces.append(inner[:, u * 128 : (u + 1) * 128])
        hi = total.astype(BF).astype(F32)
        mid = (total - hi).astype(BF).astype(F32)
        low = total - hi - mid
        sub = iota((16 * vd // 128, 8, 128), 1)
        extra.append(
            jnp.where(sub == 0, hi[None], jnp.where(sub == 1, mid[None], jnp.where(sub == 2, low[None], 0.0)))
        )
        w = mmh(qh, kh, NT) * mask
        intra[:, h * vd : (h + 1) * vd] = mmh(w, vh)
        qr[h] = qh
        kr[h] = kh
        qdt[h] = (qh * grow).T
        wts[h] = w
        dm[h] = mask
        dec[h] = jnp.broadcast_to(grow, (n, 128))
        rem[h] = jnp.broadcast_to(left, (n, 128))
    state = jnp.concatenate(pieces, axis=0).reshape(-1, 8, 128)
    send[...] = jnp.concatenate([state, jnp.concatenate(extra, axis=0)], axis=1).astype(BF)


def split3(x):
    hi = x.astype(BF)
    mid = (x - hi.astype(F32)).astype(BF)
    return hi, mid


def prefix_body(q, x, out, whi, wmid):
    n = x.shape[0]
    xf = x[...].astype(F32)
    logs = (xf[:, 8, :] + xf[:, 9, :] + xf[:, 10, :])[:, 0:1]
    ti, tj = iota((n, n), 0), iota((n, n), 1)
    after = jnp.where(ti > tj, logs, 0.0)
    earlier = jnp.where(tj < ti, 1.0, 0.0)
    seg = mmh(earlier, after)
    w = jnp.where(tj < ti, jnp.exp(seg), 0.0)
    big = 8 * n
    expand = jnp.where(iota((big, n), 0) // 8 == iota((big, n), 1), 1.0, 0.0)
    same = (iota((big, big), 0) % 8) == (iota((big, big), 1) % 8)
    fwd = jnp.where(same, mmh(mmh(expand, w), expand, NT), 0.0)
    bwd = jnp.where(same, mmh(mmh(expand, w, NT), expand, NT), 0.0)
    xs = xf[:, 0:8, :].reshape(big, 128).astype(BF)
    fhi, fmid = split3(fwd)
    out[...] = (mm(fhi, xs) + mm(fmid, xs)).astype(BF)
    bhi, bmid = split3(bwd)
    whi[...] = bhi
    wmid[...] = bmid


def suffix_body(q, x, whi, wmid, out):
    xs = x[...]
    out[...] = (mm(whi[...], xs) + mm(wmid[...], xs)).astype(BF)


def joined(state, h, vd):
    per = vd // 128
    base = h * per * 128
    return jnp.concatenate([state[base + u * 128 : base + (u + 1) * 128, :] for u in range(per)], axis=1)


def normed_body(q, state, qr, dec, intra, normed, nbf, inv):
    heads = qr.shape[0]
    vd = intra.shape[1] // heads
    st = state[...].astype(F32)
    for h in range(heads):
        sl = slice(h * vd, (h + 1) * vd)
        ret = intra[:, sl] + dec[h][:, 0:1] * mmh(qr[h], joined(st, h, vd))
        iv = lax.rsqrt(jnp.mean(ret * ret, axis=1, keepdims=True) + EPSILON)
        nm = ret * iv
        normed[:, sl] = nm
        nbf[:, sl] = nm.astype(BF)
        inv[h] = jnp.broadcast_to(iv, inv.shape[1:])


def inner_grad_body(q, r0, r1, r2, r3, p0, p1, p2, p3, normed, inv, qdt, rg, send):
    heads = qdt.shape[0]
    vd = normed.shape[1] // heads
    ng = mm(r0[...], p0[...])
    for r, p in zip((r1, r2, r3), (p1, p2, p3)):
        ng = ng + mm(r[...], p[...])
    for h in range(heads):
        sl = slice(h * vd, (h + 1) * vd)
        nm, g = normed[:, sl], ng[:, sl]
        m = jnp.mean(g * nm, axis=1, keepdims=True)
        grad = inv[h][:, 0:1] * (g - nm * m)
        rg[:, sl] = grad
        inner = mmh(qdt[h], grad)
        for u in range(vd // 128):
            base = (h * (vd // 128) + u) * 128
            send[base : base + 128, :] = inner[:, u * 128 : (u + 1) * 128].astype(BF)


def transpose_body(q, r0, r1, r2, r3, out):
    for k, r in enumerate((r0, r1, r2, r3)):
        block = (q[0] + k) % 4
        t = r[...].astype(F32).T.astype(BF)
        for lo in range(2):
            at = pl.multiple_of((block * 2 + lo) * 32, 32)
            for j in range(8):
                src = lo * 256 + j * 32
                out[j, pl.ds(at, 32), :] = t[src : src + 32, :]


def local_grads_body(q, rg, vv, dm, qr, kr, wts, dec, state, cs, sn, qg, kp, vp):
    heads = qr.shape[0]
    vd = vv.shape[2]
    st = state[...].astype(F32)
    c, s = cs[...], sn[...]
    for h in range(heads):
        grad = rg[:, h * vd : (h + 1) * vd]
        score = mmh(grad, vv[h].astype(F32), NT) * dm[h]
        qp = mmh(score, kr[h]) + dec[h][:, 0:1] * mmh(grad, joined(st, h, vd), NT)
        qg[h] = turned(qp, c, -s).astype(BF)
        kp[h] = mmh(score.T, qr[h])
        vp[h] = mmh(wts[h].T, grad)


def final_body(q, state, vv, kr, rem, kp, vp, cs, sn, kg, vg):
    heads, n, kd = kr.shape
    vd = vv.shape[2]
    st = state[...].astype(F32)
    c, s = cs[...], sn[...]
    for h in range(heads):
        fut = joined(st, h, vd)
        left = rem[h][:, 0:1]
        kt = kp[h] + left * mmh(vv[h].astype(F32), fut, NT)
        kg[h] = (turned(kt, c, -s) * (kd**-0.5)).astype(BF)
        vg[h] = (vp[h] + left * mmh(kr[h], fut)).astype(BF)


def proj_body(q, rt, nb, out):
    acc = mm(rt[0], nb[0])
    for k in range(1, rt.shape[0]):
        acc = acc + mm(rt[k], nb[k])
    out[...] = acc.astype(BF)


def add_parts_body(q, x, out):
    acc = x[0].astype(F32)
    for k in range(1, x.shape[0]):
        acc = acc + x[k].astype(F32)
    out[...] = acc


def add4_body(q, a, b, c, d, out):
    out[...] = (
        (a[...].astype(F32) + b[...].astype(F32)) + (c[...].astype(F32) + d[...].astype(F32))
    ).astype(BF)


def a2a(x, axes):
    return lax.all_to_all(x, axes, split_axis=0, concat_axis=0, tiled=True)


def shift(x, by):
    return lax.ppermute(x, TP, [(i, (i + by) % 4) for i in range(4)])


def around(x):
    far = shift(x, 2)
    return x, shift(x, 3), far, shift(x, 1)


def around_ring(x):
    half = x.shape[0] // 2
    left, right = shift(x, 1), shift(x, 3)
    a, b = shift(left[:half], 1), shift(right[half:], 3)
    return x, right, jnp.concatenate([a, b], axis=0), left


def block_rows(k, shape):
    return pl.BlockSpec(shape, lambda i, q, k=k: (lax.rem(q[0] + k, 4), 0))


def block_cols(k, shape):
    return pl.BlockSpec(shape, lambda i, q, k=k: (0, lax.rem(q[0] + k, 4)))


def per_device(
    stream,
    out_grad,
    routes,
    route_weight,
    queries,
    key_vectors,
    value_vectors,
    log_decay,
    out_proj,
    gate_weight,
    up_weight,
    down_weight,
):
    n, width = stream.shape
    quarter = width // 4
    slots = 512
    hidden = gate_weight.shape[2]
    heads, kd = queries.shape[1:]
    vd = value_vectors.shape[2]
    q = lax.axis_index(TP).astype(jnp.int32)[None]
    gate_w, up_w, down_w = gate_weight[0], up_weight[0], down_weight[0]

    own = pl.BlockSpec((n, quarter), lambda i, q: (0, q[0]))
    rows, grads, qt = call(
        "dispatch",
        dispatch_body,
        q,
        (routes, route_weight, stream, out_grad),
        [((slots, quarter), BF), ((slots, quarter), BF), ((2 * n, slots), BF)],
        in_specs={2: own, 3: own},
    )
    rows = a2a(rows.reshape(64, 8, quarter), SP).reshape(slots, quarter)
    grads = a2a(grads.reshape(64, 8, quarter), SP).reshape(slots, quarter)
    rows4 = around(rows)
    grads4 = around(grads)

    freq = 1.0 / 10000.0 ** jnp.linspace(0.0, 1.0, kd // 2, dtype=F32)
    freq = jnp.repeat(freq, 2)[None, :]
    base = (lax.axis_index(SP) * n).astype(F32) * freq
    angles = jnp.arange(n, dtype=F32)[:, None] * freq
    qv = queries.transpose(1, 0, 2)
    kv = key_vectors.transpose(1, 0, 2)
    vv = value_vectors.transpose(1, 0, 2)
    sq = (heads, n, 128)
    send, qr, kr, qdt, wts, dm, dec, rem, intra, cs, sn = call(
        "prepare",
        prepare_body,
        q,
        (qv, kv, vv, log_decay, jnp.cos(base), jnp.sin(base), jnp.cos(angles), jnp.sin(angles)),
        [((64, 16, 128), BF)]
        + [(sq, F32)] * 7
        + [((n, heads * vd), F32), ((n, kd), F32), ((n, kd), F32)],
    )
    got = a2a(send, SP)
    state, whi, wmid = call(
        "prefix",
        prefix_body,
        q,
        (got,),
        [((slots, 128), BF), ((slots, slots), BF), ((slots, slots), BF)],
    )
    state = a2a(state.reshape(64, 8, 128), SP).reshape(slots, 128)
    normed, nbf, inv = call(
        "normed",
        normed_body,
        q,
        (state, qr, dec, intra),
        [((n, heads * vd), F32), ((n, heads * vd), BF), (sq, F32)],
    )
    nball = a2a(jnp.broadcast_to(nbf, (8, *nbf.shape)), YC)

    wrow = (quarter, hidden)
    gspec = {k: block_rows(k, wrow) for k in range(4)}
    dspec = {k: block_cols(k, (hidden, quarter)) for k in range(4)}
    act, ga, ua = call(
        "gate_up",
        gate_up_body,
        q,
        (*rows4, *[gate_w] * 4, *[up_w] * 4),
        [((slots, hidden), BF), ((slots, hidden), F32), ((slots, hidden), F32)],
        in_specs={4 + k: s for k, s in gspec.items()} | {8 + k: s for k, s in gspec.items()},
    )
    gp, up, *back = call(
        "expert_back",
        expert_back_body,
        q,
        (*grads4, *[down_w] * 4, *[gate_w] * 4, *[up_w] * 4, ga, ua),
        [((slots, hidden), BF)] * 2 + [((slots, quarter), BF)] * 4,
        in_specs={4 + k: s for k, s in dspec.items()}
        | {8 + k: s for k, s in gspec.items()}
        | {12 + k: s for k, s in gspec.items()},
    )
    far = shift(back[2], 2)
    nxt, prv = shift(back[1], 1), shift(back[3], 3)
    gate_grad, up_grad, down_grad = call(
        "weight_grads",
        weight_grads_body,
        q,
        (*rows4, *grads4, gp, up, act),
        [((width, hidden), BF), ((width, hidden), BF), ((hidden, width), BF)],
        out_specs={
            0: pl.BlockSpec(wrow, lambda i, q: (lax.rem(q[0] + i, 4), 0)),
            1: pl.BlockSpec(wrow, lambda i, q: (lax.rem(q[0] + i, 4), 0)),
            2: pl.BlockSpec((hidden, quarter), lambda i, q: (0, lax.rem(q[0] + i, 4))),
        },
        grid=4,
    )
    (share,) = call("add4", add4_body, q, (back[0], nxt, far, prv), [((slots, quarter), BF)])
    share = a2a(share.reshape(64, 8, quarter), SP).reshape(slots, quarter)
    (resid,) = call(
        "combine",
        combine_body,
        q,
        (share, qt, out_grad),
        [((n, quarter), BF)],
        in_specs={2: own},
    )
    resid4 = around(resid)

    pspec = {4 + k: block_rows(k, (quarter, out_proj.shape[1])) for k in range(4)}
    rg, inner = call(
        "inner_grad",
        inner_grad_body,
        q,
        (*resid4, *[out_proj] * 4, normed, inv, qdt),
        [((n, heads * vd), F32), ((slots, 128), BF)],
        in_specs=pspec,
    )
    inner = a2a(inner.reshape(64, 8, 128), SP).reshape(slots, 128)
    (turned_rows,) = call("transpose", transpose_body, q, resid4, [((8, 256, n), BF)])
    turned_rows = a2a(turned_rows, YC)
    (part,) = call("proj", proj_body, q, (turned_rows, nball), [((256, nbf.shape[1]), BF)])
    part = a2a(part.reshape(8, 32, nbf.shape[1]), ZAX)
    (proj_grad,) = call("add_parts", add_parts_body, q, (part,), [((32, nbf.shape[1]), F32)])
    qg, kp, vp = call(
        "local_grads",
        local_grads_body,
        q,
        (rg, vv, dm, qr, kr, wts, dec, state, cs, sn),
        [(sq, BF), (sq, F32), ((heads, n, vd), F32)],
    )
    (future,) = call("suffix", suffix_body, q, (inner, whi, wmid), [((slots, 128), BF)])
    future = a2a(future.reshape(64, 8, 128), SP).reshape(slots, 128)
    kg, vg = call(
        "final",
        final_body,
        q,
        (future, vv, kr, rem, kp, vp, cs, sn),
        [(sq, BF), ((heads, n, vd), BF)],
    )
    return (
        gate_grad[None],
        up_grad[None],
        down_grad[None],
        proj_grad,
        qg.transpose(1, 0, 2),
        kg.transpose(1, 0, 2),
        vg.transpose(1, 0, 2),
    )


def solution(mesh):
    split = Mesh(mesh.devices.reshape(8, 4, 2, mesh.shape["tp"]), (*SP, TP))
    placed = (
        P(SP, None),
        P(SP, None),
        P(SP, None),
        P(SP, None),
        P(SP, TP, None),
        P(SP, TP, None),
        P(SP, TP, None),
        P(SP, TP),
        P(None, TP),
        P(SP, None, TP),
        P(SP, None, TP),
        P(SP, TP, None),
    )
    return jax.shard_map(
        per_device,
        mesh=split,
        in_specs=placed,
        out_specs=(
            P(SP, None, TP),
            P(SP, None, TP),
            P(SP, TP, None),
            P(SP, TP),
            P(SP, TP, None),
            P(SP, TP, None),
            P(SP, TP, None),
        ),
        check_vma=False,
    )
```

time: 404 us -> 256 us (0.63)
  waiting for transfers between devices: 171 us -> 71.6 us
  Pallas kernels: 0 us -> 53.5 us
  starting transfers between devices: 34 us -> 79.1 us
  blocking collectives: 73.6 us -> 30.8 us
  matrix products: 34.4 us -> 0 us
  other arithmetic: 35.3 us -> 1.09 us
  local copies, waits for them, and re-layouts: 39.3 us -> 17.3 us
  between operations: 15.3 us -> 0.88 us
    all_gather x7 -> x0, blocking collectives: 71 us -> none  [the longest x4 41 us: prefix_by_axis(): lax.all_gather(part.astype(kind), axis)]
    pallas_call x0 -> x16, Pallas kernels: none -> 53.5 us  [call(): pl.pallas_call(body, out_shape=[jax.ShapeDtypeStruct(s, d) for s, d in ou...]
    all_to_all x4 -> x9, waiting for transfers between devices: 101 us -> 54.3 us  [a2a(): return lax.all_to_all(x, axes, split_axis=0, concat_axis=0, tiled=True)]
    reduce_scatter x3 -> x0, waiting for transfers between devices: 39 us -> none  [summed_rows(): total = lax.psum_scatter(total, axis, scatter_dimension=0, tiled=True)]
    dot_general x22 -> x0, matrix products: 34.4 us -> none  [the longest x1 3.45 us: expert_local(): lax.dot_general(activated, routed_grads, (((0,), (0,)), ((), ())), prefer...]
    all_to_all x4 -> x9, starting transfers between devices: 33.3 us -> 65.8 us  [a2a(): return lax.all_to_all(x, axes, split_axis=0, concat_axis=0, tiled=True)]
    all_to_all x0 -> x1, blocking collectives: none -> 30.8 us  [a2a(): return lax.all_to_all(x, axes, split_axis=0, concat_axis=0, tiled=True)]
    all_gather x2 -> x0, waiting for transfers between devices: 30.7 us -> none  [the longest x1 30.7 us: prefix_by_axis_2(): lax.all_gather(part.astype(kind), axis)]
  transfers between devices with their start and end apart: 9 -> 21, of which waited for: 6 -> 11; matrix products, arithmetic and copies ran while one was open for 14% -> 4% of each run, Pallas kernels for 0% -> 19%
where the time goes in v1:
time: 256 us; the launch traced here: 254 us
  starting transfers between devices  79.1 us (31%)
  waiting for transfers between devices  71.6 us (28%)
  Pallas kernels  53.5 us (21%)
  blocking collectives  30.8 us (12%)
  local copies, waits for them, and re-layouts  17.3 us (7%)
    all_to_all x9, starting transfers between devices, a2a(): return lax.all_to_all(x, axes, split_axis=0, concat_axis=0, tiled=True)  65.8 us
    all_to_all x9, waiting for transfers between devices, a2a(): return lax.all_to_all(x, axes, split_axis=0, concat_axis=0, tiled=True)  54.3 us
    pallas_call x16, Pallas kernels, call(): pl.pallas_call(body, out_shape=[jax.ShapeDtypeStruct(s, d) for s, d in ou...  53.5 us
    all_to_all x1, blocking collectives, a2a(): return lax.all_to_all(x, axes, split_axis=0, concat_axis=0, tiled=True)  30.8 us
    ppermute x12, waiting for transfers between devices, shift(): return lax.ppermute(x, TP, [(i, (i + by) % 4) for i in range(4)])  17.3 us
    ppermute x12, starting transfers between devices, shift(): return lax.ppermute(x, TP, [(i, (i + by) % 4) for i in range(4)])  13.3 us
    unnamed x55, local copies, waits for them, and re-layouts  12.9 us
  transfers between devices with their start and end apart: 21, of which 11 were waited for; matrix products, arithmetic and copies ran while one was open for 4% of the time, Pallas kernels for 19%

profile of v1, /device:TPU:1, one launch (start us, length us, event | category | flops | bytes accessed | tf_op | source)
XLA Modules:
  0.0 254.4 jit_solution(1354636811103759661)
XLA Ops:
  0.7 1.5 copy.28.routes
  2.2 1.4 copy.29.rw
  3.6 2.6 %dispatch.1 = (bf16[512,512]{1,0:T(8,128)(2,1)}, bf16[512,512]{1,0:T(8,128)(2,1)}, bf16[256,512]{1,0:T(8,128)(2,1)}) custom-call(s32[1]{0:T(128)} %bitcast.q, s32[128,2]{1,0:T(8,128)} %copy.28.routes, f32[128,2]{1,0:T(8,128)} %copy.29.rw, bf16[128,2048]{1,0:T(8,128)(2,1)} %stream.1, bf16[128,2048]{1,0:T(8,128)(2,1)} %og.3), custom_call_target="tpu_custom_call" | custom-call | tf_op jit(solution)/shard_map/dispatch/pallas_call | solution.py:48
  6.2 30.8 %all_to_all.50 = bf16[64,8,512]{2,1,0:T(8,128)(2,1)S(1)} all-to-all(bf16[64,8,512]{2,1,0:T(8,128)(2,1)} %bitcast.71), channel_id=1, replica_groups=mesh['sp_0'=8,'sp_1'=4,'sp_2'=2,'tp'=4] {'sp_0','sp_1','sp_2'}, dimensions={0} | all-to-all | bytes 1048576 | tf_op jit(solution)/shard_map/all_to_all | solution.py:333
  37.0 5.7 %all-to-all-start.1 = ((bf16[64,8,512]{2,1,0:T(8,128)(2,1)}), bf16[64,8,512]{2,1,0:T(8,128)(2,1)S(1)}, u32[]{:S(2)}, u32[]{:S(2)}) async-start(bf16[64,8,512]{2,1,0:T(8,128)(2,1)} %bitcast.70), calls=%async_computation.1 | async-start | bytes 1048576 | tf_op jit(solution)/shard_map/all_to_all | solution.py:333
  42.7 2.6 %collective-permute-start = (bf16[512,512]{1,0:T(8,128)(2,1)S(1)}, bf16[512,512]{1,0:T(8,128)(2,1)S(1)}, u32[]{:S(2)}, u32[]{:S(2)}) collective-permute-start(bf16[512,512]{1,0:T(8,128)(2,1)S(1)} %bitcast.55), channel_id=1, source_target_pairs={{0,3},{1,0},{2,1},{3,2},{4,7},{5,4},{6,5},{7,6},{8,11},{9,8},{10,9... | collective-permute-start | bytes 1572872 | tf_op jit(solution)/shard_map/ppermute | solution.py:337
  45.6 0.9 fusion
  47.6 12.7 %all-to-all-done.1 = bf16[64,8,512]{2,1,0:T(8,128)(2,1)S(1)} async-done(((bf16[64,8,512]{2,1,0:T(8,128)(2,1)}), bf16[64,8,512]{2,1,0:T(8,128)(2,1)S(1)}, u32[]{:S(2)}, u32[]{:S(2)}) %all-to-all-start.1) | async-done | bytes 524320 | tf_op jit(solution)/shard_map/all_to_all | solution.py:333
  60.4 2.5 collective-permute-start.3
  67.6 3.3 %prepare.1 = (bf16[64,16,128]{2,1,0:T(8,128)(2,1)}, f32[2,128,128]{2,1,0:T(8,128)}, f32[2,128,128]{2,1,0:T(8,128)}, f32[2,128,128]{2,1,0:T(8,128)}, f32[2,128,12...) custom-call(s32[1]{0:T(128)} %bitcast.q, ...), custom_call_target="tpu_custom_call" | custom-call | tf_op jit(solution)/shard_map/prepare/pallas_call | solution.py:48
  70.9 15.3 %all-to-all-start.4 = ((bf16[64,16,128]{2,1,0:T(8,128)(2,1)}), bf16[64,16,128]{2,1,0:T(8,128)(2,1)S(1)}, u32[]{:S(2)}, u32[]{:S(2)}) async-start(bf16[64,16,128]{2,1,0:T(8,128)(2,1)} %get-tuple-element.61), calls=%async_computation.4 | async-start | bytes 524288 | tf_op jit(solution)/shard_map/all_to_all | solution.py:333
  86.2 4.7 %gate_up.1 = (bf16[512,256]{1,0:T(8,128)(2,1)}, f32[512,256]{1,0:T(8,128)}, f32[512,256]{1,0:T(8,128)}) custom-call(s32[1]{0:T(128)} %bitcast.q, bf16[512,512]{1,0:T(8,128)(2,1)} %bitcast.58, bf16[512,512]{1,0:T(8,128)(2,1)} %copy-done.8, bf16[512,512]{1,0:T(8,128)(2,1)} %collective-permute-done.1.r2, bf16[512,512]{1,0:T(8,128)(2,1)} %collective-permute-done.2.r3, ...), custom_call_target="tpu_custom_call" | custom-call | tf_op jit(solution)/shard_map/gate_up/pallas_call | solution.py:48
  90.9 4.7 %collective-permute-done.5.x3 = bf16[512,512]{1,0:T(8,128)(2,1)S(1)} collective-permute-done((bf16[512,512]{1,0:T(8,128)(2,1)S(1)}, bf16[512,512]{1,0:T(8,128)(2,1)S(1)}, u32[]{:S(2)}, u32[]{:S(2)}) %collective-permute-start.5) | collective-permute-done | bytes 524320 | tf_op jit(solution)/shard_map/ppermute | solution.py:337
  95.6 0.8 copy-done.5
  96.4 6.5 %expert_back.1 = (bf16[512,256]{1,0:T(8,128)(2,1)}, bf16[512,256]{1,0:T(8,128)(2,1)}, bf16[512,512]{1,0:T(8,128)(2,1)}, bf16[512,512]{1,0:T(8,128)(2,1)}, bf16[5...) custom-call(s32[1]{0:T(128)} %bitcast.q, bf16[512,512]{1,0:T(8,128)(2,1)} %bitcast.53, bf16[512,512]{1,0:T(8,128)(2,1)} %copy-done.3, ...), custom_call_target="tpu_custom_call" | custom-call | tf_op jit(solution)/shard_map/expert_back/pallas_call | solution.py:48
  103.6 2.0 collective-permute-start.8
  106.3 5.4 %prefix.1 = (bf16[512,128]{1,0:T(8,128)(2,1)}, bf16[512,512]{1,0:T(8,128)(2,1)}, bf16[512,512]{1,0:T(8,128)(2,1)}) custom-call(s32[1]{0:T(128)} %bitcast.q, bf16[64,16,128]{2,1,0:T(8,128)(2,1)} %copy-done.11), custom_call_target="tpu_custom_call" | custom-call | tf_op jit(solution)/shard_map/prefix/pallas_call | solution.py:48
  111.7 11.1 %all-to-all-start.5 = ((bf16[64,8,128]{2,1,0:T(8,128)(2,1)}), bf16[64,8,128]{2,1,0:T(8,128)(2,1)S(1)}, u32[]{:S(2)}, u32[]{:S(2)}) async-start(bf16[64,8,128]{2,1,0:T(8,128)(2,1)} %bitcast.73), calls=%async_computation.5 | async-start | bytes 262144 | tf_op jit(solution)/shard_map/all_to_all | solution.py:333
  122.9 5.6 %collective-permute-done.6.b = bf16[512,512]{1,0:T(8,128)(2,1)S(1)} collective-permute-done((bf16[512,512]{1,0:T(8,128)(2,1)}, bf16[512,512]{1,0:T(8,128)(2,1)S(1)}, u32[]{:S(2)}, u32[]{:S(2)}) %collective-permute-start.6) | collective-permute-done | bytes 524320 | tf_op jit(solution)/shard_map/ppermute | solution.py:337
  129.7 2.6 %add4.1 = bf16[512,512]{1,0:T(8,128)(2,1)} custom-call(s32[1]{0:T(128)} %bitcast.q, bf16[512,512]{1,0:T(8,128)(2,1)} %get-tuple-element.56.a, bf16[512,512]{1,0:T(8,128)(2,1)} %copy-done.16, bf16[512,512]{1,0:T(8,128)(2,1)} %copy-done.17, bf16[512,512]{1,0:T(8,128)(2,1)} %copy-done.18), custom_call_target="tpu_custom_call" | custom-call | tf_op jit(solution)/shard_map/add4/pallas_call | solution.py:48
  132.3 1.7 all-to-all-done.5
  134.0 9.8 %all-to-all-start.2 = ((bf16[64,8,512]{2,1,0:T(8,128)(2,1)}), bf16[64,8,512]{2,1,0:T(8,128)(2,1)S(1)}, u32[]{:S(2)}, u32[]{:S(2)}) async-start(bf16[64,8,512]{2,1,0:T(8,128)(2,1)} %bitcast.61), calls=%async_computation.2 | async-start | bytes 1048576 | tf_op jit(solution)/shard_map/all_to_all | solution.py:333
  143.8 2.4 normed.1
  146.2 15.3 %all-to-all-done.2 = bf16[64,8,512]{2,1,0:T(8,128)(2,1)S(1)} async-done(((bf16[64,8,512]{2,1,0:T(8,128)(2,1)}), bf16[64,8,512]{2,1,0:T(8,128)(2,1)S(1)}, u32[]{:S(2)}, u32[]{:S(2)}) %all-to-all-start.2) | async-done | bytes 524320 | tf_op jit(solution)/shard_map/all_to_all | solution.py:333
  161.5 2.1 broadcast_in_dim.32
  163.6 4.7 %all-to-all-start.6 = ((bf16[8,128,512]{2,1,0:T(8,128)(2,1)}), bf16[8,128,512]{2,1,0:T(8,128)(2,1)S(1)}, u32[]{:S(2)}, u32[]{:S(2)}) async-start(bf16[8,128,512]{2,1,0:T(8,128)(2,1)} %broadcast_in_dim.32), calls=%async_computation.6 | async-start | bytes 2097152 | tf_op jit(solution)/shard_map/all_to_all | solution.py:333
  168.2 2.1 combine.1.r0
  171.0 2.0 collective-permute-start.11
  173.7 3.5 %collective-permute-done.10.r2 = bf16[128,512]{1,0:T(8,128)(2,1)S(1)} collective-permute-done((bf16[128,512]{1,0:T(8,128)(2,1)}, bf16[128,512]{1,0:T(8,128)(2,1)S(1)}, u32[]{:S(2)}, u32[]{:S(2)}) %collective-permute-start.10) | collective-permute-done | bytes 131104 | tf_op jit(solution)/shard_map/ppermute | solution.py:337
  177.1 3.2 %collective-permute-done.11.r3 = bf16[128,512]{1,0:T(8,128)(2,1)S(1)} collective-permute-done((bf16[128,512]{1,0:T(8,128)(2,1)}, bf16[128,512]{1,0:T(8,128)(2,1)S(1)}, u32[]{:S(2)}, u32[]{:S(2)}) %collective-permute-start.11) | collective-permute-done | bytes 131104 | tf_op jit(solution)/shard_map/ppermute | solution.py:337
  181.0 3.4 %inner_grad.1 = (f32[128,512]{1,0:T(8,128)}, bf16[512,128]{1,0:T(8,128)(2,1)}) custom-call(s32[1]{0:T(128)} %bitcast.q, bf16[128,512]{1,0:T(8,128)(2,1)} %combine.1.r0, bf16[128,512]{1,0:T(8,128)(2,1)} %copy-done.14, bf16[128,512]{1,0:T(8,128)(2,1)} %copy-done.12, bf16[128,512]{1,0:T(8,128)(2,1)} %copy-done.13, bf16[2048,512]{1,0:T(8,128)(2,1)} %p3.1, ...), custom_call_target="tpu_custom_call" | custom-call | tf_op jit(solution)/shard_map/inner_grad/pallas_call | solution.py:48
  184.5 7.0 %all-to-all-start.8 = ((bf16[64,8,128]{2,1,0:T(8,128)(2,1)}), bf16[64,8,128]{2,1,0:T(8,128)(2,1)S(1)}, u32[]{:S(2)}, u32[]{:S(2)}) async-start(bf16[64,8,128]{2,1,0:T(8,128)(2,1)} %bitcast.74), calls=%async_computation.8 | async-start | bytes 262144 | tf_op jit(solution)/shard_map/all_to_all | solution.py:333
  191.4 2.1 transpose.29
  193.5 9.0 %all-to-all-done.8 = bf16[64,8,128]{2,1,0:T(8,128)(2,1)S(1)} async-done(((bf16[64,8,128]{2,1,0:T(8,128)(2,1)}), bf16[64,8,128]{2,1,0:T(8,128)(2,1)S(1)}, u32[]{:S(2)}, u32[]{:S(2)}) %all-to-all-start.8) | async-done | bytes 131104 | tf_op jit(solution)/shard_map/all_to_all | solution.py:333
  202.5 3.8 %all-to-all-start.3 = ((bf16[8,256,128]{2,1,0:T(8,128)(2,1)}), bf16[8,256,128]{2,1,0:T(8,128)(2,1)S(1)}, u32[]{:S(2)}, u32[]{:S(2)}) async-start(bf16[8,256,128]{2,1,0:T(8,128)(2,1)} %transpose.29), calls=%async_computation.3 | async-start | bytes 1048576 | tf_op jit(solution)/shard_map/all_to_all | solution.py:333
  206.3 2.3 suffix.1
  208.7 7.0 %all-to-all-done.3.rt = bf16[8,256,128]{2,1,0:T(8,128)(2,1)S(1)} async-done(((bf16[8,256,128]{2,1,0:T(8,128)(2,1)}), bf16[8,256,128]{2,1,0:T(8,128)(2,1)S(1)}, u32[]{:S(2)}, u32[]{:S(2)}) %all-to-all-start.3) | async-done | bytes 524320 | tf_op jit(solution)/shard_map/all_to_all | solution.py:333
  215.7 5.0 %all-to-all-start.9 = ((bf16[64,8,128]{2,1,0:T(8,128)(2,1)}), bf16[64,8,128]{2,1,0:T(8,128)(2,1)S(1)}, u32[]{:S(2)}, u32[]{:S(2)}) async-start(bf16[64,8,128]{2,1,0:T(8,128)(2,1)} %bitcast.69), calls=%async_computation.9 | async-start | bytes 262144 | tf_op jit(solution)/shard_map/all_to_all | solution.py:333
  220.8 2.8 %proj.1 = bf16[256,512]{1,0:T(8,128)(2,1)} custom-call(s32[1]{0:T(128)} %bitcast.q, bf16[8,256,128]{2,1,0:T(8,128)(2,1)} %copy-done.7, bf16[8,128,512]{2,1,0:T(8,128)(2,1)} %copy-done.2), custom_call_target="tpu_custom_call" | custom-call | tf_op jit(solution)/shard_map/proj/pallas_call | solution.py:48
  223.6 8.5 %all-to-all-done.9 = bf16[64,8,128]{2,1,0:T(8,128)(2,1)S(1)} async-done(((bf16[64,8,128]{2,1,0:T(8,128)(2,1)}), bf16[64,8,128]{2,1,0:T(8,128)(2,1)S(1)}, u32[]{:S(2)}, u32[]{:S(2)}) %all-to-all-start.9) | async-done | bytes 131104 | tf_op jit(solution)/shard_map/all_to_all | solution.py:333
  232.1 3.4 %all-to-all-start.7 = ((bf16[8,32,512]{2,1,0:T(8,128)(2,1)}), bf16[8,32,512]{2,1,0:T(8,128)(2,1)S(1)}, u32[]{:S(2)}, u32[]{:S(2)}) async-start(bf16[8,32,512]{2,1,0:T(8,128)(2,1)} %bitcast.67), calls=%async_computation.7 | async-start | bytes 524288 | tf_op jit(solution)/shard_map/all_to_all | solution.py:333
  235.5 6.1 %weight_grads.1 = (bf16[2048,256]{1,0:T(8,128)(2,1)}, bf16[2048,256]{1,0:T(8,128)(2,1)}, bf16[256,2048]{1,0:T(8,128)(2,1)}) custom-call(s32[1]{0:T(128)} %bitcast.q, bf16[512,512]{1,0:T(8,128)(2,1)} %bitcast.59, bf16[512,512]{1,0:T(8,128)(2,1)} %copy-done.8, bf16[512,512]{1,0:T(8,128)(2,1)} %collective-permute-done.1.r2, ...), custom_call_target="tpu_custom_call" | custom-call | tf_op jit(solution)/shard_map/weight_grads/pallas_call | solution.py:48
  241.6 3.2 %local_grads.1 = (bf16[2,128,128]{2,1,0:T(8,128)(2,1)}, f32[2,128,128]{2,1,0:T(8,128)}, f32[2,128,256]{2,1,0:T(8,128)}) custom-call(s32[1]{0:T(128)} %bitcast.q, f32[128,512]{1,0:T(8,128)} %get-tuple-element.70.rg, bf16[2,128,256]{2,1,0:T(8,128)(2,1)} %bitcast.63, f32[2,128,128]{2,1,0:T(8,128)} %get-tuple-element.71.dm, ...), custom_call_target="tpu_custom_call" | custom-call | tf_op jit(solution)/shard_map/local_grads/pallas_call | solution.py:48
  244.8 1.5 copy.34
  246.3 2.5 final.1
  248.8 1.7 copy.36
  250.5 1.5 copy.35
  252.7 1.6 add_parts.1
  (78 shorter events, 11.6 us)
Async XLA Ops:
  0.6 64.9 %copy-start.20 = (bf16[128,2,256]{2,1,0:T(2,128)(2,1)S(1)}, bf16[128,2,256]{2,1,0:T(2,128)(2,1)}, u32[]{:S(2)}) copy-start(bf16[128,2,256]{2,1,0:T(2,128)(2,1)} %param.18) | copy-start | bytes 393220
  0.6 65.5 %copy-start.23 = (f32[128,2]{0,1:T(2,128)S(1)}, f32[128,2]{0,1:T(2,128)}, u32[]{:S(2)}) copy-start(f32[128,2]{0,1:T(2,128)} %param.19) | copy-start | bytes 3076
  0.7 66.3 %copy-start.22 = (bf16[128,2,128]{2,1,0:T(2,128)(2,1)S(1)}, bf16[128,2,128]{2,1,0:T(2,128)(2,1)}, u32[]{:S(2)}) copy-start(bf16[128,2,128]{2,1,0:T(2,128)(2,1)} %param.16) | copy-start | bytes 196612
  0.7 66.3 %copy-start.21 = (bf16[128,2,128]{2,1,0:T(2,128)(2,1)S(1)}, bf16[128,2,128]{2,1,0:T(2,128)(2,1)}, u32[]{:S(2)}) copy-start(bf16[128,2,128]{2,1,0:T(2,128)(2,1)} %param.17) | copy-start | bytes 196612
  37.0 49.2 %copy-start.1 = (bf16[64,8,512]{2,1,0:T(8,128)(2,1)}, bf16[64,8,512]{2,1,0:T(8,128)(2,1)S(1)}, u32[]{:S(2)}) copy-start(bf16[64,8,512]{2,1,0:T(8,128)(2,1)S(1)} %all_to_all.50) | copy-start | bytes 1572868
  37.0 23.4 %all-to-all-start.1 = ((bf16[64,8,512]{2,1,0:T(8,128)(2,1)}), bf16[64,8,512]{2,1,0:T(8,128)(2,1)S(1)}, u32[]{:S(2)}, u32[]{:S(2)}) async-start(bf16[64,8,512]{2,1,0:T(8,128)(2,1)} %bitcast.70), calls=%async_computation.1 | async-start | bytes 1048576 | tf_op jit(solution)/shard_map/all_to_all | solution.py:333
  42.7 20.7 %collective-permute-start = (bf16[512,512]{1,0:T(8,128)(2,1)S(1)}, bf16[512,512]{1,0:T(8,128)(2,1)S(1)}, u32[]{:S(2)}, u32[]{:S(2)}) collective-permute-start(bf16[512,512]{1,0:T(8,128)(2,1)S(1)} %bitcast.55), channel_id=1, source_target_pairs={{0,3},{1,0},{2,1},{3,2},{4,7},{5,4},{6,5},{7,6},{8,11},{9,8},{10,9... | collective-permute-start | bytes 1572872 | tf_op jit(solution)/shard_map/ppermute | solution.py:337
  46.5 39.6 %collective-permute-start.1 = (bf16[512,512]{1,0:T(8,128)(2,1)S(1)}, bf16[512,512]{1,0:T(8,128)(2,1)}, u32[]{:S(2)}, u32[]{:S(2)}) collective-permute-start(bf16[512,512]{1,0:T(8,128)(2,1)S(1)} %bitcast.56), channel_id=1, source_target_pairs={{0,2},{1,3},{2,0},{3,1},{4,6},{5,7},{6,4},{7,5},{8,10},{9,11},{10,... | collective-permute-start | bytes 1572872 | tf_op jit(solution)/shard_map/ppermute | solution.py:337
  47.0 39.1 %collective-permute-start.2 = (bf16[512,512]{1,0:T(8,128)(2,1)S(1)}, bf16[512,512]{1,0:T(8,128)(2,1)}, u32[]{:S(2)}, u32[]{:S(2)}) collective-permute-start(bf16[512,512]{1,0:T(8,128)(2,1)S(1)} %bitcast.57), channel_id=1, source_target_pairs={{0,1},{1,2},{2,3},{3,0},{4,5},{5,6},{6,7},{7,4},{8,9},{9,10},{10,1... | collective-permute-start | bytes 1572872 | tf_op jit(solution)/shard_map/ppermute | solution.py:337
  60.4 30.5 %copy-start = (bf16[64,8,512]{2,1,0:T(8,128)(2,1)}, bf16[64,8,512]{2,1,0:T(8,128)(2,1)S(1)}, u32[]{:S(2)}) copy-start(bf16[64,8,512]{2,1,0:T(8,128)(2,1)S(1)} %all-to-all-done.1) | copy-start | bytes 1572868
  60.4 30.5 %collective-permute-start.3 = (bf16[512,512]{1,0:T(8,128)(2,1)S(1)}, bf16[512,512]{1,0:T(8,128)(2,1)S(1)}, u32[]{:S(2)}, u32[]{:S(2)}) collective-permute-start(bf16[512,512]{1,0:T(8,128)(2,1)S(1)} %bitcast.50), channel_id=1, source_target_pairs={{0,3},{1,0},{2,1},{3,2},{4,7},{5,4},{6,5},{7,6},{8,11},{9,8},{10,9... | collective-permute-start | bytes 1572872 | tf_op jit(solution)/shard_map/ppermute | solution.py:337
  62.9 28.0 %collective-permute-start.4 = (bf16[512,512]{1,0:T(8,128)(2,1)S(1)}, bf16[512,512]{1,0:T(8,128)(2,1)S(1)}, u32[]{:S(2)}, u32[]{:S(2)}) collective-permute-start(bf16[512,512]{1,0:T(8,128)(2,1)S(1)} %bitcast.51), channel_id=1, source_target_pairs={{0,2},{1,3},{2,0},{3,1},{4,6},{5,7},{6,4},{7,5},{8,10},{9,11},{10,... | collective-permute-start | bytes 1572872 | tf_op jit(solution)/shard_map/ppermute | solution.py:337
  63.4 22.8 %copy-start.8 = (bf16[512,512]{1,0:T(8,128)(2,1)}, bf16[512,512]{1,0:T(8,128)(2,1)S(1)}, u32[]{:S(2)}) copy-start(bf16[512,512]{1,0:T(8,128)(2,1)S(1)} %collective-permute-done.r1) | copy-start | bytes 1572868
  63.4 32.2 %collective-permute-start.5 = (bf16[512,512]{1,0:T(8,128)(2,1)S(1)}, bf16[512,512]{1,0:T(8,128)(2,1)S(1)}, u32[]{:S(2)}, u32[]{:S(2)}) collective-permute-start(bf16[512,512]{1,0:T(8,128)(2,1)S(1)} %bitcast.52), channel_id=1, source_target_pairs={{0,1},{1,2},{2,3},{3,0},{4,5},{5,6},{6,7},{7,4},{8,9},{9,10},{10,1... | collective-permute-start | bytes 1572872 | tf_op jit(solution)/shard_map/ppermute | solution.py:337
  70.9 34.7 %all-to-all-start.4 = ((bf16[64,16,128]{2,1,0:T(8,128)(2,1)}), bf16[64,16,128]{2,1,0:T(8,128)(2,1)S(1)}, u32[]{:S(2)}, u32[]{:S(2)}) async-start(bf16[64,16,128]{2,1,0:T(8,128)(2,1)} %get-tuple-element.61), calls=%async_computation.4 | async-start | bytes 524288 | tf_op jit(solution)/shard_map/all_to_all | solution.py:333
  90.9 4.7 %copy-start.3 = (bf16[512,512]{1,0:T(8,128)(2,1)}, bf16[512,512]{1,0:T(8,128)(2,1)S(1)}, u32[]{:S(2)}) copy-start(bf16[512,512]{1,0:T(8,128)(2,1)S(1)} %collective-permute-done.3.x1) | copy-start | bytes 1572868
  90.9 4.7 %copy-start.4 = (bf16[512,512]{1,0:T(8,128)(2,1)}, bf16[512,512]{1,0:T(8,128)(2,1)S(1)}, u32[]{:S(2)}) copy-start(bf16[512,512]{1,0:T(8,128)(2,1)S(1)} %collective-permute-done.4.x2) | copy-start | bytes 1572868
  95.6 0.8 copy-start.5
  102.9 25.6 %collective-permute-start.6 = (bf16[512,512]{1,0:T(8,128)(2,1)}, bf16[512,512]{1,0:T(8,128)(2,1)S(1)}, u32[]{:S(2)}, u32[]{:S(2)}) collective-permute-start(bf16[512,512]{1,0:T(8,128)(2,1)} %get-tuple-element.57), channel_id=1, source_target_pairs={{0,1},{1,2},{2,3},{3,0},{4,5},{5,6},{6,7},{7,4},{8,9},{9,10},{10,1... | collective-permute-start | bytes 1572872 | tf_op jit(solution)/shard_map/ppermute | solution.py:337
  102.9 25.6 %collective-permute-start.7 = (bf16[512,512]{1,0:T(8,128)(2,1)}, bf16[512,512]{1,0:T(8,128)(2,1)S(1)}, u32[]{:S(2)}, u32[]{:S(2)}) collective-permute-start(bf16[512,512]{1,0:T(8,128)(2,1)} %get-tuple-element.58), channel_id=1, source_target_pairs={{0,2},{1,3},{2,0},{3,1},{4,6},{5,7},{6,4},{7,5},{8,10},{9,11},{10,... | collective-permute-start | bytes 1572872 | tf_op jit(solution)/shard_map/ppermute | solution.py:337
  103.6 25.3 %collective-permute-start.8 = (bf16[512,512]{1,0:T(8,128)(2,1)}, bf16[512,512]{1,0:T(8,128)(2,1)S(1)}, u32[]{:S(2)}, u32[]{:S(2)}) collective-permute-start(bf16[512,512]{1,0:T(8,128)(2,1)} %get-tuple-element.59), channel_id=1, source_target_pairs={{0,3},{1,0},{2,1},{3,2},{4,7},{5,4},{6,5},{7,6},{8,11},{9,8},{10,9... | collective-permute-start | bytes 1572872 | tf_op jit(solution)/shard_map/ppermute | solution.py:337
  105.6 0.7 copy-start.11
  111.7 22.2 %all-to-all-start.5 = ((bf16[64,8,128]{2,1,0:T(8,128)(2,1)}), bf16[64,8,128]{2,1,0:T(8,128)(2,1)S(1)}, u32[]{:S(2)}, u32[]{:S(2)}) async-start(bf16[64,8,128]{2,1,0:T(8,128)(2,1)} %bitcast.73), calls=%async_computation.5 | async-start | bytes 262144 | tf_op jit(solution)/shard_map/all_to_all | solution.py:333
  128.5 0.8 copy-start.16
  128.5 1.0 copy-start.17
  128.9 0.8 copy-start.18
  134.0 9.8 %copy-start.9 = (bf16[64,8,128]{2,1,0:T(8,128)(2,1)}, bf16[64,8,128]{2,1,0:T(8,128)(2,1)S(1)}, u32[]{:S(2)}) copy-start(bf16[64,8,128]{2,1,0:T(8,128)(2,1)S(1)} %all-to-all-done.5) | copy-start | bytes 393220
  134.0 27.5 %all-to-all-start.2 = ((bf16[64,8,512]{2,1,0:T(8,128)(2,1)}), bf16[64,8,512]{2,1,0:T(8,128)(2,1)S(1)}, u32[]{:S(2)}, u32[]{:S(2)}) async-start(bf16[64,8,512]{2,1,0:T(8,128)(2,1)} %bitcast.61), calls=%async_computation.2 | async-start | bytes 1048576 | tf_op jit(solution)/shard_map/all_to_all | solution.py:333
  161.5 6.7 %copy-start.6 = (bf16[64,8,512]{2,1,0:T(8,128)(2,1)}, bf16[64,8,512]{2,1,0:T(8,128)(2,1)S(1)}, u32[]{:S(2)}) copy-start(bf16[64,8,512]{2,1,0:T(8,128)(2,1)S(1)} %all-to-all-done.2) | copy-start | bytes 1572868
  163.6 20.9 %all-to-all-start.6 = ((bf16[8,128,512]{2,1,0:T(8,128)(2,1)}), bf16[8,128,512]{2,1,0:T(8,128)(2,1)S(1)}, u32[]{:S(2)}, u32[]{:S(2)}) async-start(bf16[8,128,512]{2,1,0:T(8,128)(2,1)} %broadcast_in_dim.32), calls=%async_computation.6 | async-start | bytes 2097152 | tf_op jit(solution)/shard_map/all_to_all | solution.py:333
  170.3 6.8 %collective-permute-start.10 = (bf16[128,512]{1,0:T(8,128)(2,1)}, bf16[128,512]{1,0:T(8,128)(2,1)S(1)}, u32[]{:S(2)}, u32[]{:S(2)}) collective-permute-start(bf16[128,512]{1,0:T(8,128)(2,1)} %combine.1.r0), channel_id=1, source_target_pairs={{0,2},{1,3},{2,0},{3,1},{4,6},{5,7},{6,4},{7,5},{8,10},{9,11},{10,... | collective-permute-start | bytes 393224 | tf_op jit(solution)/shard_map/ppermute | solution.py:337
  171.0 9.3 %collective-permute-start.11 = (bf16[128,512]{1,0:T(8,128)(2,1)}, bf16[128,512]{1,0:T(8,128)(2,1)S(1)}, u32[]{:S(2)}, u32[]{:S(2)}) collective-permute-start(bf16[128,512]{1,0:T(8,128)(2,1)} %combine.1.r0), channel_id=1, source_target_pairs={{0,1},{1,2},{2,3},{3,0},{4,5},{5,6},{6,7},{7,4},{8,9},{9,10},{10,1... | collective-permute-start | bytes 393224 | tf_op jit(solution)/shard_map/ppermute | solution.py:337
  173.0 7.3 %collective-permute-start.9 = (bf16[128,512]{1,0:T(8,128)(2,1)}, bf16[128,512]{1,0:T(8,128)(2,1)S(1)}, u32[]{:S(2)}, u32[]{:S(2)}) collective-permute-start(bf16[128,512]{1,0:T(8,128)(2,1)} %combine.1.r0), channel_id=1, source_target_pairs={{0,3},{1,0},{2,1},{3,2},{4,7},{5,4},{6,5},{7,6},{8,11},{9,8},{10,9... | collective-permute-start | bytes 393224 | tf_op jit(solution)/shard_map/ppermute | solution.py:337
  177.1 3.2 %copy-start.12 = (bf16[128,512]{1,0:T(8,128)(2,1)}, bf16[128,512]{1,0:T(8,128)(2,1)S(1)}, u32[]{:S(2)}) copy-start(bf16[128,512]{1,0:T(8,128)(2,1)S(1)} %collective-permute-done.10.r2) | copy-start | bytes 393220
  180.3 0.7 copy-start.13
  180.3 0.7 copy-start.14
  184.4 36.3 %copy-start.2 = (bf16[8,128,512]{2,1,0:T(8,128)(2,1)}, bf16[8,128,512]{2,1,0:T(8,128)(2,1)S(1)}, u32[]{:S(2)}) copy-start(bf16[8,128,512]{2,1,0:T(8,128)(2,1)S(1)} %all-to-all-done.6.nb) | copy-start | bytes 3145732
  184.5 18.1 %all-to-all-start.8 = ((bf16[64,8,128]{2,1,0:T(8,128)(2,1)}), bf16[64,8,128]{2,1,0:T(8,128)(2,1)S(1)}, u32[]{:S(2)}, u32[]{:S(2)}) async-start(bf16[64,8,128]{2,1,0:T(8,128)(2,1)} %bitcast.74), calls=%async_computation.8 | async-start | bytes 262144 | tf_op jit(solution)/shard_map/all_to_all | solution.py:333
  202.5 3.8 %copy-start.15 = (bf16[64,8,128]{2,1,0:T(8,128)(2,1)}, bf16[64,8,128]{2,1,0:T(8,128)(2,1)S(1)}, u32[]{:S(2)}) copy-start(bf16[64,8,128]{2,1,0:T(8,128)(2,1)S(1)} %all-to-all-done.8) | copy-start | bytes 393220
  202.5 13.2 %all-to-all-start.3 = ((bf16[8,256,128]{2,1,0:T(8,128)(2,1)}), bf16[8,256,128]{2,1,0:T(8,128)(2,1)S(1)}, u32[]{:S(2)}, u32[]{:S(2)}) async-start(bf16[8,256,128]{2,1,0:T(8,128)(2,1)} %transpose.29), calls=%async_computation.3 | async-start | bytes 1048576 | tf_op jit(solution)/shard_map/all_to_all | solution.py:333
  215.7 5.0 %copy-start.7 = (bf16[8,256,128]{2,1,0:T(8,128)(2,1)}, bf16[8,256,128]{2,1,0:T(8,128)(2,1)S(1)}, u32[]{:S(2)}) copy-start(bf16[8,256,128]{2,1,0:T(8,128)(2,1)S(1)} %all-to-all-done.3.rt) | copy-start | bytes 1572868
  215.7 16.4 %all-to-all-start.9 = ((bf16[64,8,128]{2,1,0:T(8,128)(2,1)}), bf16[64,8,128]{2,1,0:T(8,128)(2,1)S(1)}, u32[]{:S(2)}, u32[]{:S(2)}) async-start(bf16[64,8,128]{2,1,0:T(8,128)(2,1)} %bitcast.69), calls=%async_computation.9 | async-start | bytes 262144 | tf_op jit(solution)/shard_map/all_to_all | solution.py:333
  232.1 9.5 %copy-start.19 = (bf16[64,8,128]{2,1,0:T(8,128)(2,1)}, bf16[64,8,128]{2,1,0:T(8,128)(2,1)S(1)}, u32[]{:S(2)}) copy-start(bf16[64,8,128]{2,1,0:T(8,128)(2,1)S(1)} %all-to-all-done.9) | copy-start | bytes 393220
  232.1 20.0 %all-to-all-start.7 = ((bf16[8,32,512]{2,1,0:T(8,128)(2,1)}), bf16[8,32,512]{2,1,0:T(8,128)(2,1)S(1)}, u32[]{:S(2)}, u32[]{:S(2)}) async-start(bf16[8,32,512]{2,1,0:T(8,128)(2,1)} %bitcast.67), calls=%async_computation.7 | async-start | bytes 524288 | tf_op jit(solution)/shard_map/all_to_all | solution.py:333
  252.0 0.7 copy-start.10

commit v2 on v1

v2 whole, which is shorter than its diff:
```python
import functools

import jax
import jax.numpy as jnp
import numpy as np
from jax import lax
from jax.experimental import pallas as pl
from jax.experimental.pallas import tpu as pltpu
from jax.sharding import Mesh
from jax.sharding import PartitionSpec as P

SP = ("sp_0", "sp_1", "sp_2")
YC = ("sp_1", "sp_2")
ZAX = "sp_0"
TP = "tp"

CLAMP_LIMIT = 7.0
GATE_SLOPE = 1.702
EPSILON = 1e-06
HI = lax.Precision.HIGHEST
F32 = jnp.float32
BF = jnp.bfloat16

NN = (((1,), (0,)), ((), ()))
NT = (((1,), (1,)), ((), ()))
TN = (((0,), (0,)), ((), ()))


def mm(a, b, dims=NN):
    return lax.dot_general(a, b, dims, preferred_element_type=F32)


def mmh(a, b, dims=NN):
    return lax.dot_general(a, b, dims, precision=HI, preferred_element_type=F32)


def iota(shape, dim):
    return lax.broadcasted_iota(jnp.int32, shape, dim)


def whole(shape):
    return pl.BlockSpec(shape, lambda i, q: (0,) * len(shape))


def call(name, body, q, args, outs, in_specs=None, out_specs=None, grid=1, after=(), mib=16):
    in_specs = dict(in_specs or {})
    out_specs = out_specs or {}
    used = len(args)
    args = (*args, *after)
    for i in range(used, len(args)):
        in_specs[i] = pl.BlockSpec(memory_space=pltpu.HBM)

    def kernel(q_ref, *refs):
        body(q_ref, *refs[:used], *refs[len(args) :])

    return pl.pallas_call(
        kernel,
        out_shape=[jax.ShapeDtypeStruct(s, d) for s, d in outs],
        grid_spec=pltpu.PrefetchScalarGridSpec(
            num_scalar_prefetch=1,
            grid=(grid,),
            in_specs=[in_specs.get(i, whole(a.shape)) for i, a in enumerate(args)],
            out_specs=[out_specs.get(i, whole(s)) for i, (s, _) in enumerate(outs)],
        ),
        compiler_params=pltpu.CompilerParams(vmem_limit_bytes=mib << 20),
        name=name,
    )(q, *args)


def slots_of(routes):
    n = routes.shape[1]
    ti, tj = iota((n, n), 0), iota((n, n), 1)
    eye = ti == tj
    before = ti < tj
    r = routes[...].astype(F32)

    def col(c):
        return jnp.sum(jnp.where(eye, c, 0.0), axis=1, keepdims=True)

    e0r, e1r = r[0:1], r[1:2]
    e0, e1 = col(e0r), col(e1r)

    def earlier(er):
        same = (e0 == er).astype(F32) + (e1 == er).astype(F32)
        return jnp.sum(jnp.where(before, same, 0.0), axis=0, keepdims=True)

    cap = 8
    d0 = e0r * cap + earlier(e0r)
    d1 = e1r * cap + earlier(e1r) + (e0r == e1r).astype(F32)
    return d0, d1, col


def dispatch_body(q, routes, rw, stream, og, send, qt):
    n = routes.shape[1]
    slots = qt.shape[1]
    d0, d1, col = slots_of(routes)
    w = rw[...]
    di = iota((slots, n), 0).astype(F32)
    q0, q1 = di == d0, di == d1
    weight = jnp.where(q0, w[0:1], 0.0) + jnp.where(q1, w[1:2], 0.0)
    weight = jnp.sum(weight, axis=1, keepdims=True)
    pick = (jnp.where(q0, 1.0, 0.0) + jnp.where(q1, 1.0, 0.0)).astype(BF)
    rows = mm(pick, stream[...]).reshape(64, 8, -1)
    grads = (mm(pick, og[...]) * weight).reshape(64, 8, -1)
    send[...] = jnp.concatenate([rows, grads], axis=1).astype(BF)
    dl = iota((n, slots), 1).astype(F32)
    qt[0:n, :] = jnp.where(dl == col(d0), 1.0, 0.0).astype(BF)
    qt[n : 2 * n, :] = jnp.where(dl == col(d1), 1.0, 0.0).astype(BF)


def combine_body(q, ret, qt, og, resid):
    n = og.shape[0]
    back = mm(qt[...], ret[...])
    resid[...] = ((og[...].astype(F32) + back[0:n]) + back[n : 2 * n]).astype(BF)


def gate_up_body(q, r0, r1, r2, r3, g0, g1, g2, g3, u0, u1, u2, u3, act, ga, ua):
    rows = (r0, r1, r2, r3)
    gate = mm(r0[...], g0[...])
    up = mm(r0[...], u0[...])
    for r, g, u in zip(rows[1:], (g1, g2, g3), (u1, u2, u3)):
        x = r[...]
        gate = gate + mm(x, g[...])
        up = up + mm(x, u[...])
    gc = jnp.minimum(gate, CLAMP_LIMIT)
    uc = jnp.clip(up, -CLAMP_LIMIT, CLAMP_LIMIT)
    sig = 1.0 / (1.0 + jnp.exp(-GATE_SLOPE * gc))
    gs = gc * sig
    act[...] = (gs * (uc + 1.0)).astype(BF)
    slope = sig + GATE_SLOPE * gs * (1.0 - sig)
    ga[...] = jnp.where(gate < CLAMP_LIMIT, (uc + 1.0) * slope, 0.0)
    ua[...] = jnp.where(jnp.abs(up) < CLAMP_LIMIT, gs, 0.0)


def expert_back_body(
    q, x0, x1, x2, x3, d0, d1, d2, d3, g0, g1, g2, g3, u0, u1, u2, u3, ga, ua,
    gp, up, far_lo, far_hi, right_lo, right_hi, left_lo, left_hi, mine,
):
    act_grad = mm(x0[...], d0[...], NT)
    for x, d in zip((x1, x2, x3), (d1, d2, d3)):
        act_grad = act_grad + mm(x[...], d[...], NT)
    gpg = (act_grad * ga[...]).astype(BF)
    upg = (act_grad * ua[...]).astype(BF)
    gp[...] = gpg
    up[...] = upg

    def back(g, u):
        return (mm(gpg, g[...], NT) + mm(upg, u[...], NT)).astype(BF)

    half = far_lo.shape[0]
    for lo, hi, part in ((far_lo, far_hi, back(g2, u2)), (right_lo, right_hi, back(g1, u1)), (left_lo, left_hi, back(g3, u3))):
        lo[...] = part[:half]
        hi[...] = part[half:]
    mine[...] = back(g0, u0)


def pass_on_body(q, right_lo, far_lo, left_hi, far_hi, right, left):
    right[...] = (right_lo[...].astype(F32) + far_lo[...].astype(F32)).astype(BF)
    left[...] = (left_hi[...].astype(F32) + far_hi[...].astype(F32)).astype(BF)


def share_body(q, mine, a_lo, a_hi, b_lo, b_hi, out):
    half = a_lo.shape[0]
    m = mine[...].astype(F32)
    out[:half, :] = (m[:half] + (a_lo[...].astype(F32) + b_lo[...].astype(F32))).astype(BF)
    out[half:, :] = (m[half:] + (a_hi[...].astype(F32) + b_hi[...].astype(F32))).astype(BF)


def weight_grads_body(q, r0, r1, r2, r3, x0, x1, x2, x3, gp, up, act, gw, uw, dw, token):
    token[...] = jnp.zeros(token.shape, F32)
    step = pl.program_id(0)
    for k, (r, x) in enumerate(zip((r0, r1, r2, r3), (x0, x1, x2, x3))):

        @pl.when(step == k)
        def _(r=r, x=x):
            rt = r[...]
            gw[...] = mm(rt, gp[...], TN).astype(BF)
            uw[...] = mm(rt, up[...], TN).astype(BF)
            dw[...] = mm(act[...], x[...], TN).astype(BF)


def turned(x, c, s):
    even = (iota(x.shape, 1) % 2) == 0
    n = x.shape[1]
    other = jnp.where(even, -pltpu.roll(x, n - 1, 1), pltpu.roll(x, 1, 1))
    return x * c + other * s


QR, KR, WTS, MASK, SCAL, COS, SIN, INTRA = 0, 256, 512, 768, 1024, 1152, 1280, 1408


def prepare_body(q, qv, kv, vv, ld, cb, sb, cr, sr, send, pack):
    heads, n, kd = qv.shape
    vd = vv.shape[2]
    ti, tj = iota((n, n), 0), iota((n, n), 1)
    eye, causal = ti == tj, ti >= tj
    c = cb[...] * cr[...] - sb[...] * sr[...]
    s = sb[...] * cr[...] + cb[...] * sr[...]
    pack[:, COS : COS + kd] = c
    pack[:, SIN : SIN + kd] = s
    pieces = []
    logs = jnp.zeros((1, 8, 128), F32)
    sub = iota((1, 8, 128), 1)
    scal = jnp.zeros((n, 128), F32)
    lane = iota((n, 128), 1)
    for h in range(heads):
        col = jnp.sum(jnp.where(eye, ld[h : h + 1, :], 0.0), axis=1, keepdims=True)
        rt_r = jnp.sum(jnp.where(ti <= tj, col, 0.0), axis=0, keepdims=True)
        rt_c = jnp.sum(jnp.where(eye, rt_r, 0.0), axis=1, keepdims=True)
        total = rt_r[:, n - 1 : n]
        mask = jnp.where(causal, jnp.exp(jnp.where(causal, rt_c - rt_r, 0.0)), 0.0)
        grow = jnp.exp(rt_c)
        left = jnp.exp(total - rt_c)
        qh = turned(qv[h].astype(F32), c, s)
        kh = turned(kv[h].astype(F32), c, s) * (kd**-0.5)
        vh = vv[h].astype(F32)
        inner = mmh((kh * left).T, vh)
        for u in range(vd // 128):
            pieces.append(inner[:, u * 128 : (u + 1) * 128])
        hi = total.astype(BF).astype(F32)
        mid = (total - hi).astype(BF).astype(F32)
        for k, part in enumerate((hi, mid, total - hi - mid)):
            logs = jnp.where(sub == 3 * h + k, part[None], logs)
        w = mmh(qh, kh, NT) * mask
        pack[:, INTRA + h * vd : INTRA + (h + 1) * vd] = mmh(w, vh)
        at = h * 128
        pack[:, QR + at : QR + at + 128] = qh
        pack[:, KR + at : KR + at + 128] = kh
        pack[:, WTS + at : WTS + at + 128] = w
        pack[:, MASK + at : MASK + at + 128] = mask
        scal = jnp.where(lane == h, grow, jnp.where(lane == 2 + h, left, scal))
    pack[:, SCAL : SCAL + 128] = scal
    state = jnp.concatenate(pieces, axis=0).reshape(-1, 8, 128)
    send[...] = jnp.concatenate([state, jnp.broadcast_to(logs, state.shape)], axis=1).astype(BF)


def prefix_body(q, x, out, table):
    n = x.shape[0]
    z, j = q[1], q[2]
    xf = x[...].astype(F32)
    logs = [xf[:, 8 + 3 * h, :] + xf[:, 9 + 3 * h, :] + xf[:, 10 + 3 * h, :] for h in range(2)]
    mine = jnp.where(z >= 4, logs[1], logs[0])[:, 0:1]
    ti, tj = iota((n, n), 0), iota((n, n), 1)
    after = jnp.where(ti > tj, mine, 0.0)
    seg = mmh(jnp.where(tj < ti, 1.0, 0.0), after)
    w = jnp.where(tj < ti, jnp.exp(seg), 0.0)
    acc = mmh(w, jnp.concatenate([xf[:, k, :] for k in range(8)], axis=1))
    for k in range(8):
        out[:, k, :] = acc[:, k * 128 : (k + 1) * 128]
    other = jnp.where(j >= 4, logs[1], logs[0])[:, 0:1]
    row = jnp.sum(jnp.where(ti == tj, other, 0.0), axis=0, keepdims=True)
    i, m = iota((16, n), 0), iota((16, n), 1)
    low = jnp.where(i == 8, 8 * z - 1, 8 * z + i)
    a = jnp.where((m > low) & (i < 9), row, 0.0)
    m2, c2 = iota((n, 128), 0), iota((n, 128), 1)
    high = jnp.where(c2 < 16, 8 * z + c2, 8 * (c2 - 16))
    b = jnp.where(m2 < high, 1.0, 0.0)
    decay = jnp.exp(mmh(a, b))
    i, c = iota((16, 128), 0), iota((16, 128), 1)
    used = ((c < 8) & ((i == 8) | (c > i))) | ((c == 8) & (i < 8)) | ((i == 7) & (c >= 16) & (c < 24) & (c - 16 > z))
    table[...] = jnp.where(used, decay, 0.0)


def joined(state, h, vd):
    per = vd // 128
    base = h * per * 128
    return jnp.concatenate([state[base + u * 128 : base + (u + 1) * 128, :] for u in range(per)], axis=1)


INV, QDT = 512, 640


def normed_body(q, state, pack, nbf, back):
    n = pack.shape[0]
    heads, vd = 2, 256
    st = state[...].astype(F32)
    lane = iota((n, 128), 1)
    invs = jnp.zeros((n, 128), F32)
    for h in range(heads):
        sl = slice(h * vd, (h + 1) * vd)
        qh = pack[:, QR + h * 128 : QR + (h + 1) * 128]
        grow = pack[:, SCAL + h : SCAL + h + 1]
        ret = pack[:, INTRA + h * vd : INTRA + (h + 1) * vd] + grow * mmh(qh, joined(st, h, vd))
        iv = lax.rsqrt(jnp.mean(ret * ret, axis=1, keepdims=True) + EPSILON)
        nm = ret * iv
        back[:, sl] = nm
        for k in range(nbf.shape[0]):
            nbf[k, :, sl] = nm.astype(BF)
        invs = jnp.where(lane == h, iv, invs)
        back[:, QDT + h * 128 : QDT + (h + 1) * 128] = (qh * grow).T
    back[:, INV : INV + 128] = invs


def inner_grad_body(q, r0, r1, r2, r3, p0, p1, p2, p3, back, rg, send):
    heads, vd = 2, 256
    ng = mm(r0[...], p0[...])
    for r, p in zip((r1, r2, r3), (p1, p2, p3)):
        ng = ng + mm(r[...], p[...])
    for h in range(heads):
        sl = slice(h * vd, (h + 1) * vd)
        nm, g = back[:, sl], ng[:, sl]
        m = jnp.mean(g * nm, axis=1, keepdims=True)
        grad = back[:, INV + h : INV + h + 1] * (g - nm * m)
        rg[:, sl] = grad
        inner = mmh(back[:, QDT + h * 128 : QDT + (h + 1) * 128], grad)
        for u in range(vd // 128):
            for e in range(2):
                part = inner[e * 64 : (e + 1) * 64, u * 128 : (u + 1) * 128]
                send[h * 4 + u * 2 + e, 0:64, :] = part.astype(BF)
    for k, r in enumerate((r0, r1, r2, r3)):
        block = lax.rem(q[0] + k, 4)
        t = r[...].astype(F32).T.astype(BF)
        for lo in range(2):
            at = pl.multiple_of(64 + (block * 2 + lo) * 32, 32)
            for j in range(8):
                src = lo * 256 + j * 32
                send[j, pl.ds(at, 32), :] = t[src : src + 32, :]


def local_grads_body(q, rg, vv, pack, state, qg, rest):
    n = pack.shape[0]
    heads, vd = 2, 256
    st = state[...].astype(F32)
    c, s = pack[:, COS : COS + 128], pack[:, SIN : SIN + 128]
    for h in range(heads):
        at = h * 128
        grad = rg[:, h * vd : (h + 1) * vd]
        score = mmh(grad, vv[h].astype(F32), NT) * pack[:, MASK + at : MASK + at + 128]
        grow = pack[:, SCAL + h : SCAL + h + 1]
        qp = mmh(score, pack[:, KR + at : KR + at + 128]) + grow * mmh(grad, joined(st, h, vd), NT)
        qg[h] = turned(qp, c, -s).astype(BF)
        rest[:, at : at + 128] = mmh(score.T, pack[:, QR + at : QR + at + 128])
        rest[:, 256 + h * vd : 256 + (h + 1) * vd] = mmh(pack[:, WTS + at : WTS + at + 128].T, grad)


def plane_body(q, x, nb, table, inside, send):
    blocks = x.shape[0]
    parts = [x[k, 0:64, :].astype(F32) for k in range(blocks)]
    for k in range(blocks):
        acc = jnp.zeros((64, 128), F32)
        for m in range(k + 1, blocks):
            acc = acc + table[k : k + 1, m : m + 1] * parts[m]
        inside[k] = acc
    total = jnp.zeros((64, 128), F32)
    for m in range(blocks):
        total = total + table[8:9, m : m + 1] * parts[m]
    total = total.astype(BF)
    proj = mm(x[0, 64:320, :], nb[0])
    for k in range(1, blocks):
        proj = proj + mm(x[k, 64:320, :], nb[k])
    for k in range(blocks):
        send[k, 0:64, :] = total
        for u in range(4):
            send[k, 64 + u * 32 : 96 + u * 32, :] = proj[k * 32 : (k + 1) * 32, u * 128 : (u + 1) * 128].astype(BF)


def planes_body(q, y, inside, table, out, proj):
    blocks = y.shape[0]
    later = jnp.zeros((64, 128), F32)
    for k in range(blocks):
        later = later + table[7:8, 16 + k : 17 + k] * y[k, 0:64, :].astype(F32)
    for k in range(blocks):
        out[k] = (inside[k] + table[k : k + 1, 8:9] * later).astype(BF)
    for u in range(4):
        acc = y[0, 64 + u * 32 : 96 + u * 32, :].astype(F32)
        for k in range(1, blocks):
            acc = acc + y[k, 64 + u * 32 : 96 + u * 32, :].astype(F32)
        proj[:, u * 128 : (u + 1) * 128] = acc


def final_body(q, state, vv, pack, rest, kg, vg):
    heads, vd, kd = 2, 256, 128
    st = state[...].astype(F32)
    c, s = pack[:, COS : COS + 128], pack[:, SIN : SIN + 128]
    for h in range(heads):
        at = h * 128
        fut = joined(st, h, vd)
        left = pack[:, SCAL + 2 + h : SCAL + 3 + h]
        kt = rest[:, at : at + 128] + left * mmh(vv[h].astype(F32), fut, NT)
        kg[h] = (turned(kt, c, -s) * (kd**-0.5)).astype(BF)
        vt = rest[:, 256 + h * vd : 256 + (h + 1) * vd]
        vg[h] = (vt + left * mmh(pack[:, KR + at : KR + at + 128], fut)).astype(BF)


def a2a(x, axes):
    return lax.all_to_all(x, axes, split_axis=0, concat_axis=0, tiled=True)


def shift(x, by):
    return lax.ppermute(x, TP, [(i, (i + by) % 4) for i in range(4)])


def around(x):
    far = shift(x, 2)
    return x, shift(x, 3), far, shift(x, 1)


def block_rows(k, shape):
    return pl.BlockSpec(shape, lambda i, q, k=k: (lax.rem(q[0] + k, 4), 0))


def block_cols(k, shape):
    return pl.BlockSpec(shape, lambda i, q, k=k: (0, lax.rem(q[0] + k, 4)))


def per_device(
    stream,
    out_grad,
    routes,
    route_weight,
    queries,
    key_vectors,
    value_vectors,
    log_decay,
    out_proj,
    gate_weight,
    up_weight,
    down_weight,
):
    n, width = stream.shape
    quarter = width // 4
    slots = 512
    hidden = gate_weight.shape[2]
    heads, kd = queries.shape[1:]
    vd = value_vectors.shape[2]
    sp = lax.axis_index(SP)
    q = jnp.stack([lax.axis_index(TP), sp // 8, sp % 8, sp]).astype(jnp.int32)
    gate_w, up_w, down_w = gate_weight[0], up_weight[0], down_weight[0]

    own = pl.BlockSpec((n, quarter), lambda i, q: (0, q[0]))
    sent, qt = call(
        "dispatch",
        dispatch_body,
        q,
        (routes.T, route_weight.T, stream, out_grad),
        [((64, 16, quarter), BF), ((2 * n, slots), BF)],
        in_specs={2: own, 3: own},
    )
    came = a2a(sent, SP)
    rows = came[:, :8].reshape(slots, quarter)
    rows_prev, rows_next = shift(rows, 1), shift(rows, 3)
    grads = came[:, 8:].reshape(slots, quarter)
    grads_prev, grads_next = shift(grads, 1), shift(grads, 3)
    rows4 = (rows, rows_next, shift(rows_prev, 1), rows_prev)
    grads4 = (grads, grads_next, shift(grads_next, 3), grads_prev)

    freq = 1.0 / 10000.0 ** jnp.linspace(0.0, 1.0, kd // 2, dtype=F32)
    freq = jnp.repeat(freq, 2)[None, :]
    base = (sp * n).astype(F32) * freq
    angles = jnp.arange(n, dtype=F32)[:, None] * freq
    qv = queries.transpose(1, 0, 2)
    kv = key_vectors.transpose(1, 0, 2)
    vv = value_vectors.transpose(1, 0, 2)
    send, pack = call(
        "prepare",
        prepare_body,
        q,
        (qv, kv, vv, log_decay.T, jnp.cos(base), jnp.sin(base), jnp.cos(angles), jnp.sin(angles)),
        [((64, 16, 128), BF), ((n, 1920), F32)],
        mib=60,
    )
    got = a2a(send, SP)
    state_sent, table = call("prefix", prefix_body, q, (got,), [((64, 8, 128), F32), ((16, 128), F32)])
    state = a2a(state_sent.astype(BF), SP).reshape(slots, 128)
    nbf, back = call(
        "normed", normed_body, q, (state, pack), [((8, n, heads * vd), BF), ((n, 896), F32)]
    )
    nball = a2a(nbf, YC)

    wrow = (quarter, hidden)
    gspec = {k: block_rows(k, wrow) for k in range(4)}
    dspec = {k: block_cols(k, (hidden, quarter)) for k in range(4)}
    act, ga, ua = call(
        "gate_up",
        gate_up_body,
        q,
        (*rows4, *[gate_w] * 4, *[up_w] * 4),
        [((slots, hidden), BF), ((slots, hidden), F32), ((slots, hidden), F32)],
        in_specs={4 + k: s for k, s in gspec.items()} | {8 + k: s for k, s in gspec.items()},
    )
    half = slots // 2
    gp, up, far_lo, far_hi, right_lo, right_hi, left_lo, left_hi, mine = call(
        "expert_back",
        expert_back_body,
        q,
        (*grads4, *[down_w] * 4, *[gate_w] * 4, *[up_w] * 4, ga, ua),
        [((slots, hidden), BF)] * 2 + [((half, quarter), BF)] * 6 + [((slots, quarter), BF)],
        in_specs={4 + k: s for k, s in dspec.items()}
        | {8 + k: s for k, s in gspec.items()}
        | {12 + k: s for k, s in gspec.items()},
        mib=24,
    )
    far_lo, far_hi = shift(far_lo, 1), shift(far_hi, 3)
    right_hi, left_lo = shift(right_hi, 1), shift(left_lo, 3)
    right_lo, left_hi = call(
        "pass_on", pass_on_body, q, (right_lo, far_lo, left_hi, far_hi), [((half, quarter), BF)] * 2
    )
    right_lo, left_hi = shift(right_lo, 1), shift(left_hi, 3)
    gate_grad, up_grad, down_grad, weights_done = call(
        "weight_grads",
        weight_grads_body,
        q,
        (*rows4, *grads4, gp, up, act),
        [((width, hidden), BF), ((width, hidden), BF), ((hidden, width), BF), ((8, 128), F32)],
        out_specs={
            0: pl.BlockSpec(wrow, lambda i, q: (lax.rem(q[0] + i, 4), 0)),
            1: pl.BlockSpec(wrow, lambda i, q: (lax.rem(q[0] + i, 4), 0)),
            2: pl.BlockSpec((hidden, quarter), lambda i, q: (0, lax.rem(q[0] + i, 4))),
        },
        grid=4,
        mib=24,
    )
    (share,) = call(
        "share", share_body, q, (mine, right_lo, right_hi, left_lo, left_hi), [((slots, quarter), BF)]
    )
    share = a2a(share.reshape(64, 8, quarter), SP).reshape(slots, quarter)
    (resid,) = call(
        "combine",
        combine_body,
        q,
        (share, qt, out_grad),
        [((n, quarter), BF)],
        in_specs={2: own},
        after=(weights_done, nball),
    )
    resid4 = around(resid)

    pspec = {4 + k: block_rows(k, (quarter, out_proj.shape[1])) for k in range(4)}
    rg, inner = call(
        "inner_grad",
        inner_grad_body,
        q,
        (*resid4, *[out_proj] * 4, back),
        [((n, heads * vd), F32), ((8, 320, 128), BF)],
        in_specs=pspec,
    )
    inner = a2a(inner, YC)
    qg, rest = call(
        "local_grads",
        local_grads_body,
        q,
        (rg, vv, pack, state),
        [((heads, n, kd), BF), ((n, 768), F32)],
    )
    inside, later = call(
        "plane",
        plane_body,
        q,
        (inner, nball, table),
        [((8, 64, 128), F32), ((8, 192, 128), BF)],
        after=(qg,),
    )
    later = a2a(later, ZAX)
    future, proj_grad = call(
        "planes",
        planes_body,
        q,
        (later, inside, table),
        [((8, 64, 128), BF), ((32, heads * vd), F32)],
    )
    future = a2a(future, YC).reshape(slots, 128)
    kg, vg = call(
        "final",
        final_body,
        q,
        (future, vv, pack, rest),
        [((heads, n, kd), BF), ((heads, n, vd), BF)],
    )
    return (
        gate_grad[None],
        up_grad[None],
        down_grad[None],
        proj_grad,
        qg.transpose(1, 0, 2),
        kg.transpose(1, 0, 2),
        vg.transpose(1, 0, 2),
    )


def solution(mesh):
    split = Mesh(mesh.devices.reshape(8, 4, 2, mesh.shape["tp"]), (*SP, TP))
    placed = (
        P(SP, None),
        P(SP, None),
        P(SP, None),
        P(SP, None),
        P(SP, TP, None),
        P(SP, TP, None),
        P(SP, TP, None),
        P(SP, TP),
        P(None, TP),
        P(SP, None, TP),
        P(SP, None, TP),
        P(SP, TP, None),
    )
    return jax.shard_map(
        per_device,
        mesh=split,
        in_specs=placed,
        out_specs=(
            P(SP, None, TP),
            P(SP, None, TP),
            P(SP, TP, None),
            P(SP, TP),
            P(SP, TP, None),
            P(SP, TP, None),
            P(SP, TP, None),
        ),
        check_vma=False,
    )
```

time: 256 us -> 227 us (0.89)
  Pallas kernels: 53.5 us -> 34.3 us
  blocking collectives: 30.8 us -> 16.8 us
  waiting for transfers between devices: 71.6 us -> 81.6 us
  starting transfers between devices: 79.1 us -> 69.5 us
  local copies, waits for them, and re-layouts: 17.3 us -> 21 us
    pallas_call x16 -> x15, Pallas kernels: 53.5 us -> 34.3 us  [call(): pl.pallas_call(kernel, out_shape=[jax.ShapeDtypeStruct(s, d) for s, d in...]
    all_to_all x1, blocking collectives: 30.8 us -> 16.8 us  [a2a(): return lax.all_to_all(x, axes, split_axis=0, concat_axis=0, tiled=True)]
    all_to_all x9 -> x7, starting transfers between devices: 65.8 us -> 53.4 us  [a2a(): return lax.all_to_all(x, axes, split_axis=0, concat_axis=0, tiled=True)]
    ppermute x12 -> x15, waiting for transfers between devices: 17.3 us -> 25.8 us  [shift(): return lax.ppermute(x, TP, [(i, (i + by) % 4) for i in range(4)])]
    unnamed x55 -> x64, local copies, waits for them, and re-layouts: 12.9 us -> 17.4 us
    ppermute x12 -> x15, starting transfers between devices: 13.3 us -> 16.2 us  [shift(): return lax.ppermute(x, TP, [(i, (i + by) % 4) for i in range(4)])]
    all_to_all x9 -> x7, waiting for transfers between devices: 54.3 us -> 55.8 us  [a2a(): return lax.all_to_all(x, axes, split_axis=0, concat_axis=0, tiled=True)]
  transfers between devices with their start and end apart: 21 -> 22, of which waited for: 11 -> 14; matrix products, arithmetic and copies ran while one was open for 4% -> 3% of each run, Pallas kernels for 19% -> 11%
where the time goes in v2:
time: 227 us; the launch traced here: 226 us
  waiting for transfers between devices  81.6 us (36%)
  starting transfers between devices  69.5 us (31%)
  Pallas kernels  34.3 us (15%)
  local copies, waits for them, and re-layouts  21 us (9%)
  blocking collectives  16.8 us (7%)
    all_to_all x7, waiting for transfers between devices, a2a(): return lax.all_to_all(x, axes, split_axis=0, concat_axis=0, tiled=True)  55.8 us
    all_to_all x7, starting transfers between devices, a2a(): return lax.all_to_all(x, axes, split_axis=0, concat_axis=0, tiled=True)  53.4 us
    pallas_call x15, Pallas kernels, call(): pl.pallas_call(kernel, out_shape=[jax.ShapeDtypeStruct(s, d) for s, d in...  34.3 us
    ppermute x15, waiting for transfers between devices, shift(): return lax.ppermute(x, TP, [(i, (i + by) % 4) for i in range(4)])  25.8 us
    unnamed x64, local copies, waits for them, and re-layouts  17.4 us
    all_to_all x1, blocking collectives, a2a(): return lax.all_to_all(x, axes, split_axis=0, concat_axis=0, tiled=True)  16.8 us
    ppermute x15, starting transfers between devices, shift(): return lax.ppermute(x, TP, [(i, (i + by) % 4) for i in range(4)])  16.2 us
  transfers between devices with their start and end apart: 22, of which 14 were waited for; matrix products, arithmetic and copies ran while one was open for 3% of the time, Pallas kernels for 11%

profile of v2, /device:TPU:1, one launch (start us, length us, event | category | flops | bytes accessed | tf_op | source)
XLA Modules:
  0.0 225.9 jit_solution(8157181823909879814)
XLA Ops:
  0.7 1.0 copy-done.8
  1.8 1.0 copy-done.12
  4.2 2.1 dispatch.1
  7.0 13.1 %all-to-all-start = ((bf16[64,16,512]{2,1,0:T(8,128)(2,1)}), bf16[64,16,512]{2,1,0:T(8,128)(2,1)S(1)}, u32[]{:S(2)}, u32[]{:S(2)}) async-start(bf16[64,16,512]{2,1,0:T(8,128)(2,1)} %get-tuple-element.43), calls=%async_computation | async-start | bytes 2097152 | tf_op jit(solution)/shard_map/all_to_all | solution.py:386
  24.4 4.1 %prepare.1 = (bf16[64,16,128]{2,1,0:T(8,128)(2,1)}, f32[128,1920]{1,0:T(8,128)}) custom-call(s32[4]{0:T(128)} %copy-done.23, bf16[2,128,128]{2,1,0:T(8,128)(2,1)} %get-tuple-element.100.refs_0_, bf16[2,128,128]{2,1,0:T(8,128)(2,1)} %get-tuple-element.99.refs_1_, bf16[2,128,256]{2,1,0:T(8,128)(2,1)} %bitcast.51, f32[2,128]{1,0:T(2,128)} %bitcast.62, ...), custom_call_target="tpu_custom_call" | custom-call | tf_op jit(solution)/shard_map/prepare/pallas_call | solution.py:56
  28.5 19.8 %all-to-all-done = bf16[64,16,512]{2,1,0:T(8,128)(2,1)S(1)} async-done(((bf16[64,16,512]{2,1,0:T(8,128)(2,1)}), bf16[64,16,512]{2,1,0:T(8,128)(2,1)S(1)}, u32[]{:S(2)}, u32[]{:S(2)}) %all-to-all-start) | async-done | bytes 1048608 | tf_op jit(solution)/shard_map/all_to_all | solution.py:386
  48.3 6.3 %all-to-all-start.2 = ((bf16[64,16,128]{2,1,0:T(8,128)(2,1)}), bf16[64,16,128]{2,1,0:T(8,128)(2,1)S(1)}, u32[]{:S(2)}, u32[]{:S(2)}) async-start(bf16[64,16,128]{2,1,0:T(8,128)(2,1)} %get-tuple-element.63), calls=%async_computation.2 | async-start | bytes 524288 | tf_op jit(solution)/shard_map/all_to_all | solution.py:386
  54.6 1.1 slice_bitcast_fusion
  55.6 1.2 collective-permute-start.1
  56.8 1.5 collective-permute-start.3
  58.3 9.3 %all-to-all-done.2.refs_0_ = bf16[64,16,128]{2,1,0:T(8,128)(2,1)S(1)} async-done(((bf16[64,16,128]{2,1,0:T(8,128)(2,1)}), bf16[64,16,128]{2,1,0:T(8,128)(2,1)S(1)}, u32[]{:S(2)}, u32[]{:S(2)}) %all-to-all-start.2) | async-done | bytes 262176 | tf_op jit(solution)/shard_map/all_to_all | solution.py:386
  67.6 1.3 prefix.1
  69.6 4.8 %all-to-all-start.3 = ((bf16[64,8,128]{2,1,0:T(8,128)(2,1)}), bf16[64,8,128]{2,1,0:T(8,128)(2,1)S(1)}, u32[]{:S(2)}, u32[]{:S(2)}) async-start(bf16[64,8,128]{2,1,0:T(8,128)(2,1)} %convert_element_type.7), calls=%async_computation.3 | async-start | bytes 262144 | tf_op jit(solution)/shard_map/all_to_all | solution.py:386
  74.4 2.6 %collective-permute-start = (bf16[512,512]{1,0:T(8,128)(2,1)}, bf16[512,512]{1,0:T(8,128)(2,1)}, u32[]{:S(2)}, u32[]{:S(2)}) collective-permute-start(bf16[512,512]{1,0:T(8,128)(2,1)} %get-tuple-element.96.refs_0_), channel_id=1, source_target_pairs={{0,3},{1,0},{2,1},{3,2},{4,7},{5,4},{6,5},{7,6},{8,11},{9,8},{10,9... | collective-permute-start | bytes 1572872 | tf_op jit(solution)/shard_map/ppermute | solution.py:390
  77.1 2.5 %collective-permute-start.4 = (bf16[512,512]{1,0:T(8,128)(2,1)}, bf16[512,512]{1,0:T(8,128)(2,1)}, u32[]{:S(2)}, u32[]{:S(2)}) collective-permute-start(bf16[512,512]{1,0:T(8,128)(2,1)} %collective-permute-done.3.refs_1_.refs_5_), channel_id=1, source_target_pairs={{0,3},{1,0},{2,1},{3,2},{4,7},{5,4},{6,5},{7,6},{8,11},{9,8},{10,9... | collective-permute-start | bytes 1572872 | tf_op jit(solution)/shard_map/ppermute | solution.py:390
  79.6 5.8 %all-to-all-done.3 = bf16[64,8,128]{2,1,0:T(8,128)(2,1)S(1)} async-done(((bf16[64,8,128]{2,1,0:T(8,128)(2,1)}), bf16[64,8,128]{2,1,0:T(8,128)(2,1)S(1)}, u32[]{:S(2)}, u32[]{:S(2)}) %all-to-all-start.3) | async-done | bytes 131104 | tf_op jit(solution)/shard_map/all_to_all | solution.py:386
  85.5 1.1 normed.1
  88.3 3.9 %all-to-all-start.4 = ((bf16[8,128,512]{2,1,0:T(8,128)(2,1)}), bf16[8,128,512]{2,1,0:T(8,128)(2,1)S(1)}, u32[]{:S(2)}, u32[]{:S(2)}) async-start(bf16[8,128,512]{2,1,0:T(8,128)(2,1)} %copy-done.10), calls=%async_computation.4 | async-start | bytes 2097152 | tf_op jit(solution)/shard_map/all_to_all | solution.py:386
  92.2 3.5 %gate_up.1 = (bf16[512,256]{1,0:T(8,128)(2,1)S(1)}, f32[512,256]{1,0:T(8,128)S(1)}, f32[512,256]{1,0:T(8,128)S(1)}) custom-call(s32[4]{0:T(128)S(1)} %copy-done.24, bf16[512,512]{1,0:T(8,128)(2,1)} %get-tuple-element.96.refs_0_, bf16[512,512]{1,0:T(8,128)(2,1)} %collective-permute-done.refs_1_, bf16[512,512]{1,0:T(8,128)(2,1)} %collective-permute-done.2.refs_2_, ...), custom_call_target="tpu_custom_call" | custom-call | tf_op jit(solution)/shard_map/gate_up/pallas_call | solution.py:56
  95.7 6.7 %collective-permute-done.5.refs_3_.refs_7_ = bf16[512,512]{1,0:T(8,128)(2,1)} collective-permute-done((bf16[512,512]{1,0:T(8,128)(2,1)}, bf16[512,512]{1,0:T(8,128)(2,1)}, u32[]{:S(2)}, u32[]{:S(2)}) %collective-permute-start.5) | collective-permute-done | bytes 524320 | tf_op jit(solution)/shard_map/ppermute | solution.py:390
  102.4 4.9 %expert_back.1 = (bf16[512,256]{1,0:T(8,128)(2,1)S(1)}, bf16[512,256]{1,0:T(8,128)(2,1)S(1)}, bf16[256,512]{1,0:T(8,128)(2,1)S(1)}, bf16[256,512]{1,0:T(8,128)(2...) custom-call(s32[4]{0:T(128)S(1)} %copy-done.24, ...), custom_call_target="tpu_custom_call" | custom-call | tf_op jit(solution)/shard_map/expert_back/pallas_call | solution.py:56
  107.5 2.7 %collective-permute-start.7 = (bf16[256,512]{1,0:T(8,128)(2,1)S(1)}, bf16[256,512]{1,0:T(8,128)(2,1)S(1)}, u32[]{:S(2)}, u32[]{:S(2)}) collective-permute-start(bf16[256,512]{1,0:T(8,128)(2,1)S(1)} %get-tuple-element.56), channel_id=1, source_target_pairs={{0,3},{1,0},{2,1},{3,2},{4,7},{5,4},{6,5},{7,6},{8,11},{9,8},{10,9... | collective-permute-start | bytes 786440 | tf_op jit(solution)/shard_map/ppermute | solution.py:390
  110.2 1.4 collective-permute-start.9
  111.6 3.3 %collective-permute-done.6.refs_1_ = bf16[256,512]{1,0:T(8,128)(2,1)S(1)} collective-permute-done((bf16[256,512]{1,0:T(8,128)(2,1)S(1)}, bf16[256,512]{1,0:T(8,128)(2,1)S(1)}, u32[]{:S(2)}, u32[]{:S(2)}) %collective-permute-start.6) | collective-permute-done | bytes 262176 | tf_op jit(solution)/shard_map/ppermute | solution.py:390
  115.6 2.5 %collective-permute-start.11 = (bf16[256,512]{1,0:T(8,128)(2,1)S(1)}, bf16[256,512]{1,0:T(8,128)(2,1)S(1)}, u32[]{:S(2)}, u32[]{:S(2)}) collective-permute-start(bf16[256,512]{1,0:T(8,128)(2,1)S(1)} %get-tuple-element.60), channel_id=1, source_target_pairs={{0,3},{1,0},{2,1},{3,2},{4,7},{5,4},{6,5},{7,6},{8,11},{9,8},{10,9... | collective-permute-start | bytes 786440 | tf_op jit(solution)/shard_map/ppermute | solution.py:390
  118.1 1.5 collective-permute-done.10.refs_3_
  120.6 4.6 %collective-permute-done.11.refs_4_ = bf16[256,512]{1,0:T(8,128)(2,1)S(1)} collective-permute-done((bf16[256,512]{1,0:T(8,128)(2,1)S(1)}, bf16[256,512]{1,0:T(8,128)(2,1)S(1)}, u32[]{:S(2)}, u32[]{:S(2)}) %collective-permute-start.11) | collective-permute-done | bytes 262176 | tf_op jit(solution)/shard_map/ppermute | solution.py:390
  125.2 1.5 share.1
  126.7 15.9 %all-to-all-start.1 = ((bf16[64,8,512]{2,1,0:T(8,128)(2,1)}), bf16[64,8,512]{2,1,0:T(8,128)(2,1)}, u32[]{:S(2)}, u32[]{:S(2)}) async-start(bf16[64,8,512]{2,1,0:T(8,128)(2,1)} %bitcast.14), calls=%async_computation.1 | async-start | bytes 1048576 | tf_op jit(solution)/shard_map/all_to_all | solution.py:386
  144.6 6.4 %weight_grads.1 = (bf16[2048,256]{1,0:T(8,128)(2,1)}, bf16[2048,256]{1,0:T(8,128)(2,1)}, bf16[256,2048]{1,0:T(8,128)(2,1)}, f32[8,128]{1,0:T(8,128)S(1)}) custom-call(s32[4]{0:T(128)S(1)} %copy-done.24, bf16[512,512]{1,0:T(8,128)(2,1)} %get-tuple-element.96.refs_0_, bf16[512,512]{1,0:T(8,128)(2,1)} %collective-permute-done.refs_1_, ...), custom_call_target="tpu_custom_call" | custom-call | tf_op jit(solution)/shard_map/weight_grads/pallas_call | solution.py:56
  151.0 9.3 %all-to-all-done.1 = bf16[64,8,512]{2,1,0:T(8,128)(2,1)} async-done(((bf16[64,8,512]{2,1,0:T(8,128)(2,1)}), bf16[64,8,512]{2,1,0:T(8,128)(2,1)}, u32[]{:S(2)}, u32[]{:S(2)}) %all-to-all-start.1) | async-done | bytes 524320 | tf_op jit(solution)/shard_map/all_to_all | solution.py:386
  160.3 1.0 copy-done.9
  162.3 1.9 combine.1.refs_0_
  164.6 1.1 collective-permute-start.14
  165.7 3.2 %collective-permute-done.12.refs_1_ = bf16[128,512]{1,0:T(8,128)(2,1)S(1)} collective-permute-done((bf16[128,512]{1,0:T(8,128)(2,1)S(1)}, bf16[128,512]{1,0:T(8,128)(2,1)S(1)}, u32[]{:S(2)}, u32[]{:S(2)}) %collective-permute-start.12) | collective-permute-done | bytes 131104 | tf_op jit(solution)/shard_map/ppermute | solution.py:390
  168.9 1.6 collective-permute-done.13.refs_2_
  170.5 3.8 %collective-permute-done.14.refs_3_ = bf16[128,512]{1,0:T(8,128)(2,1)S(1)} collective-permute-done((bf16[128,512]{1,0:T(8,128)(2,1)S(1)}, bf16[128,512]{1,0:T(8,128)(2,1)S(1)}, u32[]{:S(2)}, u32[]{:S(2)}) %collective-permute-start.14) | collective-permute-done | bytes 131104 | tf_op jit(solution)/shard_map/ppermute | solution.py:390
  175.4 1.5 inner_grad.1
  178.4 3.9 %all-to-all-start.5 = ((bf16[8,320,128]{2,1,0:T(8,128)(2,1)}), bf16[8,320,128]{2,1,0:T(8,128)(2,1)S(1)}, u32[]{:S(2)}, u32[]{:S(2)}) async-start(bf16[8,320,128]{2,1,0:T(8,128)(2,1)} %copy-done.11), calls=%async_computation.5 | async-start | bytes 1310720 | tf_op jit(solution)/shard_map/all_to_all | solution.py:386
  182.4 1.2 copy-done.5
  184.5 1.7 local_grads.1
  186.2 6.9 %all-to-all-done.5.refs_0_ = bf16[8,320,128]{2,1,0:T(8,128)(2,1)S(1)} async-done(((bf16[8,320,128]{2,1,0:T(8,128)(2,1)}), bf16[8,320,128]{2,1,0:T(8,128)(2,1)S(1)}, u32[]{:S(2)}, u32[]{:S(2)}) %all-to-all-start.5) | async-done | bytes 655392 | tf_op jit(solution)/shard_map/all_to_all | solution.py:386
  193.1 1.2 plane.1
  194.4 16.8 %all_to_all.40.refs_0_ = bf16[8,192,128]{2,1,0:T(8,128)(2,1)S(1)} all-to-all(bf16[8,192,128]{2,1,0:T(8,128)(2,1)S(1)} %get-tuple-element.72), channel_id=1, replica_groups=mesh['sp_0'=8,'sp_1'=4,'sp_2'=2,'tp'=4] {'sp_0'}, dimensions={0} | all-to-all | bytes 786432 | tf_op jit(solution)/shard_map/all_to_all | solution.py:386
  211.1 1.3 planes.1
  212.5 5.5 %all-to-all-start.7 = ((bf16[8,64,128]{2,1,0:T(8,128)(2,1)}), bf16[8,64,128]{2,1,0:T(8,128)(2,1)S(1)}, u32[]{:S(2)}, u32[]{:S(2)}) async-start(bf16[8,64,128]{2,1,0:T(8,128)(2,1)} %get-tuple-element.75), calls=%async_computation.7 | async-start | bytes 262144 | tf_op jit(solution)/shard_map/all_to_all | solution.py:386
  218.6 4.6 %all-to-all-done.7 = bf16[8,64,128]{2,1,0:T(8,128)(2,1)S(1)} async-done(((bf16[8,64,128]{2,1,0:T(8,128)(2,1)}), bf16[8,64,128]{2,1,0:T(8,128)(2,1)S(1)}, u32[]{:S(2)}, u32[]{:S(2)}) %all-to-all-start.7) | async-done | bytes 131104 | tf_op jit(solution)/shard_map/all_to_all | solution.py:386
  223.2 1.2 final.1
  (90 shorter events, 19.8 us)
Async XLA Ops:
  0.6 23.1 %copy-start.28 = (bf16[128,2,128]{2,1,0:T(2,128)(2,1)S(1)}, bf16[128,2,128]{2,1,0:T(2,128)(2,1)}, u32[]{:S(2)}) copy-start(bf16[128,2,128]{2,1,0:T(2,128)(2,1)} %param.17) | copy-start | bytes 196612
  0.7 23.6 %copy-start.23 = (s32[4]{0:T(128)}, s32[4]{0:T(128)S(1)}, u32[]{:S(2)}) copy-start(s32[4]{0:T(128)S(1)} %pad_add_fusion.q_ref) | copy-start | bytes 52
  0.7 1.0 copy-start.8
  1.8 1.0 copy-start.12
  4.2 17.9 %copy-start.27 = (bf16[128,2,256]{2,1,0:T(2,128)(2,1)S(1)}, bf16[128,2,256]{2,1,0:T(2,128)(2,1)}, u32[]{:S(2)}) copy-start(bf16[128,2,256]{2,1,0:T(2,128)(2,1)} %param.18) | copy-start | bytes 393220
  4.2 19.5 %copy-start.29 = (bf16[128,2,128]{2,1,0:T(2,128)(2,1)S(1)}, bf16[128,2,128]{2,1,0:T(2,128)(2,1)}, u32[]{:S(2)}) copy-start(bf16[128,2,128]{2,1,0:T(2,128)(2,1)} %param.16) | copy-start | bytes 196612
  7.0 41.3 %all-to-all-start = ((bf16[64,16,512]{2,1,0:T(8,128)(2,1)}), bf16[64,16,512]{2,1,0:T(8,128)(2,1)S(1)}, u32[]{:S(2)}, u32[]{:S(2)}) async-start(bf16[64,16,512]{2,1,0:T(8,128)(2,1)} %get-tuple-element.43), calls=%async_computation | async-start | bytes 2097152 | tf_op jit(solution)/shard_map/all_to_all | solution.py:386
  28.4 39.2 %copy-start.24 = (s32[4]{0:T(128)S(1)}, s32[4]{0:T(128)}, u32[]{:S(2)}) copy-start(s32[4]{0:T(128)} %copy-done.23) | copy-start | bytes 52
  28.4 57.0 %copy-start.4 = (f32[128,1920]{1,0:T(8,128)S(1)}, f32[128,1920]{1,0:T(8,128)}, u32[]{:S(2)}) copy-start(f32[128,1920]{1,0:T(8,128)} %get-tuple-element.65.refs_1_.refs_2_) | copy-start | bytes 2949124
  48.3 19.4 %all-to-all-start.2 = ((bf16[64,16,128]{2,1,0:T(8,128)(2,1)}), bf16[64,16,128]{2,1,0:T(8,128)(2,1)S(1)}, u32[]{:S(2)}, u32[]{:S(2)}) async-start(bf16[64,16,128]{2,1,0:T(8,128)(2,1)} %get-tuple-element.63), calls=%async_computation.2 | async-start | bytes 524288 | tf_op jit(solution)/shard_map/all_to_all | solution.py:386
  55.6 36.5 %copy-start = (bf16[1,2048,256]{2,1,0:T(8,128)(2,1)S(1)}, bf16[1,2048,256]{2,1,0:T(8,128)(2,1)}, u32[]{:S(2)}) copy-start(bf16[1,2048,256]{2,1,0:T(8,128)(2,1)} %param.21) | copy-start | bytes 3145732
  55.6 36.5 %copy-start.1 = (bf16[1,2048,256]{2,1,0:T(8,128)(2,1)S(1)}, bf16[1,2048,256]{2,1,0:T(8,128)(2,1)}, u32[]{:S(2)}) copy-start(bf16[1,2048,256]{2,1,0:T(8,128)(2,1)} %param.22) | copy-start | bytes 3145732
  55.6 21.3 %collective-permute-start.1 = (bf16[512,512]{1,0:T(8,128)(2,1)}, bf16[512,512]{1,0:T(8,128)(2,1)}, u32[]{:S(2)}, u32[]{:S(2)}) collective-permute-start(bf16[512,512]{1,0:T(8,128)(2,1)} %get-tuple-element.96.refs_0_), channel_id=1, source_target_pairs={{0,1},{1,2},{2,3},{3,0},{4,5},{5,6},{6,7},{7,4},{8,9},{9,10},{10,1... | collective-permute-start | bytes 1572872 | tf_op jit(solution)/shard_map/ppermute | solution.py:390
  56.8 20.3 %collective-permute-start.3 = (bf16[512,512]{1,0:T(8,128)(2,1)}, bf16[512,512]{1,0:T(8,128)(2,1)}, u32[]{:S(2)}, u32[]{:S(2)}) collective-permute-start(bf16[512,512]{1,0:T(8,128)(2,1)} %get-tuple-element.95.refs_0_.refs_4_), channel_id=1, source_target_pairs={{0,3},{1,0},{2,1},{3,2},{4,7},{5,4},{6,5},{7,6},{8,11},{9,8},{10,9... | collective-permute-start | bytes 1572872 | tf_op jit(solution)/shard_map/ppermute | solution.py:390
  69.6 15.9 %all-to-all-start.3 = ((bf16[64,8,128]{2,1,0:T(8,128)(2,1)}), bf16[64,8,128]{2,1,0:T(8,128)(2,1)S(1)}, u32[]{:S(2)}, u32[]{:S(2)}) async-start(bf16[64,8,128]{2,1,0:T(8,128)(2,1)} %convert_element_type.7), calls=%async_computation.3 | async-start | bytes 262144 | tf_op jit(solution)/shard_map/all_to_all | solution.py:386
  74.4 17.8 %collective-permute-start = (bf16[512,512]{1,0:T(8,128)(2,1)}, bf16[512,512]{1,0:T(8,128)(2,1)}, u32[]{:S(2)}, u32[]{:S(2)}) collective-permute-start(bf16[512,512]{1,0:T(8,128)(2,1)} %get-tuple-element.96.refs_0_), channel_id=1, source_target_pairs={{0,3},{1,0},{2,1},{3,2},{4,7},{5,4},{6,5},{7,6},{8,11},{9,8},{10,9... | collective-permute-start | bytes 1572872 | tf_op jit(solution)/shard_map/ppermute | solution.py:390
  76.9 15.2 %collective-permute-start.2 = (bf16[512,512]{1,0:T(8,128)(2,1)}, bf16[512,512]{1,0:T(8,128)(2,1)}, u32[]{:S(2)}, u32[]{:S(2)}) collective-permute-start(bf16[512,512]{1,0:T(8,128)(2,1)} %collective-permute-done.1.refs_3_), channel_id=1, source_target_pairs={{0,1},{1,2},{2,3},{3,0},{4,5},{5,6},{6,7},{7,4},{8,9},{9,10},{10,1... | collective-permute-start | bytes 1572872 | tf_op jit(solution)/shard_map/ppermute | solution.py:390
  76.9 25.5 %collective-permute-start.5 = (bf16[512,512]{1,0:T(8,128)(2,1)}, bf16[512,512]{1,0:T(8,128)(2,1)}, u32[]{:S(2)}, u32[]{:S(2)}) collective-permute-start(bf16[512,512]{1,0:T(8,128)(2,1)} %get-tuple-element.95.refs_0_.refs_4_), channel_id=1, source_target_pairs={{0,1},{1,2},{2,3},{3,0},{4,5},{5,6},{6,7},{7,4},{8,9},{9,10},{10,1... | collective-permute-start | bytes 1572872 | tf_op jit(solution)/shard_map/ppermute | solution.py:390
  77.1 25.3 %collective-permute-start.4 = (bf16[512,512]{1,0:T(8,128)(2,1)}, bf16[512,512]{1,0:T(8,128)(2,1)}, u32[]{:S(2)}, u32[]{:S(2)}) collective-permute-start(bf16[512,512]{1,0:T(8,128)(2,1)} %collective-permute-done.3.refs_1_.refs_5_), channel_id=1, source_target_pairs={{0,3},{1,0},{2,1},{3,2},{4,7},{5,4},{6,5},{7,6},{8,11},{9,8},{10,9... | collective-permute-start | bytes 1572872 | tf_op jit(solution)/shard_map/ppermute | solution.py:390
  86.5 1.0 copy-start.10
  87.5 0.8 copy-start.13
  88.3 38.5 %all-to-all-start.4 = ((bf16[8,128,512]{2,1,0:T(8,128)(2,1)}), bf16[8,128,512]{2,1,0:T(8,128)(2,1)S(1)}, u32[]{:S(2)}, u32[]{:S(2)}) async-start(bf16[8,128,512]{2,1,0:T(8,128)(2,1)} %copy-done.10), calls=%async_computation.4 | async-start | bytes 2097152 | tf_op jit(solution)/shard_map/all_to_all | solution.py:386
  92.1 10.3 %copy-start.3 = (bf16[1,256,2048]{2,1,0:T(8,128)(2,1)S(1)}, bf16[1,256,2048]{2,1,0:T(8,128)(2,1)}, u32[]{:S(2)}) copy-start(bf16[1,256,2048]{2,1,0:T(8,128)(2,1)} %param.23) | copy-start | bytes 3145732
  107.4 17.8 %copy-start.15 = (bf16[512,256]{1,0:T(8,128)(2,1)}, bf16[512,256]{1,0:T(8,128)(2,1)S(1)}, u32[]{:S(2)}) copy-start(bf16[512,256]{1,0:T(8,128)(2,1)S(1)} %get-tuple-element.46.refs_8_) | copy-start | bytes 786436
  107.4 17.8 %copy-start.17 = (bf16[512,256]{1,0:T(8,128)(2,1)}, bf16[512,256]{1,0:T(8,128)(2,1)S(1)}, u32[]{:S(2)}) copy-start(bf16[512,256]{1,0:T(8,128)(2,1)S(1)} %get-tuple-element.47.refs_9_) | copy-start | bytes 786436
  107.4 7.6 %collective-permute-start.6 = (bf16[256,512]{1,0:T(8,128)(2,1)S(1)}, bf16[256,512]{1,0:T(8,128)(2,1)S(1)}, u32[]{:S(2)}, u32[]{:S(2)}) collective-permute-start(bf16[256,512]{1,0:T(8,128)(2,1)S(1)} %get-tuple-element.54), channel_id=1, source_target_pairs={{0,1},{1,2},{2,3},{3,0},{4,5},{5,6},{6,7},{7,4},{8,9},{9,10},{10,1... | collective-permute-start | bytes 786440 | tf_op jit(solution)/shard_map/ppermute | solution.py:390
  107.5 7.5 %collective-permute-start.7 = (bf16[256,512]{1,0:T(8,128)(2,1)S(1)}, bf16[256,512]{1,0:T(8,128)(2,1)S(1)}, u32[]{:S(2)}, u32[]{:S(2)}) collective-permute-start(bf16[256,512]{1,0:T(8,128)(2,1)S(1)} %get-tuple-element.56), channel_id=1, source_target_pairs={{0,3},{1,0},{2,1},{3,2},{4,7},{5,4},{6,5},{7,6},{8,11},{9,8},{10,9... | collective-permute-start | bytes 786440 | tf_op jit(solution)/shard_map/ppermute | solution.py:390
  110.2 9.4 %collective-permute-start.10 = (bf16[256,512]{1,0:T(8,128)(2,1)S(1)}, bf16[256,512]{1,0:T(8,128)(2,1)S(1)}, u32[]{:S(2)}, u32[]{:S(2)}) collective-permute-start(bf16[256,512]{1,0:T(8,128)(2,1)S(1)} %get-tuple-element.59), channel_id=1, source_target_pairs={{0,3},{1,0},{2,1},{3,2},{4,7},{5,4},{6,5},{7,6},{8,11},{9,8},{10,9... | collective-permute-start | bytes 786440 | tf_op jit(solution)/shard_map/ppermute | solution.py:390
  110.2 10.4 %collective-permute-start.9 = (bf16[256,512]{1,0:T(8,128)(2,1)S(1)}, bf16[256,512]{1,0:T(8,128)(2,1)S(1)}, u32[]{:S(2)}, u32[]{:S(2)}) collective-permute-start(bf16[256,512]{1,0:T(8,128)(2,1)S(1)} %get-tuple-element.58), channel_id=1, source_target_pairs={{0,1},{1,2},{2,3},{3,0},{4,5},{5,6},{6,7},{7,4},{8,9},{9,10},{10,1... | collective-permute-start | bytes 786440 | tf_op jit(solution)/shard_map/ppermute | solution.py:390
  115.6 9.6 %collective-permute-start.11 = (bf16[256,512]{1,0:T(8,128)(2,1)S(1)}, bf16[256,512]{1,0:T(8,128)(2,1)S(1)}, u32[]{:S(2)}, u32[]{:S(2)}) collective-permute-start(bf16[256,512]{1,0:T(8,128)(2,1)S(1)} %get-tuple-element.60), channel_id=1, source_target_pairs={{0,3},{1,0},{2,1},{3,2},{4,7},{5,4},{6,5},{7,6},{8,11},{9,8},{10,9... | collective-permute-start | bytes 786440 | tf_op jit(solution)/shard_map/ppermute | solution.py:390
  118.1 7.1 %collective-permute-start.8 = (bf16[256,512]{1,0:T(8,128)(2,1)S(1)}, bf16[256,512]{1,0:T(8,128)(2,1)S(1)}, u32[]{:S(2)}, u32[]{:S(2)}) collective-permute-start(bf16[256,512]{1,0:T(8,128)(2,1)S(1)} %get-tuple-element.57), channel_id=1, source_target_pairs={{0,1},{1,2},{2,3},{3,0},{4,5},{5,6},{6,7},{7,4},{8,9},{9,10},{10,1... | collective-permute-start | bytes 786440 | tf_op jit(solution)/shard_map/ppermute | solution.py:390
  126.7 33.5 %all-to-all-start.1 = ((bf16[64,8,512]{2,1,0:T(8,128)(2,1)}), bf16[64,8,512]{2,1,0:T(8,128)(2,1)}, u32[]{:S(2)}, u32[]{:S(2)}) async-start(bf16[64,8,512]{2,1,0:T(8,128)(2,1)} %bitcast.14), calls=%async_computation.1 | async-start | bytes 1048576 | tf_op jit(solution)/shard_map/all_to_all | solution.py:386
  142.7 1.0 copy-start.16
  143.6 0.9 copy-start.18
  151.0 23.4 %copy-start.2 = (bf16[2048,512]{1,0:T(8,128)(2,1)S(1)}, bf16[2048,512]{1,0:T(8,128)(2,1)}, u32[]{:S(2)}) copy-start(bf16[2048,512]{1,0:T(8,128)(2,1)} %refs_7_.1) | copy-start | bytes 6291460
  160.3 1.0 copy-start.9
  161.3 0.9 copy-start.22
  164.1 4.7 %collective-permute-start.12 = (bf16[128,512]{1,0:T(8,128)(2,1)S(1)}, bf16[128,512]{1,0:T(8,128)(2,1)S(1)}, u32[]{:S(2)}, u32[]{:S(2)}) collective-permute-start(bf16[128,512]{1,0:T(8,128)(2,1)S(1)} %combine.1.refs_0_), channel_id=1, source_target_pairs={{0,3},{1,0},{2,1},{3,2},{4,7},{5,4},{6,5},{7,6},{8,11},{9,8},{10,9... | collective-permute-start | bytes 393224 | tf_op jit(solution)/shard_map/ppermute | solution.py:390
  164.6 5.9 %collective-permute-start.13 = (bf16[128,512]{1,0:T(8,128)(2,1)S(1)}, bf16[128,512]{1,0:T(8,128)(2,1)S(1)}, u32[]{:S(2)}, u32[]{:S(2)}) collective-permute-start(bf16[128,512]{1,0:T(8,128)(2,1)S(1)} %combine.1.refs_0_), channel_id=1, source_target_pairs={{0,2},{1,3},{2,0},{3,1},{4,6},{5,7},{6,4},{7,5},{8,10},{9,11},{10,... | collective-permute-start | bytes 393224 | tf_op jit(solution)/shard_map/ppermute | solution.py:390
  164.6 9.7 %collective-permute-start.14 = (bf16[128,512]{1,0:T(8,128)(2,1)S(1)}, bf16[128,512]{1,0:T(8,128)(2,1)S(1)}, u32[]{:S(2)}, u32[]{:S(2)}) collective-permute-start(bf16[128,512]{1,0:T(8,128)(2,1)S(1)} %combine.1.refs_0_), channel_id=1, source_target_pairs={{0,1},{1,2},{2,3},{3,0},{4,5},{5,6},{6,7},{7,4},{8,9},{9,10},{10,1... | collective-permute-start | bytes 393224 | tf_op jit(solution)/shard_map/ppermute | solution.py:390
  174.3 1.0 copy-start.14
  175.3 7.0 %copy-start.7 = (bf16[128,2,256]{2,0,1:T(8,128)(2,1)S(1)}, bf16[128,2,256]{2,0,1:T(8,128)(2,1)}, u32[]{:S(2)}) copy-start(bf16[128,2,256]{2,0,1:T(8,128)(2,1)} %copy.34) | copy-start | bytes 393220
  176.9 0.8 copy-start.11
  178.4 14.7 %all-to-all-start.5 = ((bf16[8,320,128]{2,1,0:T(8,128)(2,1)}), bf16[8,320,128]{2,1,0:T(8,128)(2,1)S(1)}, u32[]{:S(2)}, u32[]{:S(2)}) async-start(bf16[8,320,128]{2,1,0:T(8,128)(2,1)} %copy-done.11), calls=%async_computation.5 | async-start | bytes 1310720 | tf_op jit(solution)/shard_map/all_to_all | solution.py:386
  182.4 1.2 copy-start.5
  183.6 0.9 copy-start.20
  186.2 37.0 %copy-start.6 = (f32[128,1920]{1,0:T(8,128)S(1)}, f32[128,1920]{1,0:T(8,128)}, u32[]{:S(2)}) copy-start(f32[128,1920]{1,0:T(8,128)} %get-tuple-element.65.refs_1_.refs_2_) | copy-start | bytes 2949124
  212.5 10.7 %all-to-all-start.7 = ((bf16[8,64,128]{2,1,0:T(8,128)(2,1)}), bf16[8,64,128]{2,1,0:T(8,128)(2,1)S(1)}, u32[]{:S(2)}, u32[]{:S(2)}) async-start(bf16[8,64,128]{2,1,0:T(8,128)(2,1)} %get-tuple-element.75), calls=%async_computation.7 | async-start | bytes 262144 | tf_op jit(solution)/shard_map/all_to_all | solution.py:386
  (4 other events, 2.8 us)

commit v3 on v2

--- a/solution.py
+++ b/solution.py
@@ -1,18 +1,17 @@
-import functools
-
 import jax
 import jax.numpy as jnp
-import numpy as np
 from jax import lax
 from jax.experimental import pallas as pl
 from jax.experimental.pallas import tpu as pltpu
 from jax.sharding import Mesh
 from jax.sharding import PartitionSpec as P
 
+
 SP = ("sp_0", "sp_1", "sp_2")
 YC = ("sp_1", "sp_2")
 ZAX = "sp_0"
 TP = "tp"
+
 
 CLAMP_LIMIT = 7.0
 GATE_SLOPE = 1.702
@@ -42,11 +41,12 @@
     return pl.BlockSpec(shape, lambda i, q: (0,) * len(shape))
 
 
-def call(name, body, q, args, outs, in_specs=None, out_specs=None, grid=1, after=(), mib=16):
+def call(body, q, args, outs, in_specs=None, out_specs=None, grid=1, after=(), mib=16, hbm_in=(), hbm_out=()):
     in_specs = dict(in_specs or {})
     out_specs = out_specs or {}
     used = len(args)
     args = (*args, *after)
+    args = tuple(pltpu.with_memory_space_constraint(a, pltpu.HBM) if i in hbm_in else a for i, a in enumerate(args))
     for i in range(used, len(args)):
         in_specs[i] = pl.BlockSpec(memory_space=pltpu.HBM)
 
@@ -55,7 +55,7 @@
 
     return pl.pallas_call(
         kernel,
-        out_shape=[jax.ShapeDtypeStruct(s, d) for s, d in outs],
+        out_shape=[(pltpu.HBM if i in hbm_out else jax.ShapeDtypeStruct)(s, d) for i, (s, d) in enumerate(outs)],
         grid_spec=pltpu.PrefetchScalarGridSpec(
             num_scalar_prefetch=1,
             grid=(grid,),
@@ -63,7 +63,6 @@
             out_specs=[out_specs.get(i, whole(s)) for i, (s, _) in enumerate(outs)],
         ),
         compiler_params=pltpu.CompilerParams(vmem_limit_bytes=mib << 20),
-        name=name,
     )(q, *args)
 
 
@@ -245,8 +244,7 @@
     seg = mmh(jnp.where(tj < ti, 1.0, 0.0), after)
     w = jnp.where(tj < ti, jnp.exp(seg), 0.0)
     acc = mmh(w, jnp.concatenate([xf[:, k, :] for k in range(8)], axis=1))
-    for k in range(8):
-        out[:, k, :] = acc[:, k * 128 : (k + 1) * 128]
+    out[...] = jnp.stack([acc[:, k * 128 : (k + 1) * 128] for k in range(8)], axis=1).astype(BF)
     other = jnp.where(j >= 4, logs[1], logs[0])[:, 0:1]
     row = jnp.sum(jnp.where(ti == tj, other, 0.0), axis=0, keepdims=True)
     i, m = iota((16, n), 0), iota((16, n), 1)
@@ -318,8 +316,8 @@
 
 
 def local_grads_body(q, rg, vv, pack, state, qg, rest):
-    n = pack.shape[0]
     heads, vd = 2, 256
+    parts = []
     st = state[...].astype(F32)
     c, s = pack[:, COS : COS + 128], pack[:, SIN : SIN + 128]
     for h in range(heads):
@@ -328,9 +326,10 @@
         score = mmh(grad, vv[h].astype(F32), NT) * pack[:, MASK + at : MASK + at + 128]
         grow = pack[:, SCAL + h : SCAL + h + 1]
         qp = mmh(score, pack[:, KR + at : KR + at + 128]) + grow * mmh(grad, joined(st, h, vd), NT)
-        qg[h] = turned(qp, c, -s).astype(BF)
+        parts.append(turned(qp, c, -s))
         rest[:, at : at + 128] = mmh(score.T, pack[:, QR + at : QR + at + 128])
         rest[:, 256 + h * vd : 256 + (h + 1) * vd] = mmh(pack[:, WTS + at : WTS + at + 128].T, grad)
+    qg[...] = jnp.stack(parts, axis=1).astype(BF)
 
 
 def plane_body(q, x, nb, table, inside, send):
@@ -370,6 +369,7 @@
 
 def final_body(q, state, vv, pack, rest, kg, vg):
     heads, vd, kd = 2, 256, 128
+    keys, values = [], []
     st = state[...].astype(F32)
     c, s = pack[:, COS : COS + 128], pack[:, SIN : SIN + 128]
     for h in range(heads):
@@ -377,9 +377,11 @@
         fut = joined(st, h, vd)
         left = pack[:, SCAL + 2 + h : SCAL + 3 + h]
         kt = rest[:, at : at + 128] + left * mmh(vv[h].astype(F32), fut, NT)
-        kg[h] = (turned(kt, c, -s) * (kd**-0.5)).astype(BF)
+        keys.append(turned(kt, c, -s) * (kd**-0.5))
         vt = rest[:, 256 + h * vd : 256 + (h + 1) * vd]
-        vg[h] = (vt + left * mmh(pack[:, KR + at : KR + at + 128], fut)).astype(BF)
+        values.append(vt + left * mmh(pack[:, KR + at : KR + at + 128], fut))
+    kg[...] = jnp.stack(keys, axis=1).astype(BF)
+    vg[...] = jnp.stack(values, axis=1).astype(BF)
 
 
 def a2a(x, axes):
@@ -429,20 +431,21 @@
 
     own = pl.BlockSpec((n, quarter), lambda i, q: (0, q[0]))
     sent, qt = call(
-        "dispatch",
         dispatch_body,
         q,
         (routes.T, route_weight.T, stream, out_grad),
         [((64, 16, quarter), BF), ((2 * n, slots), BF)],
         in_specs={2: own, 3: own},
+        mib=60,
     )
     came = a2a(sent, SP)
     rows = came[:, :8].reshape(slots, quarter)
+    grads = came[:, 8:].reshape(slots, quarter)
     rows_prev, rows_next = shift(rows, 1), shift(rows, 3)
-    grads = came[:, 8:].reshape(slots, quarter)
     grads_prev, grads_next = shift(grads, 1), shift(grads, 3)
-    rows4 = (rows, rows_next, shift(rows_prev, 1), rows_prev)
-    grads4 = (grads, grads_next, shift(grads_next, 3), grads_prev)
+    rows_far, grads_far = shift(rows_prev, 1), shift(grads_next, 3)
+    rows4 = (rows, rows_next, rows_far, rows_prev)
+    grads4 = (grads, grads_next, grads_far, grads_prev)
 
     freq = 1.0 / 10000.0 ** jnp.linspace(0.0, 1.0, kd // 2, dtype=F32)
     freq = jnp.repeat(freq, 2)[None, :]
@@ -452,7 +455,6 @@
     kv = key_vectors.transpose(1, 0, 2)
     vv = value_vectors.transpose(1, 0, 2)
     send, pack = call(
-        "prepare",
         prepare_body,
         q,
         (qv, kv, vv, log_decay.T, jnp.cos(base), jnp.sin(base), jnp.cos(angles), jnp.sin(angles)),
@@ -460,10 +462,11 @@
         mib=60,
     )
     got = a2a(send, SP)
-    state_sent, table = call("prefix", prefix_body, q, (got,), [((64, 8, 128), F32), ((16, 128), F32)])
-    state = a2a(state_sent.astype(BF), SP).reshape(slots, 128)
+    state_sent, table = call(prefix_body, q, (got,), [((64, 8, 128), BF), ((16, 128), F32)])
+    state = a2a(state_sent, SP).reshape(slots, 128)
     nbf, back = call(
-        "normed", normed_body, q, (state, pack), [((8, n, heads * vd), BF), ((n, 896), F32)]
+        normed_body, q, (state, pack), [((8, n, heads * vd), BF), ((n, 896), F32)],
+        hbm_out=(0, 1),
     )
     nball = a2a(nbf, YC)
 
@@ -471,7 +474,6 @@
     gspec = {k: block_rows(k, wrow) for k in range(4)}
     dspec = {k: block_cols(k, (hidden, quarter)) for k in range(4)}
     act, ga, ua = call(
-        "gate_up",
         gate_up_body,
         q,
         (*rows4, *[gate_w] * 4, *[up_w] * 4),
@@ -480,7 +482,6 @@
     )
     half = slots // 2
     gp, up, far_lo, far_hi, right_lo, right_hi, left_lo, left_hi, mine = call(
-        "expert_back",
         expert_back_body,
         q,
         (*grads4, *[down_w] * 4, *[gate_w] * 4, *[up_w] * 4, ga, ua),
@@ -489,15 +490,16 @@
         | {8 + k: s for k, s in gspec.items()}
         | {12 + k: s for k, s in gspec.items()},
         mib=24,
+        hbm_out=range(9),
     )
     far_lo, far_hi = shift(far_lo, 1), shift(far_hi, 3)
     right_hi, left_lo = shift(right_hi, 1), shift(left_lo, 3)
     right_lo, left_hi = call(
-        "pass_on", pass_on_body, q, (right_lo, far_lo, left_hi, far_hi), [((half, quarter), BF)] * 2
+        pass_on_body, q, (right_lo, far_lo, left_hi, far_hi), [((half, quarter), BF)] * 2,
+        hbm_in=range(4), hbm_out=range(2),
     )
     right_lo, left_hi = shift(right_lo, 1), shift(left_hi, 3)
     gate_grad, up_grad, down_grad, weights_done = call(
-        "weight_grads",
         weight_grads_body,
         q,
         (*rows4, *grads4, gp, up, act),
@@ -511,69 +513,46 @@
         mib=24,
     )
     (share,) = call(
-        "share", share_body, q, (mine, right_lo, right_hi, left_lo, left_hi), [((slots, quarter), BF)]
+        share_body, q, (mine, right_lo, right_hi, left_lo, left_hi), [((slots, quarter), BF)],
+        hbm_in=range(5),
     )
     share = a2a(share.reshape(64, 8, quarter), SP).reshape(slots, quarter)
     (resid,) = call(
-        "combine",
         combine_body,
         q,
         (share, qt, out_grad),
         [((n, quarter), BF)],
         in_specs={2: own},
         after=(weights_done, nball),
+        hbm_in=(1, 2),
     )
     resid4 = around(resid)
 
     pspec = {4 + k: block_rows(k, (quarter, out_proj.shape[1])) for k in range(4)}
     rg, inner = call(
-        "inner_grad",
         inner_grad_body,
         q,
         (*resid4, *[out_proj] * 4, back),
         [((n, heads * vd), F32), ((8, 320, 128), BF)],
         in_specs=pspec,
+        hbm_in=(8,),
+        hbm_out=(0, 1),
     )
     inner = a2a(inner, YC)
-    qg, rest = call(
-        "local_grads",
-        local_grads_body,
-        q,
-        (rg, vv, pack, state),
-        [((heads, n, kd), BF), ((n, 768), F32)],
-    )
-    inside, later = call(
-        "plane",
-        plane_body,
-        q,
-        (inner, nball, table),
-        [((8, 64, 128), F32), ((8, 192, 128), BF)],
-        after=(qg,),
-    )
+    qg, rest = call(local_grads_body, q, (rg, vv, pack, state), [((n, heads, kd), BF), ((n, 768), F32)])
+    inside, later = call(plane_body, q, (inner, nball, table), [((8, 64, 128), F32), ((8, 192, 128), BF)], after=(qg,))
     later = a2a(later, ZAX)
-    future, proj_grad = call(
-        "planes",
-        planes_body,
-        q,
-        (later, inside, table),
-        [((8, 64, 128), BF), ((32, heads * vd), F32)],
-    )
+    future, proj_grad = call(planes_body, q, (later, inside, table), [((8, 64, 128), BF), ((32, heads * vd), F32)])
     future = a2a(future, YC).reshape(slots, 128)
-    kg, vg = call(
-        "final",
-        final_body,
-        q,
-        (future, vv, pack, rest),
-        [((heads, n, kd), BF), ((heads, n, vd), BF)],
-    )
+    kg, vg = call(final_body, q, (future, vv, pack, rest), [((n, heads, kd), BF), ((n, heads, vd), BF)])
     return (
         gate_grad[None],
         up_grad[None],
         down_grad[None],
         proj_grad,
-        qg.transpose(1, 0, 2),
-        kg.transpose(1, 0, 2),
-        vg.transpose(1, 0, 2),
+        qg,
+        kg,
+        vg,
     )
 
 
@@ -593,6 +572,7 @@
         P(SP, None, TP),
         P(SP, TP, None),
     )
+
     return jax.shard_map(
         per_device,
         mesh=split,

time: 227 us -> 226 us (level)
  local copies, waits for them, and re-layouts: 21 us -> 9.41 us
  Pallas kernels: 34.3 us -> 44.8 us
  blocking collectives: 16.8 us -> 26.6 us
  starting transfers between devices: 69.5 us -> 64.4 us
  waiting for transfers between devices: 81.6 us -> 77.7 us
    unnamed x64 -> x49, local copies, waits for them, and re-layouts: 17.4 us -> 5.96 us
    pallas_call x15, Pallas kernels: 34.3 us -> 44.8 us  [call(): pl.pallas_call(kernel, out_shape=[(pltpu.HBM if i in hbm_out else jax.Sha...]
    all_to_all x1 -> x2, blocking collectives: 16.8 us -> 26.6 us  [a2a(): return lax.all_to_all(x, axes, split_axis=0, concat_axis=0, tiled=True)]
    all_to_all x7 -> x6, starting transfers between devices: 53.4 us -> 48.6 us  [a2a(): return lax.all_to_all(x, axes, split_axis=0, concat_axis=0, tiled=True)]
    all_to_all x7 -> x6, waiting for transfers between devices: 55.8 us -> 52.5 us  [a2a(): return lax.all_to_all(x, axes, split_axis=0, concat_axis=0, tiled=True)]
  transfers between devices with their start and end apart: 22 -> 21, of which waited for: 14 -> 12; matrix products, arithmetic and copies ran while one was open for 3% -> 2% of each run, Pallas kernels for 11% -> 14%
where the time goes in v3:
time: 226 us
  waiting for transfers between devices  77.7 us (34%)
  starting transfers between devices  64.4 us (28%)
  Pallas kernels  44.8 us (20%)
  blocking collectives  26.6 us (12%)
  local copies, waits for them, and re-layouts  9.41 us (4%)
    all_to_all x6, waiting for transfers between devices, a2a(): return lax.all_to_all(x, axes, split_axis=0, concat_axis=0, tiled=True)  52.5 us
    all_to_all x6, starting transfers between devices, a2a(): return lax.all_to_all(x, axes, split_axis=0, concat_axis=0, tiled=True)  48.6 us
    pallas_call x15, Pallas kernels, call(): pl.pallas_call(kernel, out_shape=[(pltpu.HBM if i in hbm_out else jax.Sha...  44.8 us
    all_to_all x2, blocking collectives, a2a(): return lax.all_to_all(x, axes, split_axis=0, concat_axis=0, tiled=True)  26.6 us
    ppermute x15, waiting for transfers between devices, shift(): return lax.ppermute(x, TP, [(i, (i + by) % 4) for i in range(4)])  25.2 us
    ppermute x15, starting transfers between devices, shift(): return lax.ppermute(x, TP, [(i, (i + by) % 4) for i in range(4)])  15.9 us
    unnamed x49, local copies, waits for them, and re-layouts  5.96 us
  transfers between devices with their start and end apart: 21, of which 12 were waited for; matrix products, arithmetic and copies ran while one was open for 2% of the time, Pallas kernels for 14%

profile of v3, /device:TPU:1, one launch (start us, length us, event | category | flops | bytes accessed | tf_op | source)
XLA Modules:
  0.0 225.5 jit_solution(16709633776072476963)
XLA Ops:
  1.3 3.2 %shard_map.171 = (bf16[64,16,512]{2,1,0:T(8,128)(2,1)}, bf16[256,512]{1,0:T(8,128)(2,1)}) custom-call(s32[4]{0:T(128)} %pad_add_fusion.q_ref, s32[2,128]{1,0:T(2,128)} %bitcast.55, f32[2,128]{1,0:T(2,128)} %bitcast.56, bf16[128,2048]{1,0:T(8,128)(2,1)} %refs_2_.2, bf16[128,2048]{1,0:T(8,128)(2,1)} %refs_2_.3), custom_call_target="tpu_custom_call" | custom-call | tf_op jit(solution)/shard_map/pallas_call | solution.py:56
  4.5 13.1 %all-to-all-start = ((bf16[64,16,512]{2,1,0:T(8,128)(2,1)}), bf16[64,16,512]{2,1,0:T(8,128)(2,1)S(1)}, u32[]{:S(2)}, u32[]{:S(2)}) async-start(bf16[64,16,512]{2,1,0:T(8,128)(2,1)} %get-tuple-element.43), calls=%async_computation | async-start | bytes 2097152 | tf_op jit(solution)/shard_map/all_to_all | solution.py:388
  20.2 0.9 fusion
  21.8 4.1 %shard_map.177 = (bf16[64,16,128]{2,1,0:T(8,128)(2,1)}, f32[128,1920]{1,0:T(8,128)}) custom-call(s32[4]{0:T(128)} %pad_add_fusion.q_ref, bf16[2,128,128]{2,1,0:T(8,128)(2,1)} %get-tuple-element.86.refs_0_, bf16[2,128,128]{2,1,0:T(8,128)(2,1)} %get-tuple-element.85.refs_1_, bf16[2,128,256]{2,1,0:T(8,128)(2,1)} %bitcast.48, f32[2,128]{1,0:T(2,128)} %bitcast.54, ...), custom_call_target="tpu_custom_call" | custom-call | tf_op jit(solution)/shard_map/pallas_call | solution.py:56
  25.9 19.9 %all-to-all-done = bf16[64,16,512]{2,1,0:T(8,128)(2,1)S(1)} async-done(((bf16[64,16,512]{2,1,0:T(8,128)(2,1)}), bf16[64,16,512]{2,1,0:T(8,128)(2,1)S(1)}, u32[]{:S(2)}, u32[]{:S(2)}) %all-to-all-start) | async-done | bytes 1048608 | tf_op jit(solution)/shard_map/all_to_all | solution.py:388
  45.8 6.3 %all-to-all-start.2 = ((bf16[64,16,128]{2,1,0:T(8,128)(2,1)}), bf16[64,16,128]{2,1,0:T(8,128)(2,1)S(1)}, u32[]{:S(2)}, u32[]{:S(2)}) async-start(bf16[64,16,128]{2,1,0:T(8,128)(2,1)} %get-tuple-element.63), calls=%async_computation.2 | async-start | bytes 524288 | tf_op jit(solution)/shard_map/all_to_all | solution.py:388
  52.1 1.1 slice_bitcast_fusion
  53.1 1.2 collective-permute-start.1
  54.4 1.5 collective-permute-start.3
  55.8 9.3 %all-to-all-done.2.refs_0_ = bf16[64,16,128]{2,1,0:T(8,128)(2,1)S(1)} async-done(((bf16[64,16,128]{2,1,0:T(8,128)(2,1)}), bf16[64,16,128]{2,1,0:T(8,128)(2,1)S(1)}, u32[]{:S(2)}, u32[]{:S(2)}) %all-to-all-start.2) | async-done | bytes 262176 | tf_op jit(solution)/shard_map/all_to_all | solution.py:388
  65.2 2.0 shard_map.178
  67.1 4.8 %all-to-all-start.3 = ((bf16[64,8,128]{2,1,0:T(8,128)(2,1)}), bf16[64,8,128]{2,1,0:T(8,128)(2,1)S(1)}, u32[]{:S(2)}, u32[]{:S(2)}) async-start(bf16[64,8,128]{2,1,0:T(8,128)(2,1)} %get-tuple-element.64), calls=%async_computation.3 | async-start | bytes 262144 | tf_op jit(solution)/shard_map/all_to_all | solution.py:388
  71.9 2.6 %collective-permute-start = (bf16[512,512]{1,0:T(8,128)(2,1)}, bf16[512,512]{1,0:T(8,128)(2,1)}, u32[]{:S(2)}, u32[]{:S(2)}) collective-permute-start(bf16[512,512]{1,0:T(8,128)(2,1)} %get-tuple-element.82.refs_0_), channel_id=1, source_target_pairs={{0,3},{1,0},{2,1},{3,2},{4,7},{5,4},{6,5},{7,6},{8,11},{9,8},{10,9... | collective-permute-start | bytes 1572872 | tf_op jit(solution)/shard_map/ppermute | solution.py:392
  74.7 2.5 %collective-permute-start.4 = (bf16[512,512]{1,0:T(8,128)(2,1)}, bf16[512,512]{1,0:T(8,128)(2,1)}, u32[]{:S(2)}, u32[]{:S(2)}) collective-permute-start(bf16[512,512]{1,0:T(8,128)(2,1)} %collective-permute-done.3.refs_1_.refs_5_), channel_id=1, source_target_pairs={{0,3},{1,0},{2,1},{3,2},{4,7},{5,4},{6,5},{7,6},{8,11},{9,8},{10,9... | collective-permute-start | bytes 1572872 | tf_op jit(solution)/shard_map/ppermute | solution.py:392
  77.2 5.8 %all-to-all-done.3 = bf16[64,8,128]{2,1,0:T(8,128)(2,1)S(1)} async-done(((bf16[64,8,128]{2,1,0:T(8,128)(2,1)}), bf16[64,8,128]{2,1,0:T(8,128)(2,1)S(1)}, u32[]{:S(2)}, u32[]{:S(2)}) %all-to-all-start.3) | async-done | bytes 131104 | tf_op jit(solution)/shard_map/all_to_all | solution.py:388
  83.0 2.2 shard_map.179
  85.2 3.9 %all-to-all-start.4 = ((bf16[8,128,512]{2,1,0:T(8,128)(2,1)}), bf16[8,128,512]{2,1,0:T(8,128)(2,1)S(1)}, u32[]{:S(2)}, u32[]{:S(2)}) async-start(bf16[8,128,512]{2,1,0:T(8,128)(2,1)} %get-tuple-element.66), calls=%async_computation.4 | async-start | bytes 2097152 | tf_op jit(solution)/shard_map/all_to_all | solution.py:388
  89.1 3.5 %shard_map.172 = (bf16[512,256]{1,0:T(8,128)(2,1)S(1)}, f32[512,256]{1,0:T(8,128)S(1)}, f32[512,256]{1,0:T(8,128)S(1)}) custom-call(s32[4]{0:T(128)S(1)} %copy-done.13, bf16[512,512]{1,0:T(8,128)(2,1)} %get-tuple-element.82.refs_0_, bf16[512,512]{1,0:T(8,128)(2,1)} %collective-permute-done.refs_1_, bf16[512,512]{1,0:T(8,128)(2,1)} %collective-permute-done.2.refs_2_, ...), custom_call_target="tpu_custom_call" | custom-call | tf_op jit(solution)/shard_map/pallas_call | solution.py:56
  93.3 6.7 %collective-permute-done.5.refs_3_.refs_7_ = bf16[512,512]{1,0:T(8,128)(2,1)} collective-permute-done((bf16[512,512]{1,0:T(8,128)(2,1)}, bf16[512,512]{1,0:T(8,128)(2,1)}, u32[]{:S(2)}, u32[]{:S(2)}) %collective-permute-start.5) | collective-permute-done | bytes 524320 | tf_op jit(solution)/shard_map/ppermute | solution.py:392
  100.0 5.7 %shard_map.173 = (bf16[512,256]{1,0:T(8,128)(2,1)}, bf16[512,256]{1,0:T(8,128)(2,1)}, bf16[256,512]{1,0:T(8,128)(2,1)}, bf16[256,512]{1,0:T(8,128)(2,1)}, bf16[2...) custom-call(s32[4]{0:T(128)S(1)} %copy-done.13, ...), custom_call_target="tpu_custom_call" | custom-call | tf_op jit(solution)/shard_map/pallas_call | solution.py:56
  105.7 2.7 %collective-permute-start.7 = (bf16[256,512]{1,0:T(8,128)(2,1)}, bf16[256,512]{1,0:T(8,128)(2,1)S(1)}, u32[]{:S(2)}, u32[]{:S(2)}) collective-permute-start(bf16[256,512]{1,0:T(8,128)(2,1)} %get-tuple-element.56), channel_id=1, source_target_pairs={{0,3},{1,0},{2,1},{3,2},{4,7},{5,4},{6,5},{7,6},{8,11},{9,8},{10,9... | collective-permute-start | bytes 786440 | tf_op jit(solution)/shard_map/ppermute | solution.py:392
  108.4 1.4 collective-permute-start.9
  109.9 3.6 %collective-permute-done.6.refs_1_ = bf16[256,512]{1,0:T(8,128)(2,1)S(1)} collective-permute-done((bf16[256,512]{1,0:T(8,128)(2,1)}, bf16[256,512]{1,0:T(8,128)(2,1)S(1)}, u32[]{:S(2)}, u32[]{:S(2)}) %collective-permute-start.6) | collective-permute-done | bytes 262176 | tf_op jit(solution)/shard_map/ppermute | solution.py:392
  114.3 2.6 %shard_map.175 = (bf16[256,512]{1,0:T(8,128)(2,1)}, bf16[256,512]{1,0:T(8,128)(2,1)}) custom-call(s32[4]{0:T(128)S(1)} %copy-done.13, bf16[256,512]{1,0:T(8,128)(2,1)} %get-tuple-element.53.refs_0_, bf16[256,512]{1,0:T(8,128)(2,1)} %copy-done.19, bf16[256,512]{1,0:T(8,128)(2,1)} %get-tuple-element.55.refs_2_, bf16[256,512]{1,0:T(8,128)(2,1)} %copy-done.20), custom_call_target="tpu_custom_call" | custom-call | tf_op jit(solution)/shard_map/pallas_call | solution.py:56
  116.9 2.3 %collective-permute-start.11 = (bf16[256,512]{1,0:T(8,128)(2,1)}, bf16[256,512]{1,0:T(8,128)(2,1)S(1)}, u32[]{:S(2)}, u32[]{:S(2)}) collective-permute-start(bf16[256,512]{1,0:T(8,128)(2,1)} %get-tuple-element.60), channel_id=1, source_target_pairs={{0,3},{1,0},{2,1},{3,2},{4,7},{5,4},{6,5},{7,6},{8,11},{9,8},{10,9... | collective-permute-start | bytes 786440 | tf_op jit(solution)/shard_map/ppermute | solution.py:392
  119.2 4.1 %collective-permute-done.11.refs_4_ = bf16[256,512]{1,0:T(8,128)(2,1)S(1)} collective-permute-done((bf16[256,512]{1,0:T(8,128)(2,1)}, bf16[256,512]{1,0:T(8,128)(2,1)S(1)}, u32[]{:S(2)}, u32[]{:S(2)}) %collective-permute-start.11) | collective-permute-done | bytes 262176 | tf_op jit(solution)/shard_map/ppermute | solution.py:392
  123.3 2.5 %collective-permute-done.8.refs_1_ = bf16[256,512]{1,0:T(8,128)(2,1)S(1)} collective-permute-done((bf16[256,512]{1,0:T(8,128)(2,1)}, bf16[256,512]{1,0:T(8,128)(2,1)S(1)}, u32[]{:S(2)}, u32[]{:S(2)}) %collective-permute-start.8) | collective-permute-done | bytes 262176 | tf_op jit(solution)/shard_map/ppermute | solution.py:392
  126.5 2.9 %shard_map.176 = bf16[512,512]{1,0:T(8,128)(2,1)} custom-call(s32[4]{0:T(128)S(1)} %copy-done.13, bf16[512,512]{1,0:T(8,128)(2,1)} %get-tuple-element.52.refs_0_, bf16[256,512]{1,0:T(8,128)(2,1)} %copy-done.18, bf16[256,512]{1,0:T(8,128)(2,1)} %copy-done.16, bf16[256,512]{1,0:T(8,128)(2,1)} %copy-done.15, bf16[256,512]{1,0:T(8,128)(2,1)} %copy-done.17), custom_call_target="tpu_custom_call" | custom-call | tf_op jit(solution)/shard_map/pallas_call | solution.py:56
  129.4 16.6 %all-to-all-start.1 = ((bf16[64,8,512]{2,1,0:T(8,128)(2,1)}), bf16[64,8,512]{2,1,0:T(8,128)(2,1)}, u32[]{:S(2)}, u32[]{:S(2)}) async-start(bf16[64,8,512]{2,1,0:T(8,128)(2,1)} %bitcast.14), calls=%async_computation.1 | async-start | bytes 1048576 | tf_op jit(solution)/shard_map/all_to_all | solution.py:388
  146.0 6.4 %shard_map.174 = (bf16[2048,256]{1,0:T(8,128)(2,1)}, bf16[2048,256]{1,0:T(8,128)(2,1)}, bf16[256,2048]{1,0:T(8,128)(2,1)}, f32[8,128]{1,0:T(8,128)S(1)}) custom-call(s32[4]{0:T(128)S(1)} %copy-done.13, bf16[512,512]{1,0:T(8,128)(2,1)} %get-tuple-element.82.refs_0_, bf16[512,512]{1,0:T(8,128)(2,1)} %collective-permute-done.refs_1_, ...), custom_call_target="tpu_custom_call" | custom-call | tf_op jit(solution)/shard_map/pallas_call | solution.py:56
  152.4 11.2 %all-to-all-done.1 = bf16[64,8,512]{2,1,0:T(8,128)(2,1)} async-done(((bf16[64,8,512]{2,1,0:T(8,128)(2,1)}), bf16[64,8,512]{2,1,0:T(8,128)(2,1)}, u32[]{:S(2)}, u32[]{:S(2)}) %all-to-all-start.1) | async-done | bytes 524320 | tf_op jit(solution)/shard_map/all_to_all | solution.py:388
  163.6 2.0 shard_map.180.refs_0_
  166.0 1.2 collective-permute-start.14
  167.1 3.2 %collective-permute-done.12.refs_1_ = bf16[128,512]{1,0:T(8,128)(2,1)S(1)} collective-permute-done((bf16[128,512]{1,0:T(8,128)(2,1)S(1)}, bf16[128,512]{1,0:T(8,128)(2,1)S(1)}, u32[]{:S(2)}, u32[]{:S(2)}) %collective-permute-start.12) | collective-permute-done | bytes 131104 | tf_op jit(solution)/shard_map/ppermute | solution.py:392
  170.3 1.6 collective-permute-done.13.refs_2_
  171.9 3.6 %collective-permute-done.14.refs_3_ = bf16[128,512]{1,0:T(8,128)(2,1)S(1)} collective-permute-done((bf16[128,512]{1,0:T(8,128)(2,1)S(1)}, bf16[128,512]{1,0:T(8,128)(2,1)S(1)}, u32[]{:S(2)}, u32[]{:S(2)}) %collective-permute-start.14) | collective-permute-done | bytes 131104 | tf_op jit(solution)/shard_map/ppermute | solution.py:392
  175.5 3.4 %shard_map.181 = (f32[128,512]{1,0:T(8,128)}, bf16[8,320,128]{2,1,0:T(8,128)(2,1)}) custom-call(s32[4]{0:T(128)S(1)} %copy-done.13, bf16[128,512]{1,0:T(8,128)(2,1)S(1)} %shard_map.180.refs_0_, bf16[128,512]{1,0:T(8,128)(2,1)S(1)} %collective-permute-done.12.refs_1_, bf16[128,512]{1,0:T(8,128)(2,1)S(1)} %collective-permute-done.13.refs_2_, ...), custom_call_target="tpu_custom_call" | custom-call | tf_op jit(solution)/shard_map/pallas_call | solution.py:56
  178.8 3.9 %all-to-all-start.5 = ((bf16[8,320,128]{2,1,0:T(8,128)(2,1)}), bf16[8,320,128]{2,1,0:T(8,128)(2,1)S(1)}, u32[]{:S(2)}, u32[]{:S(2)}) async-start(bf16[8,320,128]{2,1,0:T(8,128)(2,1)} %get-tuple-element.68), calls=%async_computation.5 | async-start | bytes 1310720 | tf_op jit(solution)/shard_map/all_to_all | solution.py:388
  182.8 1.2 copy-done.5
  184.0 0.9 copy-done.12
  184.9 2.4 %shard_map.182 = (bf16[128,2,128]{2,1,0:T(2,128)(2,1)}, f32[128,768]{1,0:T(8,128)S(1)}) custom-call(s32[4]{0:T(128)S(1)} %copy-done.13, f32[128,512]{1,0:T(8,128)S(1)} %copy-done.12, bf16[2,128,256]{2,1,0:T(8,128)(2,1)S(1)} %bitcast.49, f32[128,1920]{1,0:T(8,128)S(1)} %copy-done.5, bf16[512,128]{1,0:T(8,128)(2,1)S(1)} %bitcast.52), custom_call_target="tpu_custom_call" | custom-call | tf_op jit(solution)/shard_map/pallas_call | solution.py:56
  187.3 6.2 %all-to-all-done.5.refs_0_ = bf16[8,320,128]{2,1,0:T(8,128)(2,1)S(1)} async-done(((bf16[8,320,128]{2,1,0:T(8,128)(2,1)}), bf16[8,320,128]{2,1,0:T(8,128)(2,1)S(1)}, u32[]{:S(2)}, u32[]{:S(2)}) %all-to-all-start.5) | async-done | bytes 655392 | tf_op jit(solution)/shard_map/all_to_all | solution.py:388
  193.6 0.8 copy-done.14
  194.4 1.2 shard_map.183
  195.6 16.8 %all_to_all.40.refs_0_ = bf16[8,192,128]{2,1,0:T(8,128)(2,1)S(1)} all-to-all(bf16[8,192,128]{2,1,0:T(8,128)(2,1)S(1)} %get-tuple-element.72), channel_id=1, replica_groups=mesh['sp_0'=8,'sp_1'=4,'sp_2'=2,'tp'=4] {'sp_0'}, dimensions={0} | all-to-all | bytes 786432 | tf_op jit(solution)/shard_map/all_to_all | solution.py:388
  212.4 1.3 shard_map.184
  213.6 9.8 %all_to_all.41 = bf16[8,64,128]{2,1,0:T(8,128)(2,1)S(1)} all-to-all(bf16[8,64,128]{2,1,0:T(8,128)(2,1)S(1)} %get-tuple-element.75), channel_id=1, replica_groups=mesh['sp_0'=8,'sp_1'=4,'sp_2'=2,'tp'=4] {'sp_1','sp_2'}, dimensions={0} | all-to-all | bytes 262144 | tf_op jit(solution)/shard_map/all_to_all | solution.py:388
  223.5 2.1 shard_map.185
  (73 shorter events, 6.8 us)
Async XLA Ops:
  0.6 18.9 %copy-start.21 = (bf16[128,2,256]{2,1,0:T(2,128)(2,1)S(1)}, bf16[128,2,256]{2,1,0:T(2,128)(2,1)}, u32[]{:S(2)}) copy-start(bf16[128,2,256]{2,1,0:T(2,128)(2,1)} %param.18) | copy-start | bytes 393220
  0.6 20.5 %copy-start.23 = (bf16[128,2,128]{2,1,0:T(2,128)(2,1)S(1)}, bf16[128,2,128]{2,1,0:T(2,128)(2,1)}, u32[]{:S(2)}) copy-start(bf16[128,2,128]{2,1,0:T(2,128)(2,1)} %param.16) | copy-start | bytes 196612
  0.7 20.5 %copy-start.22 = (bf16[128,2,128]{2,1,0:T(2,128)(2,1)S(1)}, bf16[128,2,128]{2,1,0:T(2,128)(2,1)}, u32[]{:S(2)}) copy-start(bf16[128,2,128]{2,1,0:T(2,128)(2,1)} %param.17) | copy-start | bytes 196612
  4.5 41.3 %all-to-all-start = ((bf16[64,16,512]{2,1,0:T(8,128)(2,1)}), bf16[64,16,512]{2,1,0:T(8,128)(2,1)S(1)}, u32[]{:S(2)}, u32[]{:S(2)}) async-start(bf16[64,16,512]{2,1,0:T(8,128)(2,1)} %get-tuple-element.43), calls=%async_computation | async-start | bytes 2097152 | tf_op jit(solution)/shard_map/all_to_all | solution.py:388
  17.6 47.5 %copy-start.13 = (s32[4]{0:T(128)S(1)}, s32[4]{0:T(128)}, u32[]{:S(2)}) copy-start(s32[4]{0:T(128)} %pad_add_fusion.q_ref) | copy-start | bytes 52
  25.9 57.1 %copy-start.4 = (f32[128,1920]{1,0:T(8,128)S(1)}, f32[128,1920]{1,0:T(8,128)}, u32[]{:S(2)}) copy-start(f32[128,1920]{1,0:T(8,128)} %get-tuple-element.65.refs_1_.refs_2_) | copy-start | bytes 2949124
  45.8 19.4 %all-to-all-start.2 = ((bf16[64,16,128]{2,1,0:T(8,128)(2,1)}), bf16[64,16,128]{2,1,0:T(8,128)(2,1)S(1)}, u32[]{:S(2)}, u32[]{:S(2)}) async-start(bf16[64,16,128]{2,1,0:T(8,128)(2,1)} %get-tuple-element.63), calls=%async_computation.2 | async-start | bytes 524288 | tf_op jit(solution)/shard_map/all_to_all | solution.py:388
  53.1 35.9 %copy-start = (bf16[1,2048,256]{2,1,0:T(8,128)(2,1)S(1)}, bf16[1,2048,256]{2,1,0:T(8,128)(2,1)}, u32[]{:S(2)}) copy-start(bf16[1,2048,256]{2,1,0:T(8,128)(2,1)} %param.21) | copy-start | bytes 3145732
  53.1 35.9 %copy-start.1 = (bf16[1,2048,256]{2,1,0:T(8,128)(2,1)S(1)}, bf16[1,2048,256]{2,1,0:T(8,128)(2,1)}, u32[]{:S(2)}) copy-start(bf16[1,2048,256]{2,1,0:T(8,128)(2,1)} %param.22) | copy-start | bytes 3145732
  53.1 21.3 %collective-permute-start.1 = (bf16[512,512]{1,0:T(8,128)(2,1)}, bf16[512,512]{1,0:T(8,128)(2,1)}, u32[]{:S(2)}, u32[]{:S(2)}) collective-permute-start(bf16[512,512]{1,0:T(8,128)(2,1)} %get-tuple-element.82.refs_0_), channel_id=1, source_target_pairs={{0,1},{1,2},{2,3},{3,0},{4,5},{5,6},{6,7},{7,4},{8,9},{9,10},{10,1... | collective-permute-start | bytes 1572872 | tf_op jit(solution)/shard_map/ppermute | solution.py:392
  54.4 20.3 %collective-permute-start.3 = (bf16[512,512]{1,0:T(8,128)(2,1)}, bf16[512,512]{1,0:T(8,128)(2,1)}, u32[]{:S(2)}, u32[]{:S(2)}) collective-permute-start(bf16[512,512]{1,0:T(8,128)(2,1)} %get-tuple-element.81.refs_0_.refs_4_), channel_id=1, source_target_pairs={{0,3},{1,0},{2,1},{3,2},{4,7},{5,4},{6,5},{7,6},{8,11},{9,8},{10,9... | collective-permute-start | bytes 1572872 | tf_op jit(solution)/shard_map/ppermute | solution.py:392
  67.1 15.9 %all-to-all-start.3 = ((bf16[64,8,128]{2,1,0:T(8,128)(2,1)}), bf16[64,8,128]{2,1,0:T(8,128)(2,1)S(1)}, u32[]{:S(2)}, u32[]{:S(2)}) async-start(bf16[64,8,128]{2,1,0:T(8,128)(2,1)} %get-tuple-element.64), calls=%async_computation.3 | async-start | bytes 262144 | tf_op jit(solution)/shard_map/all_to_all | solution.py:388
  71.9 17.1 %collective-permute-start = (bf16[512,512]{1,0:T(8,128)(2,1)}, bf16[512,512]{1,0:T(8,128)(2,1)}, u32[]{:S(2)}, u32[]{:S(2)}) collective-permute-start(bf16[512,512]{1,0:T(8,128)(2,1)} %get-tuple-element.82.refs_0_), channel_id=1, source_target_pairs={{0,3},{1,0},{2,1},{3,2},{4,7},{5,4},{6,5},{7,6},{8,11},{9,8},{10,9... | collective-permute-start | bytes 1572872 | tf_op jit(solution)/shard_map/ppermute | solution.py:392
  74.5 14.6 %collective-permute-start.2 = (bf16[512,512]{1,0:T(8,128)(2,1)}, bf16[512,512]{1,0:T(8,128)(2,1)}, u32[]{:S(2)}, u32[]{:S(2)}) collective-permute-start(bf16[512,512]{1,0:T(8,128)(2,1)} %collective-permute-done.1.refs_3_), channel_id=1, source_target_pairs={{0,1},{1,2},{2,3},{3,0},{4,5},{5,6},{6,7},{7,4},{8,9},{9,10},{10,1... | collective-permute-start | bytes 1572872 | tf_op jit(solution)/shard_map/ppermute | solution.py:392
  74.5 25.5 %collective-permute-start.5 = (bf16[512,512]{1,0:T(8,128)(2,1)}, bf16[512,512]{1,0:T(8,128)(2,1)}, u32[]{:S(2)}, u32[]{:S(2)}) collective-permute-start(bf16[512,512]{1,0:T(8,128)(2,1)} %get-tuple-element.81.refs_0_.refs_4_), channel_id=1, source_target_pairs={{0,1},{1,2},{2,3},{3,0},{4,5},{5,6},{6,7},{7,4},{8,9},{9,10},{10,1... | collective-permute-start | bytes 1572872 | tf_op jit(solution)/shard_map/ppermute | solution.py:392
  74.7 25.3 %collective-permute-start.4 = (bf16[512,512]{1,0:T(8,128)(2,1)}, bf16[512,512]{1,0:T(8,128)(2,1)}, u32[]{:S(2)}, u32[]{:S(2)}) collective-permute-start(bf16[512,512]{1,0:T(8,128)(2,1)} %collective-permute-done.3.refs_1_.refs_5_), channel_id=1, source_target_pairs={{0,3},{1,0},{2,1},{3,2},{4,7},{5,4},{6,5},{7,6},{8,11},{9,8},{10,9... | collective-permute-start | bytes 1572872 | tf_op jit(solution)/shard_map/ppermute | solution.py:392
  85.2 44.2 %all-to-all-start.4 = ((bf16[8,128,512]{2,1,0:T(8,128)(2,1)}), bf16[8,128,512]{2,1,0:T(8,128)(2,1)S(1)}, u32[]{:S(2)}, u32[]{:S(2)}) async-start(bf16[8,128,512]{2,1,0:T(8,128)(2,1)} %get-tuple-element.66), calls=%async_computation.4 | async-start | bytes 2097152 | tf_op jit(solution)/shard_map/all_to_all | solution.py:388
  89.1 10.9 %copy-start.3 = (bf16[1,256,2048]{2,1,0:T(8,128)(2,1)S(1)}, bf16[1,256,2048]{2,1,0:T(8,128)(2,1)}, u32[]{:S(2)}) copy-start(bf16[1,256,2048]{2,1,0:T(8,128)(2,1)} %param.23) | copy-start | bytes 3145732
  92.6 0.7 copy-start.8
  105.7 7.7 %collective-permute-start.6 = (bf16[256,512]{1,0:T(8,128)(2,1)}, bf16[256,512]{1,0:T(8,128)(2,1)S(1)}, u32[]{:S(2)}, u32[]{:S(2)}) collective-permute-start(bf16[256,512]{1,0:T(8,128)(2,1)} %get-tuple-element.54), channel_id=1, source_target_pairs={{0,1},{1,2},{2,3},{3,0},{4,5},{5,6},{6,7},{7,4},{8,9},{9,10},{10,1... | collective-permute-start | bytes 786440 | tf_op jit(solution)/shard_map/ppermute | solution.py:392
  105.7 7.7 %collective-permute-start.7 = (bf16[256,512]{1,0:T(8,128)(2,1)}, bf16[256,512]{1,0:T(8,128)(2,1)S(1)}, u32[]{:S(2)}, u32[]{:S(2)}) collective-permute-start(bf16[256,512]{1,0:T(8,128)(2,1)} %get-tuple-element.56), channel_id=1, source_target_pairs={{0,3},{1,0},{2,1},{3,2},{4,7},{5,4},{6,5},{7,6},{8,11},{9,8},{10,9... | collective-permute-start | bytes 786440 | tf_op jit(solution)/shard_map/ppermute | solution.py:392
  108.4 10.7 %collective-permute-start.10 = (bf16[256,512]{1,0:T(8,128)(2,1)}, bf16[256,512]{1,0:T(8,128)(2,1)S(1)}, u32[]{:S(2)}, u32[]{:S(2)}) collective-permute-start(bf16[256,512]{1,0:T(8,128)(2,1)} %get-tuple-element.59), channel_id=1, source_target_pairs={{0,3},{1,0},{2,1},{3,2},{4,7},{5,4},{6,5},{7,6},{8,11},{9,8},{10,9... | collective-permute-start | bytes 786440 | tf_op jit(solution)/shard_map/ppermute | solution.py:392
  108.4 10.7 %collective-permute-start.9 = (bf16[256,512]{1,0:T(8,128)(2,1)}, bf16[256,512]{1,0:T(8,128)(2,1)S(1)}, u32[]{:S(2)}, u32[]{:S(2)}) collective-permute-start(bf16[256,512]{1,0:T(8,128)(2,1)} %get-tuple-element.58), channel_id=1, source_target_pairs={{0,1},{1,2},{2,3},{3,0},{4,5},{5,6},{6,7},{7,4},{8,9},{9,10},{10,1... | collective-permute-start | bytes 786440 | tf_op jit(solution)/shard_map/ppermute | solution.py:392
  113.4 0.7 copy-start.19
  113.4 0.8 copy-start.20
  114.3 31.7 %copy-start.9 = (bf16[512,256]{1,0:T(8,128)(2,1)S(1)}, bf16[512,256]{1,0:T(8,128)(2,1)}, u32[]{:S(2)}) copy-start(bf16[512,256]{1,0:T(8,128)(2,1)} %copy-done.8) | copy-start | bytes 786436
  114.3 31.7 %copy-start.10 = (bf16[512,256]{1,0:T(8,128)(2,1)S(1)}, bf16[512,256]{1,0:T(8,128)(2,1)}, u32[]{:S(2)}) copy-start(bf16[512,256]{1,0:T(8,128)(2,1)} %get-tuple-element.46.refs_8_) | copy-start | bytes 786436
  114.3 31.8 %copy-start.11 = (bf16[512,256]{1,0:T(8,128)(2,1)S(1)}, bf16[512,256]{1,0:T(8,128)(2,1)}, u32[]{:S(2)}) copy-start(bf16[512,256]{1,0:T(8,128)(2,1)} %get-tuple-element.47.refs_9_) | copy-start | bytes 786436
  116.9 6.4 %collective-permute-start.11 = (bf16[256,512]{1,0:T(8,128)(2,1)}, bf16[256,512]{1,0:T(8,128)(2,1)S(1)}, u32[]{:S(2)}, u32[]{:S(2)}) collective-permute-start(bf16[256,512]{1,0:T(8,128)(2,1)} %get-tuple-element.60), channel_id=1, source_target_pairs={{0,3},{1,0},{2,1},{3,2},{4,7},{5,4},{6,5},{7,6},{8,11},{9,8},{10,9... | collective-permute-start | bytes 786440 | tf_op jit(solution)/shard_map/ppermute | solution.py:392
  119.1 6.6 %collective-permute-start.8 = (bf16[256,512]{1,0:T(8,128)(2,1)}, bf16[256,512]{1,0:T(8,128)(2,1)S(1)}, u32[]{:S(2)}, u32[]{:S(2)}) collective-permute-start(bf16[256,512]{1,0:T(8,128)(2,1)} %get-tuple-element.57), channel_id=1, source_target_pairs={{0,1},{1,2},{2,3},{3,0},{4,5},{5,6},{6,7},{7,4},{8,9},{9,10},{10,1... | collective-permute-start | bytes 786440 | tf_op jit(solution)/shard_map/ppermute | solution.py:392
  119.1 6.6 %copy-start.15 = (bf16[256,512]{1,0:T(8,128)(2,1)}, bf16[256,512]{1,0:T(8,128)(2,1)S(1)}, u32[]{:S(2)}) copy-start(bf16[256,512]{1,0:T(8,128)(2,1)S(1)} %collective-permute-done.10.refs_3_) | copy-start | bytes 786436
  119.2 6.6 %copy-start.16 = (bf16[256,512]{1,0:T(8,128)(2,1)}, bf16[256,512]{1,0:T(8,128)(2,1)S(1)}, u32[]{:S(2)}) copy-start(bf16[256,512]{1,0:T(8,128)(2,1)S(1)} %collective-permute-done.9.refs_2_) | copy-start | bytes 786436
  123.3 2.5 %copy-start.17 = (bf16[256,512]{1,0:T(8,128)(2,1)}, bf16[256,512]{1,0:T(8,128)(2,1)S(1)}, u32[]{:S(2)}) copy-start(bf16[256,512]{1,0:T(8,128)(2,1)S(1)} %collective-permute-done.11.refs_4_) | copy-start | bytes 786436
  125.8 0.7 copy-start.18
  129.4 34.2 %all-to-all-start.1 = ((bf16[64,8,512]{2,1,0:T(8,128)(2,1)}), bf16[64,8,512]{2,1,0:T(8,128)(2,1)}, u32[]{:S(2)}, u32[]{:S(2)}) async-start(bf16[64,8,512]{2,1,0:T(8,128)(2,1)} %bitcast.14), calls=%async_computation.1 | async-start | bytes 1048576 | tf_op jit(solution)/shard_map/all_to_all | solution.py:388
  152.4 23.1 %copy-start.2 = (bf16[2048,512]{1,0:T(8,128)(2,1)S(1)}, bf16[2048,512]{1,0:T(8,128)(2,1)}, u32[]{:S(2)}) copy-start(bf16[2048,512]{1,0:T(8,128)(2,1)} %refs_7_.1) | copy-start | bytes 6291460
  165.6 4.7 %collective-permute-start.12 = (bf16[128,512]{1,0:T(8,128)(2,1)S(1)}, bf16[128,512]{1,0:T(8,128)(2,1)S(1)}, u32[]{:S(2)}, u32[]{:S(2)}) collective-permute-start(bf16[128,512]{1,0:T(8,128)(2,1)S(1)} %shard_map.180.refs_0_), channel_id=1, source_target_pairs={{0,3},{1,0},{2,1},{3,2},{4,7},{5,4},{6,5},{7,6},{8,11},{9,8},{10,9... | collective-permute-start | bytes 393224 | tf_op jit(solution)/shard_map/ppermute | solution.py:392
  165.7 6.3 %collective-permute-start.13 = (bf16[128,512]{1,0:T(8,128)(2,1)S(1)}, bf16[128,512]{1,0:T(8,128)(2,1)S(1)}, u32[]{:S(2)}, u32[]{:S(2)}) collective-permute-start(bf16[128,512]{1,0:T(8,128)(2,1)S(1)} %shard_map.180.refs_0_), channel_id=1, source_target_pairs={{0,2},{1,3},{2,0},{3,1},{4,6},{5,7},{6,4},{7,5},{8,10},{9,11},{10,... | collective-permute-start | bytes 393224 | tf_op jit(solution)/shard_map/ppermute | solution.py:392
  166.0 9.5 %collective-permute-start.14 = (bf16[128,512]{1,0:T(8,128)(2,1)S(1)}, bf16[128,512]{1,0:T(8,128)(2,1)S(1)}, u32[]{:S(2)}, u32[]{:S(2)}) collective-permute-start(bf16[128,512]{1,0:T(8,128)(2,1)S(1)} %shard_map.180.refs_0_), channel_id=1, source_target_pairs={{0,1},{1,2},{2,3},{3,0},{4,5},{5,6},{6,7},{7,4},{8,9},{9,10},{10,1... | collective-permute-start | bytes 393224 | tf_op jit(solution)/shard_map/ppermute | solution.py:392
  175.5 7.3 %copy-start.7 = (bf16[128,2,256]{2,0,1:T(8,128)(2,1)S(1)}, bf16[128,2,256]{2,0,1:T(8,128)(2,1)}, u32[]{:S(2)}) copy-start(bf16[128,2,256]{2,0,1:T(8,128)(2,1)} %copy.28) | copy-start | bytes 393220
  178.8 14.7 %all-to-all-start.5 = ((bf16[8,320,128]{2,1,0:T(8,128)(2,1)}), bf16[8,320,128]{2,1,0:T(8,128)(2,1)S(1)}, u32[]{:S(2)}, u32[]{:S(2)}) async-start(bf16[8,320,128]{2,1,0:T(8,128)(2,1)} %get-tuple-element.68), calls=%async_computation.5 | async-start | bytes 1310720 | tf_op jit(solution)/shard_map/all_to_all | solution.py:388
  182.8 1.2 copy-start.5
  184.0 0.9 copy-start.12
  187.3 36.1 %copy-start.6 = (f32[128,1920]{1,0:T(8,128)S(1)}, f32[128,1920]{1,0:T(8,128)}, u32[]{:S(2)}) copy-start(f32[128,1920]{1,0:T(8,128)} %get-tuple-element.65.refs_1_.refs_2_) | copy-start | bytes 2949124
  193.6 0.8 copy-start.14

commit v4 on v3

--- a/solution.py
+++ b/solution.py
@@ -113,33 +113,29 @@
     resid[...] = ((og[...].astype(F32) + back[0:n]) + back[n : 2 * n]).astype(BF)
 
 
-def gate_up_body(q, r0, r1, r2, r3, g0, g1, g2, g3, u0, u1, u2, u3, act, ga, ua):
-    rows = (r0, r1, r2, r3)
-    gate = mm(r0[...], g0[...])
-    up = mm(r0[...], u0[...])
-    for r, g, u in zip(rows[1:], (g1, g2, g3), (u1, u2, u3)):
-        x = r[...]
-        gate = gate + mm(x, g[...])
-        up = up + mm(x, u[...])
+def early_body(q, r0, r1, r3, x0, x1, x3, g0, g1, g3, u0, u1, u3, d0, d1, d3, gate, up, act_grad):
+    a, b, c = r0[...], r1[...], r3[...]
+    gate[...] = mm(a, g0[...]) + mm(b, g1[...]) + mm(c, g3[...])
+    up[...] = mm(a, u0[...]) + mm(b, u1[...]) + mm(c, u3[...])
+    act_grad[...] = mm(x0[...], d0[...], NT) + mm(x1[...], d1[...], NT) + mm(x3[...], d3[...], NT)
+
+
+def expert_back_body(
+    q, r2, x2, d2, g0, g1, g2, g3, u0, u1, u2, u3, gate_part, up_part, act_part,
+    act, gp, up, far_lo, far_hi, right_lo, right_hi, left_lo, left_hi, mine,
+):
+    x = r2[...]
+    gate = gate_part[...] + mm(x, g2[...])
+    upv = up_part[...] + mm(x, u2[...])
+    act_grad = act_part[...] + mm(x2[...], d2[...], NT)
     gc = jnp.minimum(gate, CLAMP_LIMIT)
-    uc = jnp.clip(up, -CLAMP_LIMIT, CLAMP_LIMIT)
+    uc = jnp.clip(upv, -CLAMP_LIMIT, CLAMP_LIMIT)
     sig = 1.0 / (1.0 + jnp.exp(-GATE_SLOPE * gc))
     gs = gc * sig
     act[...] = (gs * (uc + 1.0)).astype(BF)
     slope = sig + GATE_SLOPE * gs * (1.0 - sig)
-    ga[...] = jnp.where(gate < CLAMP_LIMIT, (uc + 1.0) * slope, 0.0)
-    ua[...] = jnp.where(jnp.abs(up) < CLAMP_LIMIT, gs, 0.0)
-
-
-def expert_back_body(
-    q, x0, x1, x2, x3, d0, d1, d2, d3, g0, g1, g2, g3, u0, u1, u2, u3, ga, ua,
-    gp, up, far_lo, far_hi, right_lo, right_hi, left_lo, left_hi, mine,
-):
-    act_grad = mm(x0[...], d0[...], NT)
-    for x, d in zip((x1, x2, x3), (d1, d2, d3)):
-        act_grad = act_grad + mm(x[...], d[...], NT)
-    gpg = (act_grad * ga[...]).astype(BF)
-    upg = (act_grad * ua[...]).astype(BF)
+    gpg = jnp.where(gate < CLAMP_LIMIT, act_grad * (uc + 1.0) * slope, 0.0).astype(BF)
+    upg = jnp.where(jnp.abs(upv) < CLAMP_LIMIT, act_grad * gs, 0.0).astype(BF)
     gp[...] = gpg
     up[...] = upg
 
@@ -153,6 +149,18 @@
     mine[...] = back(g0, u0)
 
 
+def weight_grads_body(q, r0, r1, r2, r3, x0, x1, x2, x3, gp, up, act, gw, uw, dw):
+    step = pl.program_id(0)
+    for k, (r, x) in enumerate(zip((r0, r1, r2, r3), (x0, x1, x2, x3))):
+
+        @pl.when(step == k)
+        def _(r=r, x=x):
+            rt = r[...]
+            gw[...] = mm(rt, gp[...], TN).astype(BF)
+            uw[...] = mm(rt, up[...], TN).astype(BF)
+            dw[...] = mm(act[...], x[...], TN).astype(BF)
+
+
 def pass_on_body(q, right_lo, far_lo, left_hi, far_hi, right, left):
     right[...] = (right_lo[...].astype(F32) + far_lo[...].astype(F32)).astype(BF)
     left[...] = (left_hi[...].astype(F32) + far_hi[...].astype(F32)).astype(BF)
@@ -165,8 +173,7 @@
     out[half:, :] = (m[half:] + (a_hi[...].astype(F32) + b_hi[...].astype(F32))).astype(BF)
 
 
-def weight_grads_body(q, r0, r1, r2, r3, x0, x1, x2, x3, gp, up, act, gw, uw, dw, token):
-    token[...] = jnp.zeros(token.shape, F32)
+def weight_grads_body(q, r0, r1, r2, r3, x0, x1, x2, x3, gp, up, act, gw, uw, dw):
     step = pl.program_id(0)
     for k, (r, x) in enumerate(zip((r0, r1, r2, r3), (x0, x1, x2, x3))):
 
@@ -282,8 +289,7 @@
         iv = lax.rsqrt(jnp.mean(ret * ret, axis=1, keepdims=True) + EPSILON)
         nm = ret * iv
         back[:, sl] = nm
-        for k in range(nbf.shape[0]):
-            nbf[k, :, sl] = nm.astype(BF)
+        nbf[:, sl] = nm.astype(BF)
         invs = jnp.where(lane == h, iv, invs)
         back[:, QDT + h * 128 : QDT + (h + 1) * 128] = (qh * grow).T
     back[:, INV : INV + 128] = invs
@@ -332,7 +338,7 @@
     qg[...] = jnp.stack(parts, axis=1).astype(BF)
 
 
-def plane_body(q, x, nb, table, inside, send):
+def plane_body(q, x, n0, n1, n2, n3, m0, m1, m2, m3, table, inside, send):
     blocks = x.shape[0]
     parts = [x[k, 0:64, :].astype(F32) for k in range(blocks)]
     for k in range(blocks):
@@ -344,9 +350,12 @@
     for m in range(blocks):
         total = total + table[8:9, m : m + 1] * parts[m]
     total = total.astype(BF)
-    proj = mm(x[0, 64:320, :], nb[0])
-    for k in range(1, blocks):
-        proj = proj + mm(x[k, 64:320, :], nb[k])
+    proj = 0.0
+    y, core = q[2] // 2, q[2] % 2
+    for k, nb in enumerate((n0, n1, n2, n3)):
+        proj = proj + mm(x[lax.rem(y + k, 4) * 2 + core, 64:320, :], nb[...])
+    for k, nb in enumerate((m0, m1, m2, m3)):
+        proj = proj + mm(x[lax.rem(y + k, 4) * 2 + 1 - core, 64:320, :], nb[...])
     for k in range(blocks):
         send[k, 0:64, :] = total
         for u in range(4):
@@ -465,32 +474,35 @@
     state_sent, table = call(prefix_body, q, (got,), [((64, 8, 128), BF), ((16, 128), F32)])
     state = a2a(state_sent, SP).reshape(slots, 128)
     nbf, back = call(
-        normed_body, q, (state, pack), [((8, n, heads * vd), BF), ((n, 896), F32)],
+        normed_body, q, (state, pack), [((n, heads * vd), BF), ((n, 896), F32)],
         hbm_out=(0, 1),
     )
-    nball = a2a(nbf, YC)
+    along = [nbf] + [lax.ppermute(nbf, "sp_1", [(i, (i + by) % 4) for i in range(4)]) for by in (3, 2, 1)]
+    nball = along + [lax.ppermute(a, "sp_2", [(0, 1), (1, 0)]) for a in along]
 
     wrow = (quarter, hidden)
     gspec = {k: block_rows(k, wrow) for k in range(4)}
     dspec = {k: block_cols(k, (hidden, quarter)) for k in range(4)}
-    act, ga, ua = call(
-        gate_up_body,
+    near = (0, 1, 3)
+    parts = call(
+        early_body,
         q,
-        (*rows4, *[gate_w] * 4, *[up_w] * 4),
-        [((slots, hidden), BF), ((slots, hidden), F32), ((slots, hidden), F32)],
-        in_specs={4 + k: s for k, s in gspec.items()} | {8 + k: s for k, s in gspec.items()},
+        (*[rows4[k] for k in near], *[grads4[k] for k in near], *[gate_w] * 3, *[up_w] * 3, *[down_w] * 3),
+        [((slots, hidden), F32)] * 3,
+        in_specs={6 + i: gspec[k] for i, k in enumerate(near)}
+        | {9 + i: gspec[k] for i, k in enumerate(near)}
+        | {12 + i: dspec[k] for i, k in enumerate(near)},
+        mib=20,
     )
     half = slots // 2
-    gp, up, far_lo, far_hi, right_lo, right_hi, left_lo, left_hi, mine = call(
+    act, gp, up, far_lo, far_hi, right_lo, right_hi, left_lo, left_hi, mine = call(
         expert_back_body,
         q,
-        (*grads4, *[down_w] * 4, *[gate_w] * 4, *[up_w] * 4, ga, ua),
-        [((slots, hidden), BF)] * 2 + [((half, quarter), BF)] * 6 + [((slots, quarter), BF)],
-        in_specs={4 + k: s for k, s in dspec.items()}
-        | {8 + k: s for k, s in gspec.items()}
-        | {12 + k: s for k, s in gspec.items()},
+        (rows4[2], grads4[2], down_w, *[gate_w] * 4, *[up_w] * 4, *parts),
+        [((slots, hidden), BF)] * 3 + [((half, quarter), BF)] * 6 + [((slots, quarter), BF)],
+        in_specs={2: dspec[2]} | {3 + k: s for k, s in gspec.items()} | {7 + k: s for k, s in gspec.items()},
         mib=24,
-        hbm_out=range(9),
+        hbm_out=range(10),
     )
     far_lo, far_hi = shift(far_lo, 1), shift(far_hi, 3)
     right_hi, left_lo = shift(right_hi, 1), shift(left_lo, 3)
@@ -499,11 +511,11 @@
         hbm_in=range(4), hbm_out=range(2),
     )
     right_lo, left_hi = shift(right_lo, 1), shift(left_hi, 3)
-    gate_grad, up_grad, down_grad, weights_done = call(
+    gate_grad, up_grad, down_grad = call(
         weight_grads_body,
         q,
         (*rows4, *grads4, gp, up, act),
-        [((width, hidden), BF), ((width, hidden), BF), ((hidden, width), BF), ((8, 128), F32)],
+        [((width, hidden), BF), ((width, hidden), BF), ((hidden, width), BF)],
         out_specs={
             0: pl.BlockSpec(wrow, lambda i, q: (lax.rem(q[0] + i, 4), 0)),
             1: pl.BlockSpec(wrow, lambda i, q: (lax.rem(q[0] + i, 4), 0)),
@@ -517,15 +529,7 @@
         hbm_in=range(5),
     )
     share = a2a(share.reshape(64, 8, quarter), SP).reshape(slots, quarter)
-    (resid,) = call(
-        combine_body,
-        q,
-        (share, qt, out_grad),
-        [((n, quarter), BF)],
-        in_specs={2: own},
-        after=(weights_done, nball),
-        hbm_in=(1, 2),
-    )
+    (resid,) = call(combine_body, q, (share, qt, out_grad), [((n, quarter), BF)], in_specs={2: own}, hbm_in=(1, 2))
     resid4 = around(resid)
 
     pspec = {4 + k: block_rows(k, (quarter, out_proj.shape[1])) for k in range(4)}
@@ -540,7 +544,9 @@
     )
     inner = a2a(inner, YC)
     qg, rest = call(local_grads_body, q, (rg, vv, pack, state), [((n, heads, kd), BF), ((n, 768), F32)])
-    inside, later = call(plane_body, q, (inner, nball, table), [((8, 64, 128), F32), ((8, 192, 128), BF)], after=(qg,))
+    inside, later = call(
+        plane_body, q, (inner, *nball, table), [((8, 64, 128), F32), ((8, 192, 128), BF)], hbm_in=range(1, 9)
+    )
     later = a2a(later, ZAX)
     future, proj_grad = call(planes_body, q, (later, inside, table), [((8, 64, 128), BF), ((32, heads * vd), F32)])
     future = a2a(future, YC).reshape(slots, 128)

time: 226 us -> 240 us (1.062)
  blocking collectives: 26.6 us -> 61.7 us
  waiting for transfers between devices: 77.7 us -> 64.2 us
  starting transfers between devices: 64.4 us -> 59.2 us
    all_to_all x2, blocking collectives: 26.6 us -> 61.7 us  [a2a(): return lax.all_to_all(x, axes, split_axis=0, concat_axis=0, tiled=True)]
    all_to_all x6 -> x5, waiting for transfers between devices: 52.5 us -> 23.2 us  [a2a(): return lax.all_to_all(x, axes, split_axis=0, concat_axis=0, tiled=True)]
    all_to_all x6 -> x5, starting transfers between devices: 48.6 us -> 35.1 us  [a2a(): return lax.all_to_all(x, axes, split_axis=0, concat_axis=0, tiled=True)]
    ppermute x0 -> x7, waiting for transfers between devices: none -> 9.24 us  [the longest x3 8.29 us: per_device(): lax.ppermute(nbf, 'sp_1', [(i, (i + by) % 4) for i in range(4)])]
    ppermute x0 -> x7, starting transfers between devices: none -> 8.79 us  [the longest x4 5.04 us: per_device(): nball = along + [lax.ppermute(a, 'sp_2', [(0, 1), (1, 0)]) for a in along]]
    ppermute x15, waiting for transfers between devices: 25.2 us -> 31.8 us  [shift(): return lax.ppermute(x, TP, [(i, (i + by) % 4) for i in range(4)])]
    unnamed x49 -> x59, local copies, waits for them, and re-layouts: 5.96 us -> 3.67 us
  transfers between devices with their start and end apart: 21 -> 27, of which waited for: 12 -> 13; matrix products, arithmetic and copies ran while one was open for 2% -> 2% of each run, Pallas kernels for 14% -> 11%
where the time goes in v4:
time: 240 us; the launch traced here: 239 us
  waiting for transfers between devices  64.2 us (27%)
  blocking collectives  61.7 us (26%)
  starting transfers between devices  59.2 us (25%)
  Pallas kernels  44.1 us (18%)
  local copies, waits for them, and re-layouts  7.16 us (3%)
    all_to_all x2, blocking collectives, a2a(): return lax.all_to_all(x, axes, split_axis=0, concat_axis=0, tiled=True)  61.7 us
    pallas_call x15, Pallas kernels, call(): pl.pallas_call(kernel, out_shape=[(pltpu.HBM if i in hbm_out else jax.Sha...  44.1 us
    all_to_all x5, starting transfers between devices, a2a(): return lax.all_to_all(x, axes, split_axis=0, concat_axis=0, tiled=True)  35.1 us
    ppermute x15, waiting for transfers between devices, shift(): return lax.ppermute(x, TP, [(i, (i + by) % 4) for i in range(4)])  31.8 us
    all_to_all x5, waiting for transfers between devices, a2a(): return lax.all_to_all(x, axes, split_axis=0, concat_axis=0, tiled=True)  23.2 us
    ppermute x15, starting transfers between devices, shift(): return lax.ppermute(x, TP, [(i, (i + by) % 4) for i in range(4)])  15.3 us
    ppermute x3, waiting for transfers between devices, per_device(): lax.ppermute(nbf, 'sp_1', [(i, (i + by) % 4) for i in range(4)])  8.29 us
    ppermute x4, starting transfers between devices, per_device(): nball = along + [lax.ppermute(a, 'sp_2', [(0, 1), (1, 0)]) for a in along]  5.04 us
  transfers between devices with their start and end apart: 27, of which 13 were waited for; matrix products, arithmetic and copies ran while one was open for 2% of the time, Pallas kernels for 11%

profile of v4, /device:TPU:1, one launch (start us, length us, event | category | flops | bytes accessed | tf_op | source)
XLA Modules:
  0.0 239.1 jit_solution(11484565372731935509)
XLA Ops:
  1.3 3.2 %shard_map.171 = (bf16[64,16,512]{2,1,0:T(8,128)(2,1)}, bf16[256,512]{1,0:T(8,128)(2,1)}) custom-call(s32[4]{0:T(128)} %pad_add_fusion.q_ref, s32[2,128]{1,0:T(2,128)} %bitcast.54, f32[2,128]{1,0:T(2,128)} %bitcast.55, bf16[128,2048]{1,0:T(8,128)(2,1)} %refs_2_.2, bf16[128,2048]{1,0:T(8,128)(2,1)} %refs_2_.3), custom_call_target="tpu_custom_call" | custom-call | tf_op jit(solution)/shard_map/pallas_call | solution.py:56
  4.5 41.6 %all_to_all.35 = bf16[64,16,512]{2,1,0:T(8,128)(2,1)S(1)} all-to-all(bf16[64,16,512]{2,1,0:T(8,128)(2,1)} %get-tuple-element.43), channel_id=1, replica_groups=mesh['sp_0'=8,'sp_1'=4,'sp_2'=2,'tp'=4] {'sp_0','sp_1','sp_2'}, dimensions={0} | all-to-all | bytes 2097152 | tf_op jit(solution)/shard_map/all_to_all | solution.py:397
  46.1 1.1 slice_bitcast_fusion
  47.2 1.2 collective-permute-start.1
  48.4 1.5 collective-permute-start.3
  49.9 1.3 collective-permute-start
  51.4 9.7 %collective-permute-done.1.refs_2_.refs_3_ = bf16[512,512]{1,0:T(8,128)(2,1)} collective-permute-done((bf16[512,512]{1,0:T(8,128)(2,1)}, bf16[512,512]{1,0:T(8,128)(2,1)}, u32[]{:S(2)}, u32[]{:S(2)}) %collective-permute-start.1) | collective-permute-done | bytes 524320 | tf_op jit(solution)/shard_map/ppermute | solution.py:401
  61.1 2.7 %collective-permute-start.4 = (bf16[512,512]{1,0:T(8,128)(2,1)}, bf16[512,512]{1,0:T(8,128)(2,1)}, u32[]{:S(2)}, u32[]{:S(2)}) collective-permute-start(bf16[512,512]{1,0:T(8,128)(2,1)} %collective-permute-done.3.refs_4_.refs_5_), channel_id=1, source_target_pairs={{0,3},{1,0},{2,1},{3,2},{4,7},{5,4},{6,5},{7,6},{8,11},{9,8},{10,9... | collective-permute-start | bytes 1572872 | tf_op jit(solution)/shard_map/ppermute | solution.py:401
  64.1 0.9 fusion
  65.7 6.4 %collective-permute-done.refs_1_ = bf16[512,512]{1,0:T(8,128)(2,1)} collective-permute-done((bf16[512,512]{1,0:T(8,128)(2,1)}, bf16[512,512]{1,0:T(8,128)(2,1)}, u32[]{:S(2)}, u32[]{:S(2)}) %collective-permute-start) | collective-permute-done | bytes 524320 | tf_op jit(solution)/shard_map/ppermute | solution.py:401
  72.3 3.8 %shard_map.172 = (f32[512,256]{1,0:T(8,128)S(1)}, f32[512,256]{1,0:T(8,128)S(1)}, f32[512,256]{1,0:T(8,128)S(1)}) custom-call(s32[4]{0:T(128)S(1)} %copy-done.11, bf16[512,512]{1,0:T(8,128)(2,1)} %get-tuple-element.82.refs_0_, bf16[512,512]{1,0:T(8,128)(2,1)} %collective-permute-done.refs_1_, bf16[512,512]{1,0:T(8,128)(2,1)} %collective-permute-done.1.refs_2_.refs_3_, ...), custom_call_target="tpu_custom_call" | custom-call | tf_op jit(solution)/shard_map/pallas_call | solution.py:56
  76.1 7.4 %collective-permute-done.2.refs_0_.refs_2_ = bf16[512,512]{1,0:T(8,128)(2,1)} collective-permute-done((bf16[512,512]{1,0:T(8,128)(2,1)}, bf16[512,512]{1,0:T(8,128)(2,1)}, u32[]{:S(2)}, u32[]{:S(2)}) %collective-permute-start.2) | collective-permute-done | bytes 524320 | tf_op jit(solution)/shard_map/ppermute | solution.py:401
  83.5 4.6 %shard_map.173 = (bf16[512,256]{1,0:T(8,128)(2,1)}, bf16[512,256]{1,0:T(8,128)(2,1)}, bf16[512,256]{1,0:T(8,128)(2,1)}, bf16[256,512]{1,0:T(8,128)(2,1)}, bf16[2...) custom-call(s32[4]{0:T(128)S(1)} %copy-done.11, ...), custom_call_target="tpu_custom_call" | custom-call | tf_op jit(solution)/shard_map/pallas_call | solution.py:56
  88.1 0.9 collective-permute-start.6
  89.0 1.8 collective-permute-start.7
  93.0 4.0 %shard_map.178 = (bf16[64,16,128]{2,1,0:T(8,128)(2,1)}, f32[128,1920]{1,0:T(8,128)}) custom-call(s32[4]{0:T(128)} %pad_add_fusion.q_ref, bf16[2,128,128]{2,1,0:T(8,128)(2,1)} %get-tuple-element.86.refs_0_, bf16[2,128,128]{2,1,0:T(8,128)(2,1)} %get-tuple-element.85.refs_1_, bf16[2,128,256]{2,1,0:T(8,128)(2,1)} %bitcast.47, f32[2,128]{1,0:T(2,128)} %bitcast.53, ...), custom_call_target="tpu_custom_call" | custom-call | tf_op jit(solution)/shard_map/pallas_call | solution.py:56
  97.0 8.0 %all-to-all-start.2 = ((bf16[64,16,128]{2,1,0:T(8,128)(2,1)}), bf16[64,16,128]{2,1,0:T(8,128)(2,1)S(1)}, u32[]{:S(2)}, u32[]{:S(2)}) async-start(bf16[64,16,128]{2,1,0:T(8,128)(2,1)} %get-tuple-element.63), calls=%async_computation.2 | async-start | bytes 524288 | tf_op jit(solution)/shard_map/all_to_all | solution.py:397
  105.0 1.5 collective-permute-start.10
  107.4 2.6 %shard_map.175 = (bf16[256,512]{1,0:T(8,128)(2,1)}, bf16[256,512]{1,0:T(8,128)(2,1)}) custom-call(s32[4]{0:T(128)S(1)} %copy-done.12, bf16[256,512]{1,0:T(8,128)(2,1)} %get-tuple-element.54.refs_0_, bf16[256,512]{1,0:T(8,128)(2,1)} %copy-done.17, bf16[256,512]{1,0:T(8,128)(2,1)} %get-tuple-element.56.refs_2_, bf16[256,512]{1,0:T(8,128)(2,1)} %copy-done.18), custom_call_target="tpu_custom_call" | custom-call | tf_op jit(solution)/shard_map/pallas_call | solution.py:56
  109.9 2.7 %collective-permute-start.11 = (bf16[256,512]{1,0:T(8,128)(2,1)}, bf16[256,512]{1,0:T(8,128)(2,1)S(1)}, u32[]{:S(2)}, u32[]{:S(2)}) collective-permute-start(bf16[256,512]{1,0:T(8,128)(2,1)} %get-tuple-element.61), channel_id=1, source_target_pairs={{0,3},{1,0},{2,1},{3,2},{4,7},{5,4},{6,5},{7,6},{8,11},{9,8},{10,9... | collective-permute-start | bytes 786440 | tf_op jit(solution)/shard_map/ppermute | solution.py:401
  112.7 2.4 collective-permute-done.9.refs_2_
  115.1 3.4 %collective-permute-done.11.refs_4_ = bf16[256,512]{1,0:T(8,128)(2,1)S(1)} collective-permute-done((bf16[256,512]{1,0:T(8,128)(2,1)}, bf16[256,512]{1,0:T(8,128)(2,1)S(1)}, u32[]{:S(2)}, u32[]{:S(2)}) %collective-permute-start.11) | collective-permute-done | bytes 262176 | tf_op jit(solution)/shard_map/ppermute | solution.py:401
  118.5 2.1 collective-permute-done.8.refs_1_
  121.3 2.1 shard_map.176
  124.2 12.4 %all-to-all-start.1 = ((bf16[64,8,512]{2,1,0:T(8,128)(2,1)}), bf16[64,8,512]{2,1,0:T(8,128)(2,1)}, u32[]{:S(2)}, u32[]{:S(2)}) async-start(bf16[64,8,512]{2,1,0:T(8,128)(2,1)} %bitcast.46), calls=%async_computation.1 | async-start | bytes 1048576 | tf_op jit(solution)/shard_map/all_to_all | solution.py:397
  136.6 2.0 shard_map.179
  138.6 15.6 %all-to-all-done.1 = bf16[64,8,512]{2,1,0:T(8,128)(2,1)} async-done(((bf16[64,8,512]{2,1,0:T(8,128)(2,1)}), bf16[64,8,512]{2,1,0:T(8,128)(2,1)}, u32[]{:S(2)}, u32[]{:S(2)}) %all-to-all-start.1) | async-done | bytes 524320 | tf_op jit(solution)/shard_map/all_to_all | solution.py:397
  154.2 5.7 %all-to-all-start.3 = ((bf16[64,8,128]{2,1,0:T(8,128)(2,1)}), bf16[64,8,128]{2,1,0:T(8,128)(2,1)S(1)}, u32[]{:S(2)}, u32[]{:S(2)}) async-start(bf16[64,8,128]{2,1,0:T(8,128)(2,1)} %get-tuple-element.64), calls=%async_computation.3 | async-start | bytes 262144 | tf_op jit(solution)/shard_map/all_to_all | solution.py:397
  159.9 2.0 shard_map.177.refs_0_
  162.5 0.9 collective-permute-start.14
  163.4 7.6 %all-to-all-done.3 = bf16[64,8,128]{2,1,0:T(8,128)(2,1)S(1)} async-done(((bf16[64,8,128]{2,1,0:T(8,128)(2,1)}), bf16[64,8,128]{2,1,0:T(8,128)(2,1)S(1)}, u32[]{:S(2)}, u32[]{:S(2)}) %all-to-all-start.3) | async-done | bytes 131104 | tf_op jit(solution)/shard_map/all_to_all | solution.py:397
  171.0 1.8 shard_map.180
  172.8 3.5 %shard_map.181 = (f32[128,512]{1,0:T(8,128)}, bf16[8,320,128]{2,1,0:T(8,128)(2,1)}) custom-call(s32[4]{0:T(128)S(1)} %copy-done.12, bf16[128,512]{1,0:T(8,128)(2,1)S(1)} %shard_map.177.refs_0_, bf16[128,512]{1,0:T(8,128)(2,1)S(1)} %collective-permute-done.12.refs_1_, bf16[128,512]{1,0:T(8,128)(2,1)} %collective-permute-done.13.refs_2_, ...), custom_call_target="tpu_custom_call" | custom-call | tf_op jit(solution)/shard_map/pallas_call | solution.py:56
  176.3 4.2 %all-to-all-start.4 = ((bf16[8,320,128]{2,1,0:T(8,128)(2,1)}), bf16[8,320,128]{2,1,0:T(8,128)(2,1)S(1)}, u32[]{:S(2)}, u32[]{:S(2)}) async-start(bf16[8,320,128]{2,1,0:T(8,128)(2,1)} %get-tuple-element.67), calls=%async_computation.4 | async-start | bytes 1310720 | tf_op jit(solution)/shard_map/all_to_all | solution.py:397
  180.5 2.6 %collective-permute-start.15 = (bf16[128,512]{1,0:T(8,128)(2,1)}, bf16[128,512]{1,0:T(8,128)(2,1)S(1)}, u32[]{:S(2)}, u32[]{:S(2)}) collective-permute-start(bf16[128,512]{1,0:T(8,128)(2,1)} %get-tuple-element.68.refs_1_), channel_id=1, source_target_pairs={{0,24},{8,0},{16,8},{24,16},{1,25},{9,1},{17,9},{25,17},{2,26},{10... | collective-permute-start | bytes 393224 | tf_op jit(solution)/shard_map/ppermute | solution.py:480
  184.3 1.2 collective-permute-start.18
  185.5 7.1 %collective-permute-done.15.refs_2_ = bf16[128,512]{1,0:T(8,128)(2,1)S(1)} collective-permute-done((bf16[128,512]{1,0:T(8,128)(2,1)}, bf16[128,512]{1,0:T(8,128)(2,1)S(1)}, u32[]{:S(2)}, u32[]{:S(2)}) %collective-permute-start.15) | collective-permute-done | bytes 131104 | tf_op jit(solution)/shard_map/ppermute | solution.py:480
  192.6 1.5 collective-permute-start.19
  194.2 1.5 collective-permute-start.20
  195.7 1.1 collective-permute-done.17.refs_4_
  197.6 0.9 collective-permute-done.21.refs_8_
  199.2 2.5 %shard_map.182 = (f32[8,64,128]{2,1,0:T(8,128)S(1)}, bf16[8,192,128]{2,1,0:T(8,128)(2,1)S(1)}) custom-call(s32[4]{0:T(128)S(1)} %copy-done.12, bf16[8,320,128]{2,1,0:T(8,128)(2,1)S(1)} %all-to-all-done.4.refs_0_, bf16[128,512]{1,0:T(8,128)(2,1)} %get-tuple-element.68.refs_1_, bf16[128,512]{1,0:T(8,128)(2,1)} %copy-done.19, bf16[128,512]{1,0:T(8,128)(2,1)} %copy-done.20, ...), custom_call_target="tpu_custom_call" | custom-call | tf_op jit(solution)/shard_map/pallas_call | solution.py:56
  201.8 20.1 %all_to_all.36.refs_0_ = bf16[8,192,128]{2,1,0:T(8,128)(2,1)S(1)} all-to-all(bf16[8,192,128]{2,1,0:T(8,128)(2,1)S(1)} %get-tuple-element.70), channel_id=1, replica_groups=mesh['sp_0'=8,'sp_1'=4,'sp_2'=2,'tp'=4] {'sp_0'}, dimensions={0} | all-to-all | bytes 786432 | tf_op jit(solution)/shard_map/all_to_all | solution.py:397
  221.9 1.3 shard_map.183
  223.2 4.9 %all-to-all-start.6 = ((bf16[8,64,128]{2,1,0:T(8,128)(2,1)}), bf16[8,64,128]{2,1,0:T(8,128)(2,1)S(1)}, u32[]{:S(2)}, u32[]{:S(2)}) async-start(bf16[8,64,128]{2,1,0:T(8,128)(2,1)} %get-tuple-element.75), calls=%async_computation.6 | async-start | bytes 262144 | tf_op jit(solution)/shard_map/all_to_all | solution.py:397
  228.2 6.4 %shard_map.174 = (bf16[2048,256]{1,0:T(8,128)(2,1)}, bf16[2048,256]{1,0:T(8,128)(2,1)}, bf16[256,2048]{1,0:T(8,128)(2,1)}) custom-call(s32[4]{0:T(128)S(1)} %copy-done.12, bf16[512,512]{1,0:T(8,128)(2,1)} %get-tuple-element.82.refs_0_, bf16[512,512]{1,0:T(8,128)(2,1)} %collective-permute-done.refs_1_, ...), custom_call_target="tpu_custom_call" | custom-call | tf_op jit(solution)/shard_map/pallas_call | solution.py:56
  234.6 2.4 shard_map.184
  237.0 2.1 shard_map.185
  (95 shorter events, 10.1 us)
Async XLA Ops:
  4.5 60.5 %copy-start.27 = (bf16[128,2,128]{2,1,0:T(2,128)(2,1)S(1)}, bf16[128,2,128]{2,1,0:T(2,128)(2,1)}, u32[]{:S(2)}) copy-start(bf16[128,2,128]{2,1,0:T(2,128)(2,1)} %param.17) | copy-start | bytes 196612
  4.5 60.5 %copy-start.28 = (bf16[128,2,128]{2,1,0:T(2,128)(2,1)S(1)}, bf16[128,2,128]{2,1,0:T(2,128)(2,1)}, u32[]{:S(2)}) copy-start(bf16[128,2,128]{2,1,0:T(2,128)(2,1)} %param.16) | copy-start | bytes 196612
  4.5 67.8 %copy-start = (bf16[1,2048,256]{2,1,0:T(8,128)(2,1)S(1)}, bf16[1,2048,256]{2,1,0:T(8,128)(2,1)}, u32[]{:S(2)}) copy-start(bf16[1,2048,256]{2,1,0:T(8,128)(2,1)} %param.21) | copy-start | bytes 3145732
  4.5 67.8 %copy-start.1 = (bf16[1,2048,256]{2,1,0:T(8,128)(2,1)S(1)}, bf16[1,2048,256]{2,1,0:T(8,128)(2,1)}, u32[]{:S(2)}) copy-start(bf16[1,2048,256]{2,1,0:T(8,128)(2,1)} %param.22) | copy-start | bytes 3145732
  4.5 67.8 %copy-start.3 = (bf16[1,256,2048]{2,1,0:T(8,128)(2,1)S(1)}, bf16[1,256,2048]{2,1,0:T(8,128)(2,1)}, u32[]{:S(2)}) copy-start(bf16[1,256,2048]{2,1,0:T(8,128)(2,1)} %param.23) | copy-start | bytes 3145732
  4.5 67.8 %copy-start.11 = (s32[4]{0:T(128)S(1)}, s32[4]{0:T(128)}, u32[]{:S(2)}) copy-start(s32[4]{0:T(128)} %pad_add_fusion.q_ref) | copy-start | bytes 52
  47.2 13.9 %collective-permute-start.1 = (bf16[512,512]{1,0:T(8,128)(2,1)}, bf16[512,512]{1,0:T(8,128)(2,1)}, u32[]{:S(2)}, u32[]{:S(2)}) collective-permute-start(bf16[512,512]{1,0:T(8,128)(2,1)} %get-tuple-element.82.refs_0_), channel_id=1, source_target_pairs={{0,1},{1,2},{2,3},{3,0},{4,5},{5,6},{6,7},{7,4},{8,9},{9,10},{10,1... | collective-permute-start | bytes 1572872 | tf_op jit(solution)/shard_map/ppermute | solution.py:401
  48.4 12.7 %collective-permute-start.3 = (bf16[512,512]{1,0:T(8,128)(2,1)}, bf16[512,512]{1,0:T(8,128)(2,1)}, u32[]{:S(2)}, u32[]{:S(2)}) collective-permute-start(bf16[512,512]{1,0:T(8,128)(2,1)} %get-tuple-element.81.refs_3_.refs_4_), channel_id=1, source_target_pairs={{0,3},{1,0},{2,1},{3,2},{4,7},{5,4},{6,5},{7,6},{8,11},{9,8},{10,9... | collective-permute-start | bytes 1572872 | tf_op jit(solution)/shard_map/ppermute | solution.py:401
  49.9 22.1 %collective-permute-start = (bf16[512,512]{1,0:T(8,128)(2,1)}, bf16[512,512]{1,0:T(8,128)(2,1)}, u32[]{:S(2)}, u32[]{:S(2)}) collective-permute-start(bf16[512,512]{1,0:T(8,128)(2,1)} %get-tuple-element.82.refs_0_), channel_id=1, source_target_pairs={{0,3},{1,0},{2,1},{3,2},{4,7},{5,4},{6,5},{7,6},{8,11},{9,8},{10,9... | collective-permute-start | bytes 1572872 | tf_op jit(solution)/shard_map/ppermute | solution.py:401
  51.2 21.1 %collective-permute-start.5 = (bf16[512,512]{1,0:T(8,128)(2,1)}, bf16[512,512]{1,0:T(8,128)(2,1)}, u32[]{:S(2)}, u32[]{:S(2)}) collective-permute-start(bf16[512,512]{1,0:T(8,128)(2,1)} %get-tuple-element.81.refs_3_.refs_4_), channel_id=1, source_target_pairs={{0,1},{1,2},{2,3},{3,0},{4,5},{5,6},{6,7},{7,4},{8,9},{9,10},{10,1... | collective-permute-start | bytes 1572872 | tf_op jit(solution)/shard_map/ppermute | solution.py:401
  61.1 22.5 %collective-permute-start.2 = (bf16[512,512]{1,0:T(8,128)(2,1)}, bf16[512,512]{1,0:T(8,128)(2,1)}, u32[]{:S(2)}, u32[]{:S(2)}) collective-permute-start(bf16[512,512]{1,0:T(8,128)(2,1)} %collective-permute-done.1.refs_2_.refs_3_), channel_id=1, source_target_pairs={{0,1},{1,2},{2,3},{3,0},{4,5},{5,6},{6,7},{7,4},{8,9},{9,10},{10,1... | collective-permute-start | bytes 1572872 | tf_op jit(solution)/shard_map/ppermute | solution.py:401
  61.1 22.5 %collective-permute-start.4 = (bf16[512,512]{1,0:T(8,128)(2,1)}, bf16[512,512]{1,0:T(8,128)(2,1)}, u32[]{:S(2)}, u32[]{:S(2)}) collective-permute-start(bf16[512,512]{1,0:T(8,128)(2,1)} %collective-permute-done.3.refs_4_.refs_5_), channel_id=1, source_target_pairs={{0,3},{1,0},{2,1},{3,2},{4,7},{5,4},{6,5},{7,6},{8,11},{9,8},{10,9... | collective-permute-start | bytes 1572872 | tf_op jit(solution)/shard_map/ppermute | solution.py:401
  83.5 8.8 %copy-start.26 = (bf16[128,2,256]{2,1,0:T(2,128)(2,1)S(1)}, bf16[128,2,256]{2,1,0:T(2,128)(2,1)}, u32[]{:S(2)}) copy-start(bf16[128,2,256]{2,1,0:T(2,128)(2,1)} %param.18) | copy-start | bytes 393220
  83.5 23.8 %copy-start.12 = (s32[4]{0:T(128)S(1)}, s32[4]{0:T(128)}, u32[]{:S(2)}) copy-start(s32[4]{0:T(128)} %pad_add_fusion.q_ref) | copy-start | bytes 52
  88.1 18.4 %collective-permute-start.6 = (bf16[256,512]{1,0:T(8,128)(2,1)}, bf16[256,512]{1,0:T(8,128)(2,1)S(1)}, u32[]{:S(2)}, u32[]{:S(2)}) collective-permute-start(bf16[256,512]{1,0:T(8,128)(2,1)} %get-tuple-element.55), channel_id=1, source_target_pairs={{0,1},{1,2},{2,3},{3,0},{4,5},{5,6},{6,7},{7,4},{8,9},{9,10},{10,1... | collective-permute-start | bytes 786440 | tf_op jit(solution)/shard_map/ppermute | solution.py:401
  89.0 17.5 %collective-permute-start.7 = (bf16[256,512]{1,0:T(8,128)(2,1)}, bf16[256,512]{1,0:T(8,128)(2,1)S(1)}, u32[]{:S(2)}, u32[]{:S(2)}) collective-permute-start(bf16[256,512]{1,0:T(8,128)(2,1)} %get-tuple-element.57), channel_id=1, source_target_pairs={{0,3},{1,0},{2,1},{3,2},{4,7},{5,4},{6,5},{7,6},{8,11},{9,8},{10,9... | collective-permute-start | bytes 786440 | tf_op jit(solution)/shard_map/ppermute | solution.py:401
  97.0 27.2 %all-to-all-start.2 = ((bf16[64,16,128]{2,1,0:T(8,128)(2,1)}), bf16[64,16,128]{2,1,0:T(8,128)(2,1)S(1)}, u32[]{:S(2)}, u32[]{:S(2)}) async-start(bf16[64,16,128]{2,1,0:T(8,128)(2,1)} %get-tuple-element.63), calls=%async_computation.2 | async-start | bytes 524288 | tf_op jit(solution)/shard_map/all_to_all | solution.py:397
  105.0 7.7 %collective-permute-start.10 = (bf16[256,512]{1,0:T(8,128)(2,1)}, bf16[256,512]{1,0:T(8,128)(2,1)S(1)}, u32[]{:S(2)}, u32[]{:S(2)}) collective-permute-start(bf16[256,512]{1,0:T(8,128)(2,1)} %get-tuple-element.60), channel_id=1, source_target_pairs={{0,3},{1,0},{2,1},{3,2},{4,7},{5,4},{6,5},{7,6},{8,11},{9,8},{10,9... | collective-permute-start | bytes 786440 | tf_op jit(solution)/shard_map/ppermute | solution.py:401
  106.5 8.6 %collective-permute-start.9 = (bf16[256,512]{1,0:T(8,128)(2,1)}, bf16[256,512]{1,0:T(8,128)(2,1)S(1)}, u32[]{:S(2)}, u32[]{:S(2)}) collective-permute-start(bf16[256,512]{1,0:T(8,128)(2,1)} %get-tuple-element.59), channel_id=1, source_target_pairs={{0,1},{1,2},{2,3},{3,0},{4,5},{5,6},{6,7},{7,4},{8,9},{9,10},{10,1... | collective-permute-start | bytes 786440 | tf_op jit(solution)/shard_map/ppermute | solution.py:401
  109.9 8.5 %collective-permute-start.11 = (bf16[256,512]{1,0:T(8,128)(2,1)}, bf16[256,512]{1,0:T(8,128)(2,1)S(1)}, u32[]{:S(2)}, u32[]{:S(2)}) collective-permute-start(bf16[256,512]{1,0:T(8,128)(2,1)} %get-tuple-element.61), channel_id=1, source_target_pairs={{0,3},{1,0},{2,1},{3,2},{4,7},{5,4},{6,5},{7,6},{8,11},{9,8},{10,9... | collective-permute-start | bytes 786440 | tf_op jit(solution)/shard_map/ppermute | solution.py:401
  112.6 8.0 %collective-permute-start.8 = (bf16[256,512]{1,0:T(8,128)(2,1)}, bf16[256,512]{1,0:T(8,128)(2,1)S(1)}, u32[]{:S(2)}, u32[]{:S(2)}) collective-permute-start(bf16[256,512]{1,0:T(8,128)(2,1)} %get-tuple-element.58), channel_id=1, source_target_pairs={{0,1},{1,2},{2,3},{3,0},{4,5},{5,6},{6,7},{7,4},{8,9},{9,10},{10,1... | collective-permute-start | bytes 786440 | tf_op jit(solution)/shard_map/ppermute | solution.py:401
  112.7 7.9 %copy-start.13 = (bf16[256,512]{1,0:T(8,128)(2,1)}, bf16[256,512]{1,0:T(8,128)(2,1)S(1)}, u32[]{:S(2)}) copy-start(bf16[256,512]{1,0:T(8,128)(2,1)S(1)} %collective-permute-done.10.refs_3_) | copy-start | bytes 786436
  115.1 5.5 %copy-start.14 = (bf16[256,512]{1,0:T(8,128)(2,1)}, bf16[256,512]{1,0:T(8,128)(2,1)S(1)}, u32[]{:S(2)}) copy-start(bf16[256,512]{1,0:T(8,128)(2,1)S(1)} %collective-permute-done.9.refs_2_) | copy-start | bytes 786436
  118.5 2.1 copy-start.15
  121.3 49.7 %copy-start.4 = (f32[128,1920]{1,0:T(8,128)S(1)}, f32[128,1920]{1,0:T(8,128)}, u32[]{:S(2)}) copy-start(f32[128,1920]{1,0:T(8,128)} %get-tuple-element.65.refs_1_.refs_2_) | copy-start | bytes 2949124
  124.2 48.6 %copy-start.2 = (bf16[2048,512]{1,0:T(8,128)(2,1)S(1)}, bf16[2048,512]{1,0:T(8,128)(2,1)}, u32[]{:S(2)}) copy-start(bf16[2048,512]{1,0:T(8,128)(2,1)} %refs_7_.1) | copy-start | bytes 6291460
  124.2 30.0 %all-to-all-start.1 = ((bf16[64,8,512]{2,1,0:T(8,128)(2,1)}), bf16[64,8,512]{2,1,0:T(8,128)(2,1)}, u32[]{:S(2)}, u32[]{:S(2)}) async-start(bf16[64,8,512]{2,1,0:T(8,128)(2,1)} %bitcast.46), calls=%async_computation.1 | async-start | bytes 1048576 | tf_op jit(solution)/shard_map/all_to_all | solution.py:397
  154.2 16.8 %all-to-all-start.3 = ((bf16[64,8,128]{2,1,0:T(8,128)(2,1)}), bf16[64,8,128]{2,1,0:T(8,128)(2,1)S(1)}, u32[]{:S(2)}, u32[]{:S(2)}) async-start(bf16[64,8,128]{2,1,0:T(8,128)(2,1)} %get-tuple-element.64), calls=%async_computation.3 | async-start | bytes 262144 | tf_op jit(solution)/shard_map/all_to_all | solution.py:397
  161.9 10.9 %collective-permute-start.12 = (bf16[128,512]{1,0:T(8,128)(2,1)S(1)}, bf16[128,512]{1,0:T(8,128)(2,1)S(1)}, u32[]{:S(2)}, u32[]{:S(2)}) collective-permute-start(bf16[128,512]{1,0:T(8,128)(2,1)S(1)} %shard_map.177.refs_0_), channel_id=1, source_target_pairs={{0,3},{1,0},{2,1},{3,2},{4,7},{5,4},{6,5},{7,6},{8,11},{9,8},{10,9... | collective-permute-start | bytes 393224 | tf_op jit(solution)/shard_map/ppermute | solution.py:401
  162.0 10.8 %collective-permute-start.13 = (bf16[128,512]{1,0:T(8,128)(2,1)S(1)}, bf16[128,512]{1,0:T(8,128)(2,1)}, u32[]{:S(2)}, u32[]{:S(2)}) collective-permute-start(bf16[128,512]{1,0:T(8,128)(2,1)S(1)} %shard_map.177.refs_0_), channel_id=1, source_target_pairs={{0,2},{1,3},{2,0},{3,1},{4,6},{5,7},{6,4},{7,5},{8,10},{9,11},{10,... | collective-permute-start | bytes 393224 | tf_op jit(solution)/shard_map/ppermute | solution.py:401
  162.5 10.3 %collective-permute-start.14 = (bf16[128,512]{1,0:T(8,128)(2,1)S(1)}, bf16[128,512]{1,0:T(8,128)(2,1)}, u32[]{:S(2)}, u32[]{:S(2)}) collective-permute-start(bf16[128,512]{1,0:T(8,128)(2,1)S(1)} %shard_map.177.refs_0_), channel_id=1, source_target_pairs={{0,1},{1,2},{2,3},{3,0},{4,5},{5,6},{6,7},{7,4},{8,9},{9,10},{10,1... | collective-permute-start | bytes 393224 | tf_op jit(solution)/shard_map/ppermute | solution.py:401
  176.3 51.9 %copy-start.7 = (bf16[512,256]{1,0:T(8,128)(2,1)S(1)}, bf16[512,256]{1,0:T(8,128)(2,1)}, u32[]{:S(2)}) copy-start(bf16[512,256]{1,0:T(8,128)(2,1)} %get-tuple-element.49.refs_10_) | copy-start | bytes 786436
  176.3 51.9 %copy-start.8 = (bf16[512,256]{1,0:T(8,128)(2,1)S(1)}, bf16[512,256]{1,0:T(8,128)(2,1)}, u32[]{:S(2)}) copy-start(bf16[512,256]{1,0:T(8,128)(2,1)} %get-tuple-element.47.refs_8_) | copy-start | bytes 786436
  176.3 51.9 %copy-start.9 = (bf16[512,256]{1,0:T(8,128)(2,1)S(1)}, bf16[512,256]{1,0:T(8,128)(2,1)}, u32[]{:S(2)}) copy-start(bf16[512,256]{1,0:T(8,128)(2,1)} %get-tuple-element.48.refs_9_) | copy-start | bytes 786436
  176.3 22.3 %all-to-all-start.4 = ((bf16[8,320,128]{2,1,0:T(8,128)(2,1)}), bf16[8,320,128]{2,1,0:T(8,128)(2,1)S(1)}, u32[]{:S(2)}, u32[]{:S(2)}) async-start(bf16[8,320,128]{2,1,0:T(8,128)(2,1)} %get-tuple-element.67), calls=%async_computation.4 | async-start | bytes 1310720 | tf_op jit(solution)/shard_map/all_to_all | solution.py:397
  180.5 12.1 %collective-permute-start.15 = (bf16[128,512]{1,0:T(8,128)(2,1)}, bf16[128,512]{1,0:T(8,128)(2,1)S(1)}, u32[]{:S(2)}, u32[]{:S(2)}) collective-permute-start(bf16[128,512]{1,0:T(8,128)(2,1)} %get-tuple-element.68.refs_1_), channel_id=1, source_target_pairs={{0,24},{8,0},{16,8},{24,16},{1,25},{9,1},{17,9},{25,17},{2,26},{10... | collective-permute-start | bytes 393224 | tf_op jit(solution)/shard_map/ppermute | solution.py:480
  183.1 11.1 %collective-permute-start.16 = (bf16[128,512]{1,0:T(8,128)(2,1)}, bf16[128,512]{1,0:T(8,128)(2,1)S(1)}, u32[]{:S(2)}, u32[]{:S(2)}) collective-permute-start(bf16[128,512]{1,0:T(8,128)(2,1)} %get-tuple-element.68.refs_1_), channel_id=1, source_target_pairs={{0,16},{8,24},{16,0},{24,8},{1,17},{9,25},{17,1},{25,9},{2,18},{10... | collective-permute-start | bytes 393224 | tf_op jit(solution)/shard_map/ppermute | solution.py:480
  183.7 13.2 %collective-permute-start.17 = (bf16[128,512]{1,0:T(8,128)(2,1)}, bf16[128,512]{1,0:T(8,128)(2,1)S(1)}, u32[]{:S(2)}, u32[]{:S(2)}) collective-permute-start(bf16[128,512]{1,0:T(8,128)(2,1)} %get-tuple-element.68.refs_1_), channel_id=1, source_target_pairs={{0,8},{8,16},{16,24},{24,0},{1,9},{9,17},{17,25},{25,1},{2,10},{10... | collective-permute-start | bytes 393224 | tf_op jit(solution)/shard_map/ppermute | solution.py:480
  184.3 13.3 %collective-permute-start.18 = (bf16[128,512]{1,0:T(8,128)(2,1)}, bf16[128,512]{1,0:T(8,128)(2,1)S(1)}, u32[]{:S(2)}, u32[]{:S(2)}) collective-permute-start(bf16[128,512]{1,0:T(8,128)(2,1)} %get-tuple-element.68.refs_1_), channel_id=1, source_target_pairs={{0,4},{4,0},{1,5},{5,1},{2,6},{6,2},{3,7},{7,3},{8,12},{12,8},{9,1... | collective-permute-start | bytes 393224 | tf_op jit(solution)/shard_map/ppermute | solution.py:481
  192.6 6.0 %copy-start.19 = (bf16[128,512]{1,0:T(8,128)(2,1)}, bf16[128,512]{1,0:T(8,128)(2,1)S(1)}, u32[]{:S(2)}) copy-start(bf16[128,512]{1,0:T(8,128)(2,1)S(1)} %collective-permute-done.15.refs_2_) | copy-start | bytes 393220
  192.6 5.0 %collective-permute-start.19 = (bf16[128,512]{1,0:T(8,128)(2,1)S(1)}, bf16[128,512]{1,0:T(8,128)(2,1)S(1)}, u32[]{:S(2)}, u32[]{:S(2)}) collective-permute-start(bf16[128,512]{1,0:T(8,128)(2,1)S(1)} %collective-permute-done.15.refs_2_), channel_id=1, source_target_pairs={{0,4},{4,0},{1,5},{5,1},{2,6},{6,2},{3,7},{7,3},{8,12},{12,8},{9,1... | collective-permute-start | bytes 393224 | tf_op jit(solution)/shard_map/ppermute | solution.py:481
  194.2 4.4 %copy-start.20 = (bf16[128,512]{1,0:T(8,128)(2,1)}, bf16[128,512]{1,0:T(8,128)(2,1)S(1)}, u32[]{:S(2)}) copy-start(bf16[128,512]{1,0:T(8,128)(2,1)S(1)} %collective-permute-done.16.refs_3_) | copy-start | bytes 393220
  194.2 3.5 %collective-permute-start.20 = (bf16[128,512]{1,0:T(8,128)(2,1)S(1)}, bf16[128,512]{1,0:T(8,128)(2,1)S(1)}, u32[]{:S(2)}, u32[]{:S(2)}) collective-permute-start(bf16[128,512]{1,0:T(8,128)(2,1)S(1)} %collective-permute-done.16.refs_3_), channel_id=1, source_target_pairs={{0,4},{4,0},{1,5},{5,1},{2,6},{6,2},{3,7},{7,3},{8,12},{12,8},{9,1... | collective-permute-start | bytes 393224 | tf_op jit(solution)/shard_map/ppermute | solution.py:481
  196.8 1.8 copy-start.21
  196.8 1.8 collective-permute-start.21
  223.2 13.8 %all-to-all-start.6 = ((bf16[8,64,128]{2,1,0:T(8,128)(2,1)}), bf16[8,64,128]{2,1,0:T(8,128)(2,1)S(1)}, u32[]{:S(2)}, u32[]{:S(2)}) async-start(bf16[8,64,128]{2,1,0:T(8,128)(2,1)} %get-tuple-element.75), calls=%async_computation.6 | async-start | bytes 262144 | tf_op jit(solution)/shard_map/all_to_all | solution.py:397
  228.2 6.4 %copy-start.6 = (bf16[128,2,256]{2,0,1:T(8,128)(2,1)S(1)}, bf16[128,2,256]{2,0,1:T(8,128)(2,1)}, u32[]{:S(2)}) copy-start(bf16[128,2,256]{2,0,1:T(8,128)(2,1)} %copy.28) | copy-start | bytes 393220
  228.2 6.4 %copy-start.10 = (f32[128,512]{1,0:T(8,128)S(1)}, f32[128,512]{1,0:T(8,128)}, u32[]{:S(2)}) copy-start(f32[128,512]{1,0:T(8,128)} %get-tuple-element.73.refs_0_) | copy-start | bytes 786436
  (8 other events, 6.7 us)

commit v5 on v4

--- a/solution.py
+++ b/solution.py
@@ -89,10 +89,10 @@
     return d0, d1, col
 
 
-def dispatch_body(q, routes, rw, stream, og, send, qt):
+def dispatch_body(q, routes, rw, stream, og, send):
     n = routes.shape[1]
-    slots = qt.shape[1]
-    d0, d1, col = slots_of(routes)
+    slots = send.shape[0] * 8
+    d0, d1, _ = slots_of(routes)
     w = rw[...]
     di = iota((slots, n), 0).astype(F32)
     q0, q1 = di == d0, di == d1
@@ -102,6 +102,11 @@
     rows = mm(pick, stream[...]).reshape(64, 8, -1)
     grads = (mm(pick, og[...]) * weight).reshape(64, 8, -1)
     send[...] = jnp.concatenate([rows, grads], axis=1).astype(BF)
+
+
+def back_picks_body(q, routes, qt):
+    n, slots = routes.shape[1], qt.shape[1]
+    d0, d1, col = slots_of(routes)
     dl = iota((n, slots), 1).astype(F32)
     qt[0:n, :] = jnp.where(dl == col(d0), 1.0, 0.0).astype(BF)
     qt[n : 2 * n, :] = jnp.where(dl == col(d1), 1.0, 0.0).astype(BF)
@@ -120,10 +125,7 @@
     act_grad[...] = mm(x0[...], d0[...], NT) + mm(x1[...], d1[...], NT) + mm(x3[...], d3[...], NT)
 
 
-def expert_back_body(
-    q, r2, x2, d2, g0, g1, g2, g3, u0, u1, u2, u3, gate_part, up_part, act_part,
-    act, gp, up, far_lo, far_hi, right_lo, right_hi, left_lo, left_hi, mine,
-):
+def hidden_grads_body(q, r2, x2, d2, g2, u2, gate_part, up_part, act_part, act, gp, up, far_lo, far_hi):
     x = r2[...]
     gate = gate_part[...] + mm(x, g2[...])
     upv = up_part[...] + mm(x, u2[...])
@@ -138,12 +140,20 @@
     upg = jnp.where(jnp.abs(upv) < CLAMP_LIMIT, act_grad * gs, 0.0).astype(BF)
     gp[...] = gpg
     up[...] = upg
+    half = far_lo.shape[0]
+    part = (mm(gpg, g2[...], NT) + mm(upg, u2[...], NT)).astype(BF)
+    far_lo[...] = part[:half]
+    far_hi[...] = part[half:]
+
+
+def expert_back_body(q, gp, up, g0, g1, g3, u0, u1, u3, right_lo, right_hi, left_lo, left_hi, mine):
+    gpg, upg = gp[...], up[...]
 
     def back(g, u):
         return (mm(gpg, g[...], NT) + mm(upg, u[...], NT)).astype(BF)
 
-    half = far_lo.shape[0]
-    for lo, hi, part in ((far_lo, far_hi, back(g2, u2)), (right_lo, right_hi, back(g1, u1)), (left_lo, left_hi, back(g3, u3))):
+    half = right_lo.shape[0]
+    for lo, hi, part in ((right_lo, right_hi, back(g1, u1)), (left_lo, left_hi, back(g3, u3))):
         lo[...] = part[:half]
         hi[...] = part[half:]
     mine[...] = back(g0, u0)
@@ -439,11 +449,11 @@
     gate_w, up_w, down_w = gate_weight[0], up_weight[0], down_weight[0]
 
     own = pl.BlockSpec((n, quarter), lambda i, q: (0, q[0]))
-    sent, qt = call(
+    (sent,) = call(
         dispatch_body,
         q,
         (routes.T, route_weight.T, stream, out_grad),
-        [((64, 16, quarter), BF), ((2 * n, slots), BF)],
+        [((64, 16, quarter), BF)],
         in_specs={2: own, 3: own},
         mib=60,
     )
@@ -463,6 +473,7 @@
     qv = queries.transpose(1, 0, 2)
     kv = key_vectors.transpose(1, 0, 2)
     vv = value_vectors.transpose(1, 0, 2)
+    (qt,) = call(back_picks_body, q, (routes.T,), [((2 * n, slots), BF)], hbm_out=(0,))
     send, pack = call(
         prepare_body,
         q,
@@ -495,20 +506,30 @@
         mib=20,
     )
     half = slots // 2
-    act, gp, up, far_lo, far_hi, right_lo, right_hi, left_lo, left_hi, mine = call(
+    act, gp, up, far_lo, far_hi = call(
+        hidden_grads_body,
+        q,
+        (rows4[2], grads4[2], down_w, gate_w, up_w, *parts),
+        [((slots, hidden), BF)] * 3 + [((half, quarter), BF)] * 2,
+        in_specs={2: dspec[2], 3: gspec[2], 4: gspec[2]},
+        mib=20,
+        hbm_out=range(5),
+    )
+    right_lo, right_hi, left_lo, left_hi, mine = call(
         expert_back_body,
         q,
-        (rows4[2], grads4[2], down_w, *[gate_w] * 4, *[up_w] * 4, *parts),
-        [((slots, hidden), BF)] * 3 + [((half, quarter), BF)] * 6 + [((slots, quarter), BF)],
-        in_specs={2: dspec[2]} | {3 + k: s for k, s in gspec.items()} | {7 + k: s for k, s in gspec.items()},
-        mib=24,
-        hbm_out=range(10),
+        (gp, up, *[gate_w] * 3, *[up_w] * 3),
+        [((half, quarter), BF)] * 4 + [((slots, quarter), BF)],
+        in_specs={2 + i: gspec[k] for i, k in enumerate(near)} | {5 + i: gspec[k] for i, k in enumerate(near)},
+        mib=20,
+        hbm_in=(0, 1),
+        hbm_out=range(5),
     )
     far_lo, far_hi = shift(far_lo, 1), shift(far_hi, 3)
     right_hi, left_lo = shift(right_hi, 1), shift(left_lo, 3)
     right_lo, left_hi = call(
         pass_on_body, q, (right_lo, far_lo, left_hi, far_hi), [((half, quarter), BF)] * 2,
-        hbm_in=range(4), hbm_out=range(2),
+        hbm_in=(0, 2),
     )
     right_lo, left_hi = shift(right_lo, 1), shift(left_hi, 3)
     gate_grad, up_grad, down_grad = call(
@@ -526,7 +547,8 @@
     )
     (share,) = call(
         share_body, q, (mine, right_lo, right_hi, left_lo, left_hi), [((slots, quarter), BF)],
-        hbm_in=range(5),
+        hbm_in=(0,),
+        hbm_out=(0,),
     )
     share = a2a(share.reshape(64, 8, quarter), SP).reshape(slots, quarter)
     (resid,) = call(combine_body, q, (share, qt, out_grad), [((n, quarter), BF)], in_specs={2: own}, hbm_in=(1, 2))

time: 240 us -> 244 us (1.017)
  Pallas kernels: 44.1 us -> 48 us
  starting transfers between devices: 59.2 us -> 62.9 us
    pallas_call x15 -> x17, Pallas kernels: 44.1 us -> 48 us  [call(): pl.pallas_call(kernel, out_shape=[(pltpu.HBM if i in hbm_out else jax.Sha...]
    all_to_all x5, waiting for transfers between devices: 23.2 us -> 19.8 us  [a2a(): return lax.all_to_all(x, axes, split_axis=0, concat_axis=0, tiled=True)]
    ppermute x15, starting transfers between devices: 15.3 us -> 18.3 us  [shift(): return lax.ppermute(x, TP, [(i, (i + by) % 4) for i in range(4)])]
  transfers between devices with their start and end apart: 27 -> 27, of which waited for: 13 -> 12; matrix products, arithmetic and copies ran while one was open for 2% -> 2% of each run, Pallas kernels for 11% -> 13%
where the time goes in v5:
time: 244 us; the launch traced here: 243 us
  starting transfers between devices  62.9 us (26%)
  waiting for transfers between devices  62.7 us (26%)
  blocking collectives  61.9 us (25%)
  Pallas kernels  48 us (20%)
  local copies, waits for them, and re-layouts  4.92 us (2%)
    all_to_all x2, blocking collectives, a2a(): return lax.all_to_all(x, axes, split_axis=0, concat_axis=0, tiled=True)  61.9 us
    pallas_call x17, Pallas kernels, call(): pl.pallas_call(kernel, out_shape=[(pltpu.HBM if i in hbm_out else jax.Sha...  48 us
    all_to_all x5, starting transfers between devices, a2a(): return lax.all_to_all(x, axes, split_axis=0, concat_axis=0, tiled=True)  35.8 us
    ppermute x15, waiting for transfers between devices, shift(): return lax.ppermute(x, TP, [(i, (i + by) % 4) for i in range(4)])  33.7 us
    all_to_all x5, waiting for transfers between devices, a2a(): return lax.all_to_all(x, axes, split_axis=0, concat_axis=0, tiled=True)  19.8 us
    ppermute x15, starting transfers between devices, shift(): return lax.ppermute(x, TP, [(i, (i + by) % 4) for i in range(4)])  18.3 us
    ppermute x3, waiting for transfers between devices, per_device(): lax.ppermute(nbf, 'sp_1', [(i, (i + by) % 4) for i in range(4)])  8.26 us
    ppermute x4, starting transfers between devices, per_device(): nball = along + [lax.ppermute(a, 'sp_2', [(0, 1), (1, 0)]) for a in along]  5.07 us
  transfers between devices with their start and end apart: 27, of which 12 were waited for; matrix products, arithmetic and copies ran while one was open for 2% of the time, Pallas kernels for 13%

profile of v5, /device:TPU:1, one launch (start us, length us, event | category | flops | bytes accessed | tf_op | source)
XLA Modules:
  0.0 243.0 jit_solution(5960957344836610135)
XLA Ops:
  1.3 3.2 %shard_map.171 = bf16[64,16,512]{2,1,0:T(8,128)(2,1)} custom-call(s32[4]{0:T(128)} %pad_add_fusion.q_ref, s32[2,128]{1,0:T(2,128)} %bitcast.52, f32[2,128]{1,0:T(2,128)} %bitcast.55, bf16[128,2048]{1,0:T(8,128)(2,1)} %refs_2_.2, bf16[128,2048]{1,0:T(8,128)(2,1)} %refs_2_.3), custom_call_target="tpu_custom_call" | custom-call | tf_op jit(solution)/shard_map/pallas_call | solution.py:56
  4.5 41.6 %all_to_all.35 = bf16[64,16,512]{2,1,0:T(8,128)(2,1)S(1)} all-to-all(bf16[64,16,512]{2,1,0:T(8,128)(2,1)} %shard_map.171), channel_id=1, replica_groups=mesh['sp_0'=8,'sp_1'=4,'sp_2'=2,'tp'=4] {'sp_0','sp_1','sp_2'}, dimensions={0} | all-to-all | bytes 2097152 | tf_op jit(solution)/shard_map/all_to_all | solution.py:407
  46.1 1.1 slice_bitcast_fusion
  47.2 1.2 collective-permute-start.1
  48.4 1.5 collective-permute-start.3
  49.9 1.3 collective-permute-start
  51.4 9.7 %collective-permute-done.1.refs_2_.refs_3_ = bf16[512,512]{1,0:T(8,128)(2,1)} collective-permute-done((bf16[512,512]{1,0:T(8,128)(2,1)}, bf16[512,512]{1,0:T(8,128)(2,1)}, u32[]{:S(2)}, u32[]{:S(2)}) %collective-permute-start.1) | collective-permute-done | bytes 524320 | tf_op jit(solution)/shard_map/ppermute | solution.py:411
  61.1 2.7 %collective-permute-start.4 = (bf16[512,512]{1,0:T(8,128)(2,1)}, bf16[512,512]{1,0:T(8,128)(2,1)}, u32[]{:S(2)}, u32[]{:S(2)}) collective-permute-start(bf16[512,512]{1,0:T(8,128)(2,1)} %collective-permute-done.3.refs_4_.refs_5_), channel_id=1, source_target_pairs={{0,3},{1,0},{2,1},{3,2},{4,7},{5,4},{6,5},{7,6},{8,11},{9,8},{10,9... | collective-permute-start | bytes 1572872 | tf_op jit(solution)/shard_map/ppermute | solution.py:411
  65.7 6.3 %collective-permute-done.refs_1_ = bf16[512,512]{1,0:T(8,128)(2,1)} collective-permute-done((bf16[512,512]{1,0:T(8,128)(2,1)}, bf16[512,512]{1,0:T(8,128)(2,1)}, u32[]{:S(2)}, u32[]{:S(2)}) %collective-permute-start) | collective-permute-done | bytes 524320 | tf_op jit(solution)/shard_map/ppermute | solution.py:411
  72.3 3.8 %shard_map.172 = (f32[512,256]{1,0:T(8,128)S(1)}, f32[512,256]{1,0:T(8,128)S(1)}, f32[512,256]{1,0:T(8,128)S(1)}) custom-call(s32[4]{0:T(128)S(1)} %copy-done.10, bf16[512,512]{1,0:T(8,128)(2,1)} %get-tuple-element.78.refs_0_, bf16[512,512]{1,0:T(8,128)(2,1)} %collective-permute-done.refs_1_, bf16[512,512]{1,0:T(8,128)(2,1)} %collective-permute-done.1.refs_2_.refs_3_, ...), custom_call_target="tpu_custom_call" | custom-call | tf_op jit(solution)/shard_map/pallas_call | solution.py:56
  76.1 7.4 %collective-permute-done.2.refs_0_.refs_2_ = bf16[512,512]{1,0:T(8,128)(2,1)} collective-permute-done((bf16[512,512]{1,0:T(8,128)(2,1)}, bf16[512,512]{1,0:T(8,128)(2,1)}, u32[]{:S(2)}, u32[]{:S(2)}) %collective-permute-start.2) | collective-permute-done | bytes 524320 | tf_op jit(solution)/shard_map/ppermute | solution.py:411
  83.6 4.0 %shard_map.173 = (bf16[512,256]{1,0:T(8,128)(2,1)}, bf16[512,256]{1,0:T(8,128)(2,1)}, bf16[512,256]{1,0:T(8,128)(2,1)}, bf16[256,512]{1,0:T(8,128)(2,1)}, bf16[256,512]{1,0:T(8,128)(2,1)}) custom-call(s32[4]{0:T(128)S(1)} %copy-done.10, bf16[512,512]{1,0:T(8,128)(2,1)} %collective-permute-done.2.refs_0_.refs_2_, ...), custom_call_target="tpu_custom_call" | custom-call | tf_op jit(solution)/shard_map/pallas_call | solution.py:56
  88.5 1.7 collective-permute-start.7
  92.5 4.0 %shard_map.180 = (bf16[64,16,128]{2,1,0:T(8,128)(2,1)}, f32[128,1920]{1,0:T(8,128)}) custom-call(s32[4]{0:T(128)} %pad_add_fusion.q_ref, bf16[2,128,128]{2,1,0:T(8,128)(2,1)} %get-tuple-element.82.refs_0_, bf16[2,128,128]{2,1,0:T(8,128)(2,1)} %get-tuple-element.81.refs_1_, bf16[2,128,256]{2,1,0:T(8,128)(2,1)} %bitcast.46, f32[2,128]{1,0:T(2,128)} %bitcast.56, ...), custom_call_target="tpu_custom_call" | custom-call | tf_op jit(solution)/shard_map/pallas_call | solution.py:56
  96.5 8.1 %all-to-all-start.2 = ((bf16[64,16,128]{2,1,0:T(8,128)(2,1)}), bf16[64,16,128]{2,1,0:T(8,128)(2,1)S(1)}, u32[]{:S(2)}, u32[]{:S(2)}) async-start(bf16[64,16,128]{2,1,0:T(8,128)(2,1)} %get-tuple-element.59), calls=%async_computation.2 | async-start | bytes 524288 | tf_op jit(solution)/shard_map/all_to_all | solution.py:407
  104.6 3.4 %shard_map.175 = (bf16[256,512]{1,0:T(8,128)(2,1)}, bf16[256,512]{1,0:T(8,128)(2,1)}, bf16[256,512]{1,0:T(8,128)(2,1)}, bf16[256,512]{1,0:T(8,128)(2,1)}, bf16[512,512]{1,0:T(8,128)(2,1)}) custom-call(s32[4]{0:T(128)S(1)} %copy-done.11, bf16[512,256]{1,0:T(8,128)(2,1)} %get-tuple-element.44.refs_8_.refs_0_, ...), custom_call_target="tpu_custom_call" | custom-call | tf_op jit(solution)/shard_map/pallas_call | solution.py:56
  108.0 2.7 %collective-permute-start.10 = (bf16[256,512]{1,0:T(8,128)(2,1)}, bf16[256,512]{1,0:T(8,128)(2,1)S(1)}, u32[]{:S(2)}, u32[]{:S(2)}) collective-permute-start(bf16[256,512]{1,0:T(8,128)(2,1)} %get-tuple-element.57), channel_id=1, source_target_pairs={{0,3},{1,0},{2,1},{3,2},{4,7},{5,4},{6,5},{7,6},{8,11},{9,8},{10,9... | collective-permute-start | bytes 786440 | tf_op jit(solution)/shard_map/ppermute | solution.py:411
  110.7 1.7 shard_map.176
  112.5 2.7 %collective-permute-start.11 = (bf16[256,512]{1,0:T(8,128)(2,1)S(1)}, bf16[256,512]{1,0:T(8,128)(2,1)S(1)}, u32[]{:S(2)}, u32[]{:S(2)}) collective-permute-start(bf16[256,512]{1,0:T(8,128)(2,1)S(1)} %get-tuple-element.58), channel_id=1, source_target_pairs={{0,3},{1,0},{2,1},{3,2},{4,7},{5,4},{6,5},{7,6},{8,11},{9,8},{10,9... | collective-permute-start | bytes 786440 | tf_op jit(solution)/shard_map/ppermute | solution.py:411
  115.2 1.7 collective-permute-done.9.refs_2_
  116.9 5.6 %collective-permute-done.8.refs_1_ = bf16[256,512]{1,0:T(8,128)(2,1)S(1)} collective-permute-done((bf16[256,512]{1,0:T(8,128)(2,1)S(1)}, bf16[256,512]{1,0:T(8,128)(2,1)S(1)}, u32[]{:S(2)}, u32[]{:S(2)}) %collective-permute-start.8) | collective-permute-done | bytes 262176 | tf_op jit(solution)/shard_map/ppermute | solution.py:411
  122.5 2.6 %shard_map.177 = bf16[512,512]{1,0:T(8,128)(2,1)} custom-call(s32[4]{0:T(128)S(1)} %copy-done.11, bf16[512,512]{1,0:T(8,128)(2,1)} %get-tuple-element.50.refs_0_, bf16[256,512]{1,0:T(8,128)(2,1)S(1)} %collective-permute-done.8.refs_1_, bf16[256,512]{1,0:T(8,128)(2,1)S(1)} %collective-permute-done.9.refs_2_, ...), custom_call_target="tpu_custom_call" | custom-call | tf_op jit(solution)/shard_map/pallas_call | solution.py:56
  125.1 11.7 %all-to-all-start.1 = ((bf16[64,8,512]{2,1,0:T(8,128)(2,1)}), bf16[64,8,512]{2,1,0:T(8,128)(2,1)}, u32[]{:S(2)}, u32[]{:S(2)}) async-start(bf16[64,8,512]{2,1,0:T(8,128)(2,1)} %bitcast.54), calls=%async_computation.1 | async-start | bytes 1048576 | tf_op jit(solution)/shard_map/all_to_all | solution.py:407
  136.8 2.0 shard_map.181
  138.7 15.6 %all-to-all-done.1 = bf16[64,8,512]{2,1,0:T(8,128)(2,1)} async-done(((bf16[64,8,512]{2,1,0:T(8,128)(2,1)}), bf16[64,8,512]{2,1,0:T(8,128)(2,1)}, u32[]{:S(2)}, u32[]{:S(2)}) %all-to-all-start.1) | async-done | bytes 524320 | tf_op jit(solution)/shard_map/all_to_all | solution.py:407
  154.4 5.7 %all-to-all-start.3 = ((bf16[64,8,128]{2,1,0:T(8,128)(2,1)}), bf16[64,8,128]{2,1,0:T(8,128)(2,1)S(1)}, u32[]{:S(2)}, u32[]{:S(2)}) async-start(bf16[64,8,128]{2,1,0:T(8,128)(2,1)} %get-tuple-element.60), calls=%async_computation.3 | async-start | bytes 262144 | tf_op jit(solution)/shard_map/all_to_all | solution.py:407
  160.1 1.5 shard_map.178.refs_1_
  161.6 2.0 shard_map.179.refs_0_
  163.5 2.8 %collective-permute-start.12 = (bf16[128,512]{1,0:T(8,128)(2,1)S(1)}, bf16[128,512]{1,0:T(8,128)(2,1)S(1)}, u32[]{:S(2)}, u32[]{:S(2)}) collective-permute-start(bf16[128,512]{1,0:T(8,128)(2,1)S(1)} %shard_map.179.refs_0_), channel_id=1, source_target_pairs={{0,3},{1,0},{2,1},{3,2},{4,7},{5,4},{6,5},{7,6},{8,11},{9,8},{10,9... | collective-permute-start | bytes 393224 | tf_op jit(solution)/shard_map/ppermute | solution.py:411
  167.0 4.2 %all-to-all-done.3 = bf16[64,8,128]{2,1,0:T(8,128)(2,1)S(1)} async-done(((bf16[64,8,128]{2,1,0:T(8,128)(2,1)}), bf16[64,8,128]{2,1,0:T(8,128)(2,1)S(1)}, u32[]{:S(2)}, u32[]{:S(2)}) %all-to-all-start.3) | async-done | bytes 131104 | tf_op jit(solution)/shard_map/all_to_all | solution.py:407
  171.2 1.8 shard_map.182
  173.0 2.6 %collective-permute-done.14.refs_3_ = bf16[128,512]{1,0:T(8,128)(2,1)} collective-permute-done((bf16[128,512]{1,0:T(8,128)(2,1)S(1)}, bf16[128,512]{1,0:T(8,128)(2,1)}, u32[]{:S(2)}, u32[]{:S(2)}) %collective-permute-start.14) | collective-permute-done | bytes 131104 | tf_op jit(solution)/shard_map/ppermute | solution.py:411
  175.6 3.5 %shard_map.183 = (f32[128,512]{1,0:T(8,128)}, bf16[8,320,128]{2,1,0:T(8,128)(2,1)}) custom-call(s32[4]{0:T(128)S(1)} %copy-done.11, bf16[128,512]{1,0:T(8,128)(2,1)S(1)} %shard_map.179.refs_0_, bf16[128,512]{1,0:T(8,128)(2,1)S(1)} %collective-permute-done.12.refs_1_, bf16[128,512]{1,0:T(8,128)(2,1)} %collective-permute-done.13.refs_2_, ...), custom_call_target="tpu_custom_call" | custom-call | tf_op jit(solution)/shard_map/pallas_call | solution.py:56
  179.0 5.3 %all-to-all-start.4 = ((bf16[8,320,128]{2,1,0:T(8,128)(2,1)}), bf16[8,320,128]{2,1,0:T(8,128)(2,1)S(1)}, u32[]{:S(2)}, u32[]{:S(2)}) async-start(bf16[8,320,128]{2,1,0:T(8,128)(2,1)} %get-tuple-element.63), calls=%async_computation.4 | async-start | bytes 1310720 | tf_op jit(solution)/shard_map/all_to_all | solution.py:407
  184.4 2.6 %collective-permute-start.15 = (bf16[128,512]{1,0:T(8,128)(2,1)}, bf16[128,512]{1,0:T(8,128)(2,1)S(1)}, u32[]{:S(2)}, u32[]{:S(2)}) collective-permute-start(bf16[128,512]{1,0:T(8,128)(2,1)} %get-tuple-element.64.refs_1_), channel_id=1, source_target_pairs={{0,24},{8,0},{16,8},{24,16},{1,25},{9,1},{17,9},{25,17},{2,26},{10... | collective-permute-start | bytes 393224 | tf_op jit(solution)/shard_map/ppermute | solution.py:491
  188.1 1.2 collective-permute-start.18
  189.3 7.1 %collective-permute-done.15.refs_2_ = bf16[128,512]{1,0:T(8,128)(2,1)S(1)} collective-permute-done((bf16[128,512]{1,0:T(8,128)(2,1)}, bf16[128,512]{1,0:T(8,128)(2,1)S(1)}, u32[]{:S(2)}, u32[]{:S(2)}) %collective-permute-start.15) | collective-permute-done | bytes 131104 | tf_op jit(solution)/shard_map/ppermute | solution.py:491
  196.5 1.5 collective-permute-start.19
  198.0 1.5 collective-permute-start.20
  199.5 1.1 collective-permute-done.17.refs_4_
  201.5 0.9 collective-permute-done.21.refs_8_
  203.1 2.5 %shard_map.184 = (f32[8,64,128]{2,1,0:T(8,128)S(1)}, bf16[8,192,128]{2,1,0:T(8,128)(2,1)S(1)}) custom-call(s32[4]{0:T(128)S(1)} %copy-done.11, bf16[8,320,128]{2,1,0:T(8,128)(2,1)S(1)} %all-to-all-done.4.refs_0_, bf16[128,512]{1,0:T(8,128)(2,1)} %get-tuple-element.64.refs_1_, bf16[128,512]{1,0:T(8,128)(2,1)} %copy-done.13, bf16[128,512]{1,0:T(8,128)(2,1)} %copy-done.14, ...), custom_call_target="tpu_custom_call" | custom-call | tf_op jit(solution)/shard_map/pallas_call | solution.py:56
  205.6 20.3 %all_to_all.36.refs_0_ = bf16[8,192,128]{2,1,0:T(8,128)(2,1)S(1)} all-to-all(bf16[8,192,128]{2,1,0:T(8,128)(2,1)S(1)} %get-tuple-element.66), channel_id=1, replica_groups=mesh['sp_0'=8,'sp_1'=4,'sp_2'=2,'tp'=4] {'sp_0'}, dimensions={0} | all-to-all | bytes 786432 | tf_op jit(solution)/shard_map/all_to_all | solution.py:407
  225.9 1.3 shard_map.185
  227.2 4.9 %all-to-all-start.6 = ((bf16[8,64,128]{2,1,0:T(8,128)(2,1)}), bf16[8,64,128]{2,1,0:T(8,128)(2,1)S(1)}, u32[]{:S(2)}, u32[]{:S(2)}) async-start(bf16[8,64,128]{2,1,0:T(8,128)(2,1)} %get-tuple-element.71), calls=%async_computation.6 | async-start | bytes 262144 | tf_op jit(solution)/shard_map/all_to_all | solution.py:407
  232.2 6.4 %shard_map.174 = (bf16[2048,256]{1,0:T(8,128)(2,1)}, bf16[2048,256]{1,0:T(8,128)(2,1)}, bf16[256,2048]{1,0:T(8,128)(2,1)}) custom-call(s32[4]{0:T(128)S(1)} %copy-done.11, bf16[512,512]{1,0:T(8,128)(2,1)} %get-tuple-element.78.refs_0_, bf16[512,512]{1,0:T(8,128)(2,1)} %collective-permute-done.refs_1_, ...), custom_call_target="tpu_custom_call" | custom-call | tf_op jit(solution)/shard_map/pallas_call | solution.py:56
  238.6 2.4 shard_map.186
  241.0 2.0 shard_map.187
  (85 shorter events, 9.7 us)
Async XLA Ops:
  4.5 60.5 %copy-start.21 = (bf16[128,2,128]{2,1,0:T(2,128)(2,1)S(1)}, bf16[128,2,128]{2,1,0:T(2,128)(2,1)}, u32[]{:S(2)}) copy-start(bf16[128,2,128]{2,1,0:T(2,128)(2,1)} %param.17) | copy-start | bytes 196612
  4.5 60.5 %copy-start.22 = (bf16[128,2,128]{2,1,0:T(2,128)(2,1)S(1)}, bf16[128,2,128]{2,1,0:T(2,128)(2,1)}, u32[]{:S(2)}) copy-start(bf16[128,2,128]{2,1,0:T(2,128)(2,1)} %param.16) | copy-start | bytes 196612
  4.5 67.8 %copy-start = (bf16[1,2048,256]{2,1,0:T(8,128)(2,1)S(1)}, bf16[1,2048,256]{2,1,0:T(8,128)(2,1)}, u32[]{:S(2)}) copy-start(bf16[1,2048,256]{2,1,0:T(8,128)(2,1)} %param.21) | copy-start | bytes 3145732
  4.5 67.8 %copy-start.1 = (bf16[1,2048,256]{2,1,0:T(8,128)(2,1)S(1)}, bf16[1,2048,256]{2,1,0:T(8,128)(2,1)}, u32[]{:S(2)}) copy-start(bf16[1,2048,256]{2,1,0:T(8,128)(2,1)} %param.22) | copy-start | bytes 3145732
  4.5 67.8 %copy-start.3 = (bf16[1,256,2048]{2,1,0:T(8,128)(2,1)S(1)}, bf16[1,256,2048]{2,1,0:T(8,128)(2,1)}, u32[]{:S(2)}) copy-start(bf16[1,256,2048]{2,1,0:T(8,128)(2,1)} %param.23) | copy-start | bytes 3145732
  4.5 67.8 %copy-start.10 = (s32[4]{0:T(128)S(1)}, s32[4]{0:T(128)}, u32[]{:S(2)}) copy-start(s32[4]{0:T(128)} %pad_add_fusion.q_ref) | copy-start | bytes 52
  47.2 13.9 %collective-permute-start.1 = (bf16[512,512]{1,0:T(8,128)(2,1)}, bf16[512,512]{1,0:T(8,128)(2,1)}, u32[]{:S(2)}, u32[]{:S(2)}) collective-permute-start(bf16[512,512]{1,0:T(8,128)(2,1)} %get-tuple-element.78.refs_0_), channel_id=1, source_target_pairs={{0,1},{1,2},{2,3},{3,0},{4,5},{5,6},{6,7},{7,4},{8,9},{9,10},{10,1... | collective-permute-start | bytes 1572872 | tf_op jit(solution)/shard_map/ppermute | solution.py:411
  48.4 12.7 %collective-permute-start.3 = (bf16[512,512]{1,0:T(8,128)(2,1)}, bf16[512,512]{1,0:T(8,128)(2,1)}, u32[]{:S(2)}, u32[]{:S(2)}) collective-permute-start(bf16[512,512]{1,0:T(8,128)(2,1)} %get-tuple-element.77.refs_3_.refs_4_), channel_id=1, source_target_pairs={{0,3},{1,0},{2,1},{3,2},{4,7},{5,4},{6,5},{7,6},{8,11},{9,8},{10,9... | collective-permute-start | bytes 1572872 | tf_op jit(solution)/shard_map/ppermute | solution.py:411
  49.9 22.1 %collective-permute-start = (bf16[512,512]{1,0:T(8,128)(2,1)}, bf16[512,512]{1,0:T(8,128)(2,1)}, u32[]{:S(2)}, u32[]{:S(2)}) collective-permute-start(bf16[512,512]{1,0:T(8,128)(2,1)} %get-tuple-element.78.refs_0_), channel_id=1, source_target_pairs={{0,3},{1,0},{2,1},{3,2},{4,7},{5,4},{6,5},{7,6},{8,11},{9,8},{10,9... | collective-permute-start | bytes 1572872 | tf_op jit(solution)/shard_map/ppermute | solution.py:411
  51.2 21.1 %collective-permute-start.5 = (bf16[512,512]{1,0:T(8,128)(2,1)}, bf16[512,512]{1,0:T(8,128)(2,1)}, u32[]{:S(2)}, u32[]{:S(2)}) collective-permute-start(bf16[512,512]{1,0:T(8,128)(2,1)} %get-tuple-element.77.refs_3_.refs_4_), channel_id=1, source_target_pairs={{0,1},{1,2},{2,3},{3,0},{4,5},{5,6},{6,7},{7,4},{8,9},{9,10},{10,1... | collective-permute-start | bytes 1572872 | tf_op jit(solution)/shard_map/ppermute | solution.py:411
  61.1 22.5 %collective-permute-start.2 = (bf16[512,512]{1,0:T(8,128)(2,1)}, bf16[512,512]{1,0:T(8,128)(2,1)}, u32[]{:S(2)}, u32[]{:S(2)}) collective-permute-start(bf16[512,512]{1,0:T(8,128)(2,1)} %collective-permute-done.1.refs_2_.refs_3_), channel_id=1, source_target_pairs={{0,1},{1,2},{2,3},{3,0},{4,5},{5,6},{6,7},{7,4},{8,9},{9,10},{10,1... | collective-permute-start | bytes 1572872 | tf_op jit(solution)/shard_map/ppermute | solution.py:411
  61.1 22.5 %collective-permute-start.4 = (bf16[512,512]{1,0:T(8,128)(2,1)}, bf16[512,512]{1,0:T(8,128)(2,1)}, u32[]{:S(2)}, u32[]{:S(2)}) collective-permute-start(bf16[512,512]{1,0:T(8,128)(2,1)} %collective-permute-done.3.refs_4_.refs_5_), channel_id=1, source_target_pairs={{0,3},{1,0},{2,1},{3,2},{4,7},{5,4},{6,5},{7,6},{8,11},{9,8},{10,9... | collective-permute-start | bytes 1572872 | tf_op jit(solution)/shard_map/ppermute | solution.py:411
  83.6 6.7 %copy-start.20 = (bf16[128,2,256]{2,1,0:T(2,128)(2,1)S(1)}, bf16[128,2,256]{2,1,0:T(2,128)(2,1)}, u32[]{:S(2)}) copy-start(bf16[128,2,256]{2,1,0:T(2,128)(2,1)} %param.18) | copy-start | bytes 393220
  83.6 21.1 %copy-start.11 = (s32[4]{0:T(128)S(1)}, s32[4]{0:T(128)}, u32[]{:S(2)}) copy-start(s32[4]{0:T(128)} %pad_add_fusion.q_ref) | copy-start | bytes 52
  87.6 23.1 %collective-permute-start.6 = (bf16[256,512]{1,0:T(8,128)(2,1)}, bf16[256,512]{1,0:T(8,128)(2,1)S(1)}, u32[]{:S(2)}, u32[]{:S(2)}) collective-permute-start(bf16[256,512]{1,0:T(8,128)(2,1)} %get-tuple-element.52), channel_id=1, source_target_pairs={{0,1},{1,2},{2,3},{3,0},{4,5},{5,6},{6,7},{7,4},{8,9},{9,10},{10,1... | collective-permute-start | bytes 786440 | tf_op jit(solution)/shard_map/ppermute | solution.py:411
  88.5 22.2 %collective-permute-start.7 = (bf16[256,512]{1,0:T(8,128)(2,1)}, bf16[256,512]{1,0:T(8,128)(2,1)S(1)}, u32[]{:S(2)}, u32[]{:S(2)}) collective-permute-start(bf16[256,512]{1,0:T(8,128)(2,1)} %get-tuple-element.54), channel_id=1, source_target_pairs={{0,3},{1,0},{2,1},{3,2},{4,7},{5,4},{6,5},{7,6},{8,11},{9,8},{10,9... | collective-permute-start | bytes 786440 | tf_op jit(solution)/shard_map/ppermute | solution.py:411
  96.5 28.6 %all-to-all-start.2 = ((bf16[64,16,128]{2,1,0:T(8,128)(2,1)}), bf16[64,16,128]{2,1,0:T(8,128)(2,1)S(1)}, u32[]{:S(2)}, u32[]{:S(2)}) async-start(bf16[64,16,128]{2,1,0:T(8,128)(2,1)} %get-tuple-element.59), calls=%async_computation.2 | async-start | bytes 524288 | tf_op jit(solution)/shard_map/all_to_all | solution.py:407
  108.0 8.8 %collective-permute-start.9 = (bf16[256,512]{1,0:T(8,128)(2,1)}, bf16[256,512]{1,0:T(8,128)(2,1)S(1)}, u32[]{:S(2)}, u32[]{:S(2)}) collective-permute-start(bf16[256,512]{1,0:T(8,128)(2,1)} %get-tuple-element.56), channel_id=1, source_target_pairs={{0,1},{1,2},{2,3},{3,0},{4,5},{5,6},{6,7},{7,4},{8,9},{9,10},{10,1... | collective-permute-start | bytes 786440 | tf_op jit(solution)/shard_map/ppermute | solution.py:411
  108.0 8.8 %collective-permute-start.10 = (bf16[256,512]{1,0:T(8,128)(2,1)}, bf16[256,512]{1,0:T(8,128)(2,1)S(1)}, u32[]{:S(2)}, u32[]{:S(2)}) collective-permute-start(bf16[256,512]{1,0:T(8,128)(2,1)} %get-tuple-element.57), channel_id=1, source_target_pairs={{0,3},{1,0},{2,1},{3,2},{4,7},{5,4},{6,5},{7,6},{8,11},{9,8},{10,9... | collective-permute-start | bytes 786440 | tf_op jit(solution)/shard_map/ppermute | solution.py:411
  112.4 47.7 %copy-start.12 = (s32[128,2]{0,1:T(2,128)S(1)}, s32[128,2]{0,1:T(2,128)}, u32[]{:S(2)}) copy-start(s32[128,2]{0,1:T(2,128)} %param.14) | copy-start | bytes 3076
  112.4 10.1 %collective-permute-start.8 = (bf16[256,512]{1,0:T(8,128)(2,1)S(1)}, bf16[256,512]{1,0:T(8,128)(2,1)S(1)}, u32[]{:S(2)}, u32[]{:S(2)}) collective-permute-start(bf16[256,512]{1,0:T(8,128)(2,1)S(1)} %get-tuple-element.55), channel_id=1, source_target_pairs={{0,1},{1,2},{2,3},{3,0},{4,5},{5,6},{6,7},{7,4},{8,9},{9,10},{10,1... | collective-permute-start | bytes 786440 | tf_op jit(solution)/shard_map/ppermute | solution.py:411
  112.5 10.0 %collective-permute-start.11 = (bf16[256,512]{1,0:T(8,128)(2,1)S(1)}, bf16[256,512]{1,0:T(8,128)(2,1)S(1)}, u32[]{:S(2)}, u32[]{:S(2)}) collective-permute-start(bf16[256,512]{1,0:T(8,128)(2,1)S(1)} %get-tuple-element.58), channel_id=1, source_target_pairs={{0,3},{1,0},{2,1},{3,2},{4,7},{5,4},{6,5},{7,6},{8,11},{9,8},{10,9... | collective-permute-start | bytes 786440 | tf_op jit(solution)/shard_map/ppermute | solution.py:411
  125.1 46.1 %copy-start.4 = (f32[128,1920]{1,0:T(8,128)S(1)}, f32[128,1920]{1,0:T(8,128)}, u32[]{:S(2)}) copy-start(f32[128,1920]{1,0:T(8,128)} %get-tuple-element.61.refs_1_.refs_2_) | copy-start | bytes 2949124
  125.1 50.5 %copy-start.2 = (bf16[2048,512]{1,0:T(8,128)(2,1)S(1)}, bf16[2048,512]{1,0:T(8,128)(2,1)}, u32[]{:S(2)}) copy-start(bf16[2048,512]{1,0:T(8,128)(2,1)} %refs_7_.1) | copy-start | bytes 6291460
  125.1 29.3 %all-to-all-start.1 = ((bf16[64,8,512]{2,1,0:T(8,128)(2,1)}), bf16[64,8,512]{2,1,0:T(8,128)(2,1)}, u32[]{:S(2)}, u32[]{:S(2)}) async-start(bf16[64,8,512]{2,1,0:T(8,128)(2,1)} %bitcast.54), calls=%async_computation.1 | async-start | bytes 1048576 | tf_op jit(solution)/shard_map/all_to_all | solution.py:407
  154.4 16.8 %all-to-all-start.3 = ((bf16[64,8,128]{2,1,0:T(8,128)(2,1)}), bf16[64,8,128]{2,1,0:T(8,128)(2,1)S(1)}, u32[]{:S(2)}, u32[]{:S(2)}) async-start(bf16[64,8,128]{2,1,0:T(8,128)(2,1)} %get-tuple-element.60), calls=%async_computation.3 | async-start | bytes 262144 | tf_op jit(solution)/shard_map/all_to_all | solution.py:407
  163.5 9.4 %collective-permute-start.12 = (bf16[128,512]{1,0:T(8,128)(2,1)S(1)}, bf16[128,512]{1,0:T(8,128)(2,1)S(1)}, u32[]{:S(2)}, u32[]{:S(2)}) collective-permute-start(bf16[128,512]{1,0:T(8,128)(2,1)S(1)} %shard_map.179.refs_0_), channel_id=1, source_target_pairs={{0,3},{1,0},{2,1},{3,2},{4,7},{5,4},{6,5},{7,6},{8,11},{9,8},{10,9... | collective-permute-start | bytes 393224 | tf_op jit(solution)/shard_map/ppermute | solution.py:411
  166.3 6.7 %collective-permute-start.13 = (bf16[128,512]{1,0:T(8,128)(2,1)S(1)}, bf16[128,512]{1,0:T(8,128)(2,1)}, u32[]{:S(2)}, u32[]{:S(2)}) collective-permute-start(bf16[128,512]{1,0:T(8,128)(2,1)S(1)} %shard_map.179.refs_0_), channel_id=1, source_target_pairs={{0,2},{1,3},{2,0},{3,1},{4,6},{5,7},{6,4},{7,5},{8,10},{9,11},{10,... | collective-permute-start | bytes 393224 | tf_op jit(solution)/shard_map/ppermute | solution.py:411
  166.3 9.3 %collective-permute-start.14 = (bf16[128,512]{1,0:T(8,128)(2,1)S(1)}, bf16[128,512]{1,0:T(8,128)(2,1)}, u32[]{:S(2)}, u32[]{:S(2)}) collective-permute-start(bf16[128,512]{1,0:T(8,128)(2,1)S(1)} %shard_map.179.refs_0_), channel_id=1, source_target_pairs={{0,1},{1,2},{2,3},{3,0},{4,5},{5,6},{6,7},{7,4},{8,9},{9,10},{10,1... | collective-permute-start | bytes 393224 | tf_op jit(solution)/shard_map/ppermute | solution.py:411
  179.0 53.1 %copy-start.6 = (bf16[512,256]{1,0:T(8,128)(2,1)S(1)}, bf16[512,256]{1,0:T(8,128)(2,1)}, u32[]{:S(2)}) copy-start(bf16[512,256]{1,0:T(8,128)(2,1)} %get-tuple-element.44.refs_8_.refs_0_) | copy-start | bytes 786436
  179.0 53.1 %copy-start.7 = (bf16[512,256]{1,0:T(8,128)(2,1)S(1)}, bf16[512,256]{1,0:T(8,128)(2,1)}, u32[]{:S(2)}) copy-start(bf16[512,256]{1,0:T(8,128)(2,1)} %get-tuple-element.45.refs_9_.refs_1_) | copy-start | bytes 786436
  179.0 53.1 %copy-start.8 = (bf16[512,256]{1,0:T(8,128)(2,1)S(1)}, bf16[512,256]{1,0:T(8,128)(2,1)}, u32[]{:S(2)}) copy-start(bf16[512,256]{1,0:T(8,128)(2,1)} %get-tuple-element.46.refs_10_) | copy-start | bytes 786436
  179.0 23.4 %all-to-all-start.4 = ((bf16[8,320,128]{2,1,0:T(8,128)(2,1)}), bf16[8,320,128]{2,1,0:T(8,128)(2,1)S(1)}, u32[]{:S(2)}, u32[]{:S(2)}) async-start(bf16[8,320,128]{2,1,0:T(8,128)(2,1)} %get-tuple-element.63), calls=%async_computation.4 | async-start | bytes 1310720 | tf_op jit(solution)/shard_map/all_to_all | solution.py:407
  184.4 12.1 %collective-permute-start.15 = (bf16[128,512]{1,0:T(8,128)(2,1)}, bf16[128,512]{1,0:T(8,128)(2,1)S(1)}, u32[]{:S(2)}, u32[]{:S(2)}) collective-permute-start(bf16[128,512]{1,0:T(8,128)(2,1)} %get-tuple-element.64.refs_1_), channel_id=1, source_target_pairs={{0,24},{8,0},{16,8},{24,16},{1,25},{9,1},{17,9},{25,17},{2,26},{10... | collective-permute-start | bytes 393224 | tf_op jit(solution)/shard_map/ppermute | solution.py:491
  187.0 11.1 %collective-permute-start.16 = (bf16[128,512]{1,0:T(8,128)(2,1)}, bf16[128,512]{1,0:T(8,128)(2,1)S(1)}, u32[]{:S(2)}, u32[]{:S(2)}) collective-permute-start(bf16[128,512]{1,0:T(8,128)(2,1)} %get-tuple-element.64.refs_1_), channel_id=1, source_target_pairs={{0,16},{8,24},{16,0},{24,8},{1,17},{9,25},{17,1},{25,9},{2,18},{10... | collective-permute-start | bytes 393224 | tf_op jit(solution)/shard_map/ppermute | solution.py:491
  187.5 13.1 %collective-permute-start.17 = (bf16[128,512]{1,0:T(8,128)(2,1)}, bf16[128,512]{1,0:T(8,128)(2,1)S(1)}, u32[]{:S(2)}, u32[]{:S(2)}) collective-permute-start(bf16[128,512]{1,0:T(8,128)(2,1)} %get-tuple-element.64.refs_1_), channel_id=1, source_target_pairs={{0,8},{8,16},{16,24},{24,0},{1,9},{9,17},{17,25},{25,1},{2,10},{10... | collective-permute-start | bytes 393224 | tf_op jit(solution)/shard_map/ppermute | solution.py:491
  188.1 13.3 %collective-permute-start.18 = (bf16[128,512]{1,0:T(8,128)(2,1)}, bf16[128,512]{1,0:T(8,128)(2,1)S(1)}, u32[]{:S(2)}, u32[]{:S(2)}) collective-permute-start(bf16[128,512]{1,0:T(8,128)(2,1)} %get-tuple-element.64.refs_1_), channel_id=1, source_target_pairs={{0,4},{4,0},{1,5},{5,1},{2,6},{6,2},{3,7},{7,3},{8,12},{12,8},{9,1... | collective-permute-start | bytes 393224 | tf_op jit(solution)/shard_map/ppermute | solution.py:492
  196.5 6.6 %copy-start.13 = (bf16[128,512]{1,0:T(8,128)(2,1)}, bf16[128,512]{1,0:T(8,128)(2,1)S(1)}, u32[]{:S(2)}) copy-start(bf16[128,512]{1,0:T(8,128)(2,1)S(1)} %collective-permute-done.15.refs_2_) | copy-start | bytes 393220
  196.5 5.0 %collective-permute-start.19 = (bf16[128,512]{1,0:T(8,128)(2,1)S(1)}, bf16[128,512]{1,0:T(8,128)(2,1)S(1)}, u32[]{:S(2)}, u32[]{:S(2)}) collective-permute-start(bf16[128,512]{1,0:T(8,128)(2,1)S(1)} %collective-permute-done.15.refs_2_), channel_id=1, source_target_pairs={{0,4},{4,0},{1,5},{5,1},{2,6},{6,2},{3,7},{7,3},{8,12},{12,8},{9,1... | collective-permute-start | bytes 393224 | tf_op jit(solution)/shard_map/ppermute | solution.py:492
  198.0 5.0 %copy-start.14 = (bf16[128,512]{1,0:T(8,128)(2,1)}, bf16[128,512]{1,0:T(8,128)(2,1)S(1)}, u32[]{:S(2)}) copy-start(bf16[128,512]{1,0:T(8,128)(2,1)S(1)} %collective-permute-done.16.refs_3_) | copy-start | bytes 393220
  198.0 3.4 %collective-permute-start.20 = (bf16[128,512]{1,0:T(8,128)(2,1)S(1)}, bf16[128,512]{1,0:T(8,128)(2,1)S(1)}, u32[]{:S(2)}, u32[]{:S(2)}) collective-permute-start(bf16[128,512]{1,0:T(8,128)(2,1)S(1)} %collective-permute-done.16.refs_3_), channel_id=1, source_target_pairs={{0,4},{4,0},{1,5},{5,1},{2,6},{6,2},{3,7},{7,3},{8,12},{12,8},{9,1... | collective-permute-start | bytes 393224 | tf_op jit(solution)/shard_map/ppermute | solution.py:492
  200.6 2.4 copy-start.15
  200.6 1.8 collective-permute-start.21
  201.4 1.6 copy-start.16
  201.4 1.0 copy-start.17
  227.2 13.8 %all-to-all-start.6 = ((bf16[8,64,128]{2,1,0:T(8,128)(2,1)}), bf16[8,64,128]{2,1,0:T(8,128)(2,1)S(1)}, u32[]{:S(2)}, u32[]{:S(2)}) async-start(bf16[8,64,128]{2,1,0:T(8,128)(2,1)} %get-tuple-element.71), calls=%async_computation.6 | async-start | bytes 262144 | tf_op jit(solution)/shard_map/all_to_all | solution.py:407
  232.2 6.4 %copy-start.5 = (bf16[128,2,256]{2,0,1:T(8,128)(2,1)S(1)}, bf16[128,2,256]{2,0,1:T(8,128)(2,1)}, u32[]{:S(2)}) copy-start(bf16[128,2,256]{2,0,1:T(8,128)(2,1)} %copy.28) | copy-start | bytes 393220
  232.2 6.4 %copy-start.9 = (f32[128,512]{1,0:T(8,128)S(1)}, f32[128,512]{1,0:T(8,128)}, u32[]{:S(2)}) copy-start(f32[128,512]{1,0:T(8,128)} %get-tuple-element.69.refs_0_) | copy-start | bytes 786436
  (2 other events, 1.6 us)

commit v6 on v5

--- a/solution.py
+++ b/solution.py
@@ -31,6 +31,22 @@
 
 def mmh(a, b, dims=NN):
     return lax.dot_general(a, b, dims, precision=HI, preferred_element_type=F32)
+
+
+def mms(a, b, dims=NN):
+    def parts(x):
+        if x.dtype == BF:
+            return [x]
+        hi = x.astype(BF)
+        return [hi, (x - hi.astype(F32)).astype(BF)]
+
+    pa, pb = parts(a), parts(b)
+    out = mm(pa[0], pb[0], dims)
+    for x in pa[1:]:
+        out = out + mm(x, pb[0], dims)
+    for x in pb[1:]:
+        out = out + mm(pa[0], x, dims)
+    return out
 
 
 def iota(shape, dim):
@@ -229,16 +245,16 @@
         left = jnp.exp(total - rt_c)
         qh = turned(qv[h].astype(F32), c, s)
         kh = turned(kv[h].astype(F32), c, s) * (kd**-0.5)
-        vh = vv[h].astype(F32)
-        inner = mmh((kh * left).T, vh)
+        vh = vv[h]
+        inner = mms((kh * left).T, vh)
         for u in range(vd // 128):
             pieces.append(inner[:, u * 128 : (u + 1) * 128])
         hi = total.astype(BF).astype(F32)
         mid = (total - hi).astype(BF).astype(F32)
         for k, part in enumerate((hi, mid, total - hi - mid)):
             logs = jnp.where(sub == 3 * h + k, part[None], logs)
-        w = mmh(qh, kh, NT) * mask
-        pack[:, INTRA + h * vd : INTRA + (h + 1) * vd] = mmh(w, vh)
+        w = mms(qh, kh, NT) * mask
+        pack[:, INTRA + h * vd : INTRA + (h + 1) * vd] = mms(w, vh)
         at = h * 128
         pack[:, QR + at : QR + at + 128] = qh
         pack[:, KR + at : KR + at + 128] = kh
@@ -288,14 +304,14 @@
 def normed_body(q, state, pack, nbf, back):
     n = pack.shape[0]
     heads, vd = 2, 256
-    st = state[...].astype(F32)
+    st = state[...]
     lane = iota((n, 128), 1)
     invs = jnp.zeros((n, 128), F32)
     for h in range(heads):
         sl = slice(h * vd, (h + 1) * vd)
         qh = pack[:, QR + h * 128 : QR + (h + 1) * 128]
         grow = pack[:, SCAL + h : SCAL + h + 1]
-        ret = pack[:, INTRA + h * vd : INTRA + (h + 1) * vd] + grow * mmh(qh, joined(st, h, vd))
+        ret = pack[:, INTRA + h * vd : INTRA + (h + 1) * vd] + grow * mms(qh, joined(st, h, vd))
         iv = lax.rsqrt(jnp.mean(ret * ret, axis=1, keepdims=True) + EPSILON)
         nm = ret * iv
         back[:, sl] = nm
@@ -316,7 +332,7 @@
         m = jnp.mean(g * nm, axis=1, keepdims=True)
         grad = back[:, INV + h : INV + h + 1] * (g - nm * m)
         rg[:, sl] = grad
-        inner = mmh(back[:, QDT + h * 128 : QDT + (h + 1) * 128], grad)
+        inner = mms(back[:, QDT + h * 128 : QDT + (h + 1) * 128], grad)
         for u in range(vd // 128):
             for e in range(2):
                 part = inner[e * 64 : (e + 1) * 64, u * 128 : (u + 1) * 128]
@@ -334,17 +350,17 @@
 def local_grads_body(q, rg, vv, pack, state, qg, rest):
     heads, vd = 2, 256
     parts = []
-    st = state[...].astype(F32)
+    st = state[...]
     c, s = pack[:, COS : COS + 128], pack[:, SIN : SIN + 128]
     for h in range(heads):
         at = h * 128
         grad = rg[:, h * vd : (h + 1) * vd]
-        score = mmh(grad, vv[h].astype(F32), NT) * pack[:, MASK + at : MASK + at + 128]
+        score = mms(grad, vv[h], NT) * pack[:, MASK + at : MASK + at + 128]
         grow = pack[:, SCAL + h : SCAL + h + 1]
-        qp = mmh(score, pack[:, KR + at : KR + at + 128]) + grow * mmh(grad, joined(st, h, vd), NT)
+        qp = mms(score, pack[:, KR + at : KR + at + 128]) + grow * mms(grad, joined(st, h, vd), NT)
         parts.append(turned(qp, c, -s))
-        rest[:, at : at + 128] = mmh(score.T, pack[:, QR + at : QR + at + 128])
-        rest[:, 256 + h * vd : 256 + (h + 1) * vd] = mmh(pack[:, WTS + at : WTS + at + 128].T, grad)
+        rest[:, at : at + 128] = mms(score.T, pack[:, QR + at : QR + at + 128])
+        rest[:, 256 + h * vd : 256 + (h + 1) * vd] = mms(pack[:, WTS + at : WTS + at + 128].T, grad)
     qg[...] = jnp.stack(parts, axis=1).astype(BF)
 
 
@@ -389,16 +405,16 @@
 def final_body(q, state, vv, pack, rest, kg, vg):
     heads, vd, kd = 2, 256, 128
     keys, values = [], []
-    st = state[...].astype(F32)
+    st = state[...]
     c, s = pack[:, COS : COS + 128], pack[:, SIN : SIN + 128]
     for h in range(heads):
         at = h * 128
         fut = joined(st, h, vd)
         left = pack[:, SCAL + 2 + h : SCAL + 3 + h]
-        kt = rest[:, at : at + 128] + left * mmh(vv[h].astype(F32), fut, NT)
+        kt = rest[:, at : at + 128] + left * mms(vv[h], fut, NT)
         keys.append(turned(kt, c, -s) * (kd**-0.5))
         vt = rest[:, 256 + h * vd : 256 + (h + 1) * vd]
-        values.append(vt + left * mmh(pack[:, KR + at : KR + at + 128], fut))
+        values.append(vt + left * mms(pack[:, KR + at : KR + at + 128], fut))
     kg[...] = jnp.stack(keys, axis=1).astype(BF)
     vg[...] = jnp.stack(values, axis=1).astype(BF)
 

time: 244 us -> 243 us (level)
  no operation moved by 1% of the time
where the time goes in v6:
time: 243 us; the launch traced here: 242 us
  waiting for transfers between devices  62.8 us (26%)
  starting transfers between devices  62.7 us (26%)
  blocking collectives  61.9 us (25%)
  Pallas kernels  46.9 us (19%)
  local copies, waits for them, and re-layouts  4.92 us (2%)
    all_to_all x2, blocking collectives, a2a(): return lax.all_to_all(x, axes, split_axis=0, concat_axis=0, tiled=True)  61.9 us
    pallas_call x17, Pallas kernels, call(): pl.pallas_call(kernel, out_shape=[(pltpu.HBM if i in hbm_out else jax.Sha...  46.9 us
    all_to_all x5, starting transfers between devices, a2a(): return lax.all_to_all(x, axes, split_axis=0, concat_axis=0, tiled=True)  35.6 us
    ppermute x15, waiting for transfers between devices, shift(): return lax.ppermute(x, TP, [(i, (i + by) % 4) for i in range(4)])  33.8 us
    all_to_all x5, waiting for transfers between devices, a2a(): return lax.all_to_all(x, axes, split_axis=0, concat_axis=0, tiled=True)  19.8 us
    ppermute x15, starting transfers between devices, shift(): return lax.ppermute(x, TP, [(i, (i + by) % 4) for i in range(4)])  18.3 us
    ppermute x3, waiting for transfers between devices, per_device(): lax.ppermute(nbf, 'sp_1', [(i, (i + by) % 4) for i in range(4)])  8.26 us
    ppermute x4, starting transfers between devices, per_device(): nball = along + [lax.ppermute(a, 'sp_2', [(0, 1), (1, 0)]) for a in along]  5.07 us
  transfers between devices with their start and end apart: 27, of which 12 were waited for; matrix products, arithmetic and copies ran while one was open for 2% of the time, Pallas kernels for 13%

profile of v6, /device:TPU:1, one launch (start us, length us, event | category | flops | bytes accessed | tf_op | source)
XLA Modules:
  0.0 241.8 jit_solution(5159023236836045351)
XLA Ops:
  1.3 3.2 %shard_map.171 = bf16[64,16,512]{2,1,0:T(8,128)(2,1)} custom-call(s32[4]{0:T(128)} %pad_add_fusion.q_ref, s32[2,128]{1,0:T(2,128)} %bitcast.52, f32[2,128]{1,0:T(2,128)} %bitcast.55, bf16[128,2048]{1,0:T(8,128)(2,1)} %refs_2_.2, bf16[128,2048]{1,0:T(8,128)(2,1)} %refs_2_.3), custom_call_target="tpu_custom_call" | custom-call | tf_op jit(solution)/shard_map/pallas_call | solution.py:72
  4.5 41.6 %all_to_all.35 = bf16[64,16,512]{2,1,0:T(8,128)(2,1)S(1)} all-to-all(bf16[64,16,512]{2,1,0:T(8,128)(2,1)} %shard_map.171), channel_id=1, replica_groups=mesh['sp_0'=8,'sp_1'=4,'sp_2'=2,'tp'=4] {'sp_0','sp_1','sp_2'}, dimensions={0} | all-to-all | bytes 2097152 | tf_op jit(solution)/shard_map/all_to_all | solution.py:423
  46.1 1.1 slice_bitcast_fusion
  47.2 1.2 collective-permute-start.1
  48.4 1.5 collective-permute-start.3
  49.9 1.3 collective-permute-start
  51.4 9.7 %collective-permute-done.1.refs_2_.refs_3_ = bf16[512,512]{1,0:T(8,128)(2,1)} collective-permute-done((bf16[512,512]{1,0:T(8,128)(2,1)}, bf16[512,512]{1,0:T(8,128)(2,1)}, u32[]{:S(2)}, u32[]{:S(2)}) %collective-permute-start.1) | collective-permute-done | bytes 524320 | tf_op jit(solution)/shard_map/ppermute | solution.py:427
  61.1 2.7 %collective-permute-start.4 = (bf16[512,512]{1,0:T(8,128)(2,1)}, bf16[512,512]{1,0:T(8,128)(2,1)}, u32[]{:S(2)}, u32[]{:S(2)}) collective-permute-start(bf16[512,512]{1,0:T(8,128)(2,1)} %collective-permute-done.3.refs_4_.refs_5_), channel_id=1, source_target_pairs={{0,3},{1,0},{2,1},{3,2},{4,7},{5,4},{6,5},{7,6},{8,11},{9,8},{10,9... | collective-permute-start | bytes 1572872 | tf_op jit(solution)/shard_map/ppermute | solution.py:427
  65.7 6.3 %collective-permute-done.refs_1_ = bf16[512,512]{1,0:T(8,128)(2,1)} collective-permute-done((bf16[512,512]{1,0:T(8,128)(2,1)}, bf16[512,512]{1,0:T(8,128)(2,1)}, u32[]{:S(2)}, u32[]{:S(2)}) %collective-permute-start) | collective-permute-done | bytes 524320 | tf_op jit(solution)/shard_map/ppermute | solution.py:427
  72.3 3.8 %shard_map.172 = (f32[512,256]{1,0:T(8,128)S(1)}, f32[512,256]{1,0:T(8,128)S(1)}, f32[512,256]{1,0:T(8,128)S(1)}) custom-call(s32[4]{0:T(128)S(1)} %copy-done.10, bf16[512,512]{1,0:T(8,128)(2,1)} %get-tuple-element.78.refs_0_, bf16[512,512]{1,0:T(8,128)(2,1)} %collective-permute-done.refs_1_, bf16[512,512]{1,0:T(8,128)(2,1)} %collective-permute-done.1.refs_2_.refs_3_, ...), custom_call_target="tpu_custom_call" | custom-call | tf_op jit(solution)/shard_map/pallas_call | solution.py:72
  76.1 7.4 %collective-permute-done.2.refs_0_.refs_2_ = bf16[512,512]{1,0:T(8,128)(2,1)} collective-permute-done((bf16[512,512]{1,0:T(8,128)(2,1)}, bf16[512,512]{1,0:T(8,128)(2,1)}, u32[]{:S(2)}, u32[]{:S(2)}) %collective-permute-start.2) | collective-permute-done | bytes 524320 | tf_op jit(solution)/shard_map/ppermute | solution.py:427
  83.6 4.0 %shard_map.173 = (bf16[512,256]{1,0:T(8,128)(2,1)}, bf16[512,256]{1,0:T(8,128)(2,1)}, bf16[512,256]{1,0:T(8,128)(2,1)}, bf16[256,512]{1,0:T(8,128)(2,1)}, bf16[256,512]{1,0:T(8,128)(2,1)}) custom-call(s32[4]{0:T(128)S(1)} %copy-done.10, bf16[512,512]{1,0:T(8,128)(2,1)} %collective-permute-done.2.refs_0_.refs_2_, ...), custom_call_target="tpu_custom_call" | custom-call | tf_op jit(solution)/shard_map/pallas_call | solution.py:72
  88.5 1.7 collective-permute-start.7
  92.5 3.7 %shard_map.180 = (bf16[64,16,128]{2,1,0:T(8,128)(2,1)}, f32[128,1920]{1,0:T(8,128)}) custom-call(s32[4]{0:T(128)} %pad_add_fusion.q_ref, bf16[2,128,128]{2,1,0:T(8,128)(2,1)} %get-tuple-element.82.refs_0_, bf16[2,128,128]{2,1,0:T(8,128)(2,1)} %get-tuple-element.81.refs_1_, bf16[2,128,256]{2,1,0:T(8,128)(2,1)} %bitcast.46, f32[2,128]{1,0:T(2,128)} %bitcast.56, ...), custom_call_target="tpu_custom_call" | custom-call | tf_op jit(solution)/shard_map/pallas_call | solution.py:72
  96.2 7.9 %all-to-all-start.2 = ((bf16[64,16,128]{2,1,0:T(8,128)(2,1)}), bf16[64,16,128]{2,1,0:T(8,128)(2,1)S(1)}, u32[]{:S(2)}, u32[]{:S(2)}) async-start(bf16[64,16,128]{2,1,0:T(8,128)(2,1)} %get-tuple-element.59), calls=%async_computation.2 | async-start | bytes 524288 | tf_op jit(solution)/shard_map/all_to_all | solution.py:423
  104.2 3.4 %shard_map.175 = (bf16[256,512]{1,0:T(8,128)(2,1)}, bf16[256,512]{1,0:T(8,128)(2,1)}, bf16[256,512]{1,0:T(8,128)(2,1)}, bf16[256,512]{1,0:T(8,128)(2,1)}, bf16[512,512]{1,0:T(8,128)(2,1)}) custom-call(s32[4]{0:T(128)S(1)} %copy-done.11, bf16[512,256]{1,0:T(8,128)(2,1)} %get-tuple-element.44.refs_8_.refs_0_, ...), custom_call_target="tpu_custom_call" | custom-call | tf_op jit(solution)/shard_map/pallas_call | solution.py:72
  107.5 2.7 %collective-permute-start.10 = (bf16[256,512]{1,0:T(8,128)(2,1)}, bf16[256,512]{1,0:T(8,128)(2,1)S(1)}, u32[]{:S(2)}, u32[]{:S(2)}) collective-permute-start(bf16[256,512]{1,0:T(8,128)(2,1)} %get-tuple-element.57), channel_id=1, source_target_pairs={{0,3},{1,0},{2,1},{3,2},{4,7},{5,4},{6,5},{7,6},{8,11},{9,8},{10,9... | collective-permute-start | bytes 786440 | tf_op jit(solution)/shard_map/ppermute | solution.py:427
  110.2 1.7 shard_map.176
  112.0 2.7 %collective-permute-start.11 = (bf16[256,512]{1,0:T(8,128)(2,1)S(1)}, bf16[256,512]{1,0:T(8,128)(2,1)S(1)}, u32[]{:S(2)}, u32[]{:S(2)}) collective-permute-start(bf16[256,512]{1,0:T(8,128)(2,1)S(1)} %get-tuple-element.58), channel_id=1, source_target_pairs={{0,3},{1,0},{2,1},{3,2},{4,7},{5,4},{6,5},{7,6},{8,11},{9,8},{10,9... | collective-permute-start | bytes 786440 | tf_op jit(solution)/shard_map/ppermute | solution.py:427
  114.7 1.7 collective-permute-done.9.refs_2_
  116.4 5.6 %collective-permute-done.8.refs_1_ = bf16[256,512]{1,0:T(8,128)(2,1)S(1)} collective-permute-done((bf16[256,512]{1,0:T(8,128)(2,1)S(1)}, bf16[256,512]{1,0:T(8,128)(2,1)S(1)}, u32[]{:S(2)}, u32[]{:S(2)}) %collective-permute-start.8) | collective-permute-done | bytes 262176 | tf_op jit(solution)/shard_map/ppermute | solution.py:427
  122.0 2.6 %shard_map.177 = bf16[512,512]{1,0:T(8,128)(2,1)} custom-call(s32[4]{0:T(128)S(1)} %copy-done.11, bf16[512,512]{1,0:T(8,128)(2,1)} %get-tuple-element.50.refs_0_, bf16[256,512]{1,0:T(8,128)(2,1)S(1)} %collective-permute-done.8.refs_1_, bf16[256,512]{1,0:T(8,128)(2,1)S(1)} %collective-permute-done.9.refs_2_, ...), custom_call_target="tpu_custom_call" | custom-call | tf_op jit(solution)/shard_map/pallas_call | solution.py:72
  124.6 11.7 %all-to-all-start.1 = ((bf16[64,8,512]{2,1,0:T(8,128)(2,1)}), bf16[64,8,512]{2,1,0:T(8,128)(2,1)}, u32[]{:S(2)}, u32[]{:S(2)}) async-start(bf16[64,8,512]{2,1,0:T(8,128)(2,1)} %bitcast.54), calls=%async_computation.1 | async-start | bytes 1048576 | tf_op jit(solution)/shard_map/all_to_all | solution.py:423
  136.3 2.0 shard_map.181
  138.3 15.6 %all-to-all-done.1 = bf16[64,8,512]{2,1,0:T(8,128)(2,1)} async-done(((bf16[64,8,512]{2,1,0:T(8,128)(2,1)}), bf16[64,8,512]{2,1,0:T(8,128)(2,1)}, u32[]{:S(2)}, u32[]{:S(2)}) %all-to-all-start.1) | async-done | bytes 524320 | tf_op jit(solution)/shard_map/all_to_all | solution.py:423
  153.9 5.7 %all-to-all-start.3 = ((bf16[64,8,128]{2,1,0:T(8,128)(2,1)}), bf16[64,8,128]{2,1,0:T(8,128)(2,1)S(1)}, u32[]{:S(2)}, u32[]{:S(2)}) async-start(bf16[64,8,128]{2,1,0:T(8,128)(2,1)} %get-tuple-element.60), calls=%async_computation.3 | async-start | bytes 262144 | tf_op jit(solution)/shard_map/all_to_all | solution.py:423
  159.6 1.5 shard_map.178.refs_1_
  161.1 2.0 shard_map.179.refs_0_
  163.1 2.8 %collective-permute-start.12 = (bf16[128,512]{1,0:T(8,128)(2,1)S(1)}, bf16[128,512]{1,0:T(8,128)(2,1)S(1)}, u32[]{:S(2)}, u32[]{:S(2)}) collective-permute-start(bf16[128,512]{1,0:T(8,128)(2,1)S(1)} %shard_map.179.refs_0_), channel_id=1, source_target_pairs={{0,3},{1,0},{2,1},{3,2},{4,7},{5,4},{6,5},{7,6},{8,11},{9,8},{10,9... | collective-permute-start | bytes 393224 | tf_op jit(solution)/shard_map/ppermute | solution.py:427
  166.5 4.2 %all-to-all-done.3 = bf16[64,8,128]{2,1,0:T(8,128)(2,1)S(1)} async-done(((bf16[64,8,128]{2,1,0:T(8,128)(2,1)}), bf16[64,8,128]{2,1,0:T(8,128)(2,1)S(1)}, u32[]{:S(2)}, u32[]{:S(2)}) %all-to-all-start.3) | async-done | bytes 131104 | tf_op jit(solution)/shard_map/all_to_all | solution.py:423
  170.7 1.7 shard_map.182
  172.4 2.7 %collective-permute-done.14.refs_3_ = bf16[128,512]{1,0:T(8,128)(2,1)} collective-permute-done((bf16[128,512]{1,0:T(8,128)(2,1)S(1)}, bf16[128,512]{1,0:T(8,128)(2,1)}, u32[]{:S(2)}, u32[]{:S(2)}) %collective-permute-start.14) | collective-permute-done | bytes 131104 | tf_op jit(solution)/shard_map/ppermute | solution.py:427
  175.1 3.4 %shard_map.183 = (f32[128,512]{1,0:T(8,128)}, bf16[8,320,128]{2,1,0:T(8,128)(2,1)}) custom-call(s32[4]{0:T(128)S(1)} %copy-done.11, bf16[128,512]{1,0:T(8,128)(2,1)S(1)} %shard_map.179.refs_0_, bf16[128,512]{1,0:T(8,128)(2,1)S(1)} %collective-permute-done.12.refs_1_, bf16[128,512]{1,0:T(8,128)(2,1)} %collective-permute-done.13.refs_2_, ...), custom_call_target="tpu_custom_call" | custom-call | tf_op jit(solution)/shard_map/pallas_call | solution.py:72
  178.5 5.3 %all-to-all-start.4 = ((bf16[8,320,128]{2,1,0:T(8,128)(2,1)}), bf16[8,320,128]{2,1,0:T(8,128)(2,1)S(1)}, u32[]{:S(2)}, u32[]{:S(2)}) async-start(bf16[8,320,128]{2,1,0:T(8,128)(2,1)} %get-tuple-element.63), calls=%async_computation.4 | async-start | bytes 1310720 | tf_op jit(solution)/shard_map/all_to_all | solution.py:423
  183.8 2.6 %collective-permute-start.15 = (bf16[128,512]{1,0:T(8,128)(2,1)}, bf16[128,512]{1,0:T(8,128)(2,1)S(1)}, u32[]{:S(2)}, u32[]{:S(2)}) collective-permute-start(bf16[128,512]{1,0:T(8,128)(2,1)} %get-tuple-element.64.refs_1_), channel_id=1, source_target_pairs={{0,24},{8,0},{16,8},{24,16},{1,25},{9,1},{17,9},{25,17},{2,26},{10... | collective-permute-start | bytes 393224 | tf_op jit(solution)/shard_map/ppermute | solution.py:507
  187.5 1.2 collective-permute-start.18
  188.7 7.1 %collective-permute-done.15.refs_2_ = bf16[128,512]{1,0:T(8,128)(2,1)S(1)} collective-permute-done((bf16[128,512]{1,0:T(8,128)(2,1)}, bf16[128,512]{1,0:T(8,128)(2,1)S(1)}, u32[]{:S(2)}, u32[]{:S(2)}) %collective-permute-start.15) | collective-permute-done | bytes 131104 | tf_op jit(solution)/shard_map/ppermute | solution.py:507
  195.9 1.5 collective-permute-start.19
  197.4 1.5 collective-permute-start.20
  198.9 1.1 collective-permute-done.17.refs_4_
  200.9 0.9 collective-permute-done.21.refs_8_
  202.5 2.5 %shard_map.184 = (f32[8,64,128]{2,1,0:T(8,128)S(1)}, bf16[8,192,128]{2,1,0:T(8,128)(2,1)S(1)}) custom-call(s32[4]{0:T(128)S(1)} %copy-done.11, bf16[8,320,128]{2,1,0:T(8,128)(2,1)S(1)} %all-to-all-done.4.refs_0_, bf16[128,512]{1,0:T(8,128)(2,1)} %get-tuple-element.64.refs_1_, bf16[128,512]{1,0:T(8,128)(2,1)} %copy-done.13, bf16[128,512]{1,0:T(8,128)(2,1)} %copy-done.14, ...), custom_call_target="tpu_custom_call" | custom-call | tf_op jit(solution)/shard_map/pallas_call | solution.py:72
  205.0 20.3 %all_to_all.36.refs_0_ = bf16[8,192,128]{2,1,0:T(8,128)(2,1)S(1)} all-to-all(bf16[8,192,128]{2,1,0:T(8,128)(2,1)S(1)} %get-tuple-element.66), channel_id=1, replica_groups=mesh['sp_0'=8,'sp_1'=4,'sp_2'=2,'tp'=4] {'sp_0'}, dimensions={0} | all-to-all | bytes 786432 | tf_op jit(solution)/shard_map/all_to_all | solution.py:423
  225.3 1.3 shard_map.185
  226.6 4.9 %all-to-all-start.6 = ((bf16[8,64,128]{2,1,0:T(8,128)(2,1)}), bf16[8,64,128]{2,1,0:T(8,128)(2,1)S(1)}, u32[]{:S(2)}, u32[]{:S(2)}) async-start(bf16[8,64,128]{2,1,0:T(8,128)(2,1)} %get-tuple-element.71), calls=%async_computation.6 | async-start | bytes 262144 | tf_op jit(solution)/shard_map/all_to_all | solution.py:423
  231.6 6.4 %shard_map.174 = (bf16[2048,256]{1,0:T(8,128)(2,1)}, bf16[2048,256]{1,0:T(8,128)(2,1)}, bf16[256,2048]{1,0:T(8,128)(2,1)}) custom-call(s32[4]{0:T(128)S(1)} %copy-done.11, bf16[512,512]{1,0:T(8,128)(2,1)} %get-tuple-element.78.refs_0_, bf16[512,512]{1,0:T(8,128)(2,1)} %collective-permute-done.refs_1_, ...), custom_call_target="tpu_custom_call" | custom-call | tf_op jit(solution)/shard_map/pallas_call | solution.py:72
  238.0 2.0 shard_map.186
  240.1 1.8 shard_map.187
  (85 shorter events, 9.7 us)
Async XLA Ops:
  4.5 60.5 %copy-start.21 = (bf16[128,2,128]{2,1,0:T(2,128)(2,1)S(1)}, bf16[128,2,128]{2,1,0:T(2,128)(2,1)}, u32[]{:S(2)}) copy-start(bf16[128,2,128]{2,1,0:T(2,128)(2,1)} %param.17) | copy-start | bytes 196612
  4.5 60.5 %copy-start.22 = (bf16[128,2,128]{2,1,0:T(2,128)(2,1)S(1)}, bf16[128,2,128]{2,1,0:T(2,128)(2,1)}, u32[]{:S(2)}) copy-start(bf16[128,2,128]{2,1,0:T(2,128)(2,1)} %param.16) | copy-start | bytes 196612
  4.5 67.8 %copy-start = (bf16[1,2048,256]{2,1,0:T(8,128)(2,1)S(1)}, bf16[1,2048,256]{2,1,0:T(8,128)(2,1)}, u32[]{:S(2)}) copy-start(bf16[1,2048,256]{2,1,0:T(8,128)(2,1)} %param.21) | copy-start | bytes 3145732
  4.5 67.8 %copy-start.1 = (bf16[1,2048,256]{2,1,0:T(8,128)(2,1)S(1)}, bf16[1,2048,256]{2,1,0:T(8,128)(2,1)}, u32[]{:S(2)}) copy-start(bf16[1,2048,256]{2,1,0:T(8,128)(2,1)} %param.22) | copy-start | bytes 3145732
  4.5 67.8 %copy-start.3 = (bf16[1,256,2048]{2,1,0:T(8,128)(2,1)S(1)}, bf16[1,256,2048]{2,1,0:T(8,128)(2,1)}, u32[]{:S(2)}) copy-start(bf16[1,256,2048]{2,1,0:T(8,128)(2,1)} %param.23) | copy-start | bytes 3145732
  4.5 67.8 %copy-start.10 = (s32[4]{0:T(128)S(1)}, s32[4]{0:T(128)}, u32[]{:S(2)}) copy-start(s32[4]{0:T(128)} %pad_add_fusion.q_ref) | copy-start | bytes 52
  47.2 13.9 %collective-permute-start.1 = (bf16[512,512]{1,0:T(8,128)(2,1)}, bf16[512,512]{1,0:T(8,128)(2,1)}, u32[]{:S(2)}, u32[]{:S(2)}) collective-permute-start(bf16[512,512]{1,0:T(8,128)(2,1)} %get-tuple-element.78.refs_0_), channel_id=1, source_target_pairs={{0,1},{1,2},{2,3},{3,0},{4,5},{5,6},{6,7},{7,4},{8,9},{9,10},{10,1... | collective-permute-start | bytes 1572872 | tf_op jit(solution)/shard_map/ppermute | solution.py:427
  48.4 12.7 %collective-permute-start.3 = (bf16[512,512]{1,0:T(8,128)(2,1)}, bf16[512,512]{1,0:T(8,128)(2,1)}, u32[]{:S(2)}, u32[]{:S(2)}) collective-permute-start(bf16[512,512]{1,0:T(8,128)(2,1)} %get-tuple-element.77.refs_3_.refs_4_), channel_id=1, source_target_pairs={{0,3},{1,0},{2,1},{3,2},{4,7},{5,4},{6,5},{7,6},{8,11},{9,8},{10,9... | collective-permute-start | bytes 1572872 | tf_op jit(solution)/shard_map/ppermute | solution.py:427
  49.9 22.1 %collective-permute-start = (bf16[512,512]{1,0:T(8,128)(2,1)}, bf16[512,512]{1,0:T(8,128)(2,1)}, u32[]{:S(2)}, u32[]{:S(2)}) collective-permute-start(bf16[512,512]{1,0:T(8,128)(2,1)} %get-tuple-element.78.refs_0_), channel_id=1, source_target_pairs={{0,3},{1,0},{2,1},{3,2},{4,7},{5,4},{6,5},{7,6},{8,11},{9,8},{10,9... | collective-permute-start | bytes 1572872 | tf_op jit(solution)/shard_map/ppermute | solution.py:427
  51.2 21.1 %collective-permute-start.5 = (bf16[512,512]{1,0:T(8,128)(2,1)}, bf16[512,512]{1,0:T(8,128)(2,1)}, u32[]{:S(2)}, u32[]{:S(2)}) collective-permute-start(bf16[512,512]{1,0:T(8,128)(2,1)} %get-tuple-element.77.refs_3_.refs_4_), channel_id=1, source_target_pairs={{0,1},{1,2},{2,3},{3,0},{4,5},{5,6},{6,7},{7,4},{8,9},{9,10},{10,1... | collective-permute-start | bytes 1572872 | tf_op jit(solution)/shard_map/ppermute | solution.py:427
  61.1 22.5 %collective-permute-start.2 = (bf16[512,512]{1,0:T(8,128)(2,1)}, bf16[512,512]{1,0:T(8,128)(2,1)}, u32[]{:S(2)}, u32[]{:S(2)}) collective-permute-start(bf16[512,512]{1,0:T(8,128)(2,1)} %collective-permute-done.1.refs_2_.refs_3_), channel_id=1, source_target_pairs={{0,1},{1,2},{2,3},{3,0},{4,5},{5,6},{6,7},{7,4},{8,9},{9,10},{10,1... | collective-permute-start | bytes 1572872 | tf_op jit(solution)/shard_map/ppermute | solution.py:427
  61.1 22.5 %collective-permute-start.4 = (bf16[512,512]{1,0:T(8,128)(2,1)}, bf16[512,512]{1,0:T(8,128)(2,1)}, u32[]{:S(2)}, u32[]{:S(2)}) collective-permute-start(bf16[512,512]{1,0:T(8,128)(2,1)} %collective-permute-done.3.refs_4_.refs_5_), channel_id=1, source_target_pairs={{0,3},{1,0},{2,1},{3,2},{4,7},{5,4},{6,5},{7,6},{8,11},{9,8},{10,9... | collective-permute-start | bytes 1572872 | tf_op jit(solution)/shard_map/ppermute | solution.py:427
  83.6 6.7 %copy-start.20 = (bf16[128,2,256]{2,1,0:T(2,128)(2,1)S(1)}, bf16[128,2,256]{2,1,0:T(2,128)(2,1)}, u32[]{:S(2)}) copy-start(bf16[128,2,256]{2,1,0:T(2,128)(2,1)} %param.18) | copy-start | bytes 393220
  83.6 20.6 %copy-start.11 = (s32[4]{0:T(128)S(1)}, s32[4]{0:T(128)}, u32[]{:S(2)}) copy-start(s32[4]{0:T(128)} %pad_add_fusion.q_ref) | copy-start | bytes 52
  87.6 22.7 %collective-permute-start.6 = (bf16[256,512]{1,0:T(8,128)(2,1)}, bf16[256,512]{1,0:T(8,128)(2,1)S(1)}, u32[]{:S(2)}, u32[]{:S(2)}) collective-permute-start(bf16[256,512]{1,0:T(8,128)(2,1)} %get-tuple-element.52), channel_id=1, source_target_pairs={{0,1},{1,2},{2,3},{3,0},{4,5},{5,6},{6,7},{7,4},{8,9},{9,10},{10,1... | collective-permute-start | bytes 786440 | tf_op jit(solution)/shard_map/ppermute | solution.py:427
  88.5 21.7 %collective-permute-start.7 = (bf16[256,512]{1,0:T(8,128)(2,1)}, bf16[256,512]{1,0:T(8,128)(2,1)S(1)}, u32[]{:S(2)}, u32[]{:S(2)}) collective-permute-start(bf16[256,512]{1,0:T(8,128)(2,1)} %get-tuple-element.54), channel_id=1, source_target_pairs={{0,3},{1,0},{2,1},{3,2},{4,7},{5,4},{6,5},{7,6},{8,11},{9,8},{10,9... | collective-permute-start | bytes 786440 | tf_op jit(solution)/shard_map/ppermute | solution.py:427
  96.2 28.4 %all-to-all-start.2 = ((bf16[64,16,128]{2,1,0:T(8,128)(2,1)}), bf16[64,16,128]{2,1,0:T(8,128)(2,1)S(1)}, u32[]{:S(2)}, u32[]{:S(2)}) async-start(bf16[64,16,128]{2,1,0:T(8,128)(2,1)} %get-tuple-element.59), calls=%async_computation.2 | async-start | bytes 524288 | tf_op jit(solution)/shard_map/all_to_all | solution.py:423
  107.5 8.8 %collective-permute-start.9 = (bf16[256,512]{1,0:T(8,128)(2,1)}, bf16[256,512]{1,0:T(8,128)(2,1)S(1)}, u32[]{:S(2)}, u32[]{:S(2)}) collective-permute-start(bf16[256,512]{1,0:T(8,128)(2,1)} %get-tuple-element.56), channel_id=1, source_target_pairs={{0,1},{1,2},{2,3},{3,0},{4,5},{5,6},{6,7},{7,4},{8,9},{9,10},{10,1... | collective-permute-start | bytes 786440 | tf_op jit(solution)/shard_map/ppermute | solution.py:427
  107.5 8.8 %collective-permute-start.10 = (bf16[256,512]{1,0:T(8,128)(2,1)}, bf16[256,512]{1,0:T(8,128)(2,1)S(1)}, u32[]{:S(2)}, u32[]{:S(2)}) collective-permute-start(bf16[256,512]{1,0:T(8,128)(2,1)} %get-tuple-element.57), channel_id=1, source_target_pairs={{0,3},{1,0},{2,1},{3,2},{4,7},{5,4},{6,5},{7,6},{8,11},{9,8},{10,9... | collective-permute-start | bytes 786440 | tf_op jit(solution)/shard_map/ppermute | solution.py:427
  111.9 47.7 %copy-start.12 = (s32[128,2]{0,1:T(2,128)S(1)}, s32[128,2]{0,1:T(2,128)}, u32[]{:S(2)}) copy-start(s32[128,2]{0,1:T(2,128)} %param.14) | copy-start | bytes 3076
  111.9 10.1 %collective-permute-start.8 = (bf16[256,512]{1,0:T(8,128)(2,1)S(1)}, bf16[256,512]{1,0:T(8,128)(2,1)S(1)}, u32[]{:S(2)}, u32[]{:S(2)}) collective-permute-start(bf16[256,512]{1,0:T(8,128)(2,1)S(1)} %get-tuple-element.55), channel_id=1, source_target_pairs={{0,1},{1,2},{2,3},{3,0},{4,5},{5,6},{6,7},{7,4},{8,9},{9,10},{10,1... | collective-permute-start | bytes 786440 | tf_op jit(solution)/shard_map/ppermute | solution.py:427
  112.0 10.0 %collective-permute-start.11 = (bf16[256,512]{1,0:T(8,128)(2,1)S(1)}, bf16[256,512]{1,0:T(8,128)(2,1)S(1)}, u32[]{:S(2)}, u32[]{:S(2)}) collective-permute-start(bf16[256,512]{1,0:T(8,128)(2,1)S(1)} %get-tuple-element.58), channel_id=1, source_target_pairs={{0,3},{1,0},{2,1},{3,2},{4,7},{5,4},{6,5},{7,6},{8,11},{9,8},{10,9... | collective-permute-start | bytes 786440 | tf_op jit(solution)/shard_map/ppermute | solution.py:427
  124.6 46.1 %copy-start.4 = (f32[128,1920]{1,0:T(8,128)S(1)}, f32[128,1920]{1,0:T(8,128)}, u32[]{:S(2)}) copy-start(f32[128,1920]{1,0:T(8,128)} %get-tuple-element.61.refs_1_.refs_2_) | copy-start | bytes 2949124
  124.6 50.5 %copy-start.2 = (bf16[2048,512]{1,0:T(8,128)(2,1)S(1)}, bf16[2048,512]{1,0:T(8,128)(2,1)}, u32[]{:S(2)}) copy-start(bf16[2048,512]{1,0:T(8,128)(2,1)} %refs_7_.1) | copy-start | bytes 6291460
  124.6 29.3 %all-to-all-start.1 = ((bf16[64,8,512]{2,1,0:T(8,128)(2,1)}), bf16[64,8,512]{2,1,0:T(8,128)(2,1)}, u32[]{:S(2)}, u32[]{:S(2)}) async-start(bf16[64,8,512]{2,1,0:T(8,128)(2,1)} %bitcast.54), calls=%async_computation.1 | async-start | bytes 1048576 | tf_op jit(solution)/shard_map/all_to_all | solution.py:423
  153.9 16.8 %all-to-all-start.3 = ((bf16[64,8,128]{2,1,0:T(8,128)(2,1)}), bf16[64,8,128]{2,1,0:T(8,128)(2,1)S(1)}, u32[]{:S(2)}, u32[]{:S(2)}) async-start(bf16[64,8,128]{2,1,0:T(8,128)(2,1)} %get-tuple-element.60), calls=%async_computation.3 | async-start | bytes 262144 | tf_op jit(solution)/shard_map/all_to_all | solution.py:423
  163.1 9.3 %collective-permute-start.12 = (bf16[128,512]{1,0:T(8,128)(2,1)S(1)}, bf16[128,512]{1,0:T(8,128)(2,1)S(1)}, u32[]{:S(2)}, u32[]{:S(2)}) collective-permute-start(bf16[128,512]{1,0:T(8,128)(2,1)S(1)} %shard_map.179.refs_0_), channel_id=1, source_target_pairs={{0,3},{1,0},{2,1},{3,2},{4,7},{5,4},{6,5},{7,6},{8,11},{9,8},{10,9... | collective-permute-start | bytes 393224 | tf_op jit(solution)/shard_map/ppermute | solution.py:427
  165.8 6.5 %collective-permute-start.13 = (bf16[128,512]{1,0:T(8,128)(2,1)S(1)}, bf16[128,512]{1,0:T(8,128)(2,1)}, u32[]{:S(2)}, u32[]{:S(2)}) collective-permute-start(bf16[128,512]{1,0:T(8,128)(2,1)S(1)} %shard_map.179.refs_0_), channel_id=1, source_target_pairs={{0,2},{1,3},{2,0},{3,1},{4,6},{5,7},{6,4},{7,5},{8,10},{9,11},{10,... | collective-permute-start | bytes 393224 | tf_op jit(solution)/shard_map/ppermute | solution.py:427
  165.8 9.3 %collective-permute-start.14 = (bf16[128,512]{1,0:T(8,128)(2,1)S(1)}, bf16[128,512]{1,0:T(8,128)(2,1)}, u32[]{:S(2)}, u32[]{:S(2)}) collective-permute-start(bf16[128,512]{1,0:T(8,128)(2,1)S(1)} %shard_map.179.refs_0_), channel_id=1, source_target_pairs={{0,1},{1,2},{2,3},{3,0},{4,5},{5,6},{6,7},{7,4},{8,9},{9,10},{10,1... | collective-permute-start | bytes 393224 | tf_op jit(solution)/shard_map/ppermute | solution.py:427
  178.4 53.1 %copy-start.6 = (bf16[512,256]{1,0:T(8,128)(2,1)S(1)}, bf16[512,256]{1,0:T(8,128)(2,1)}, u32[]{:S(2)}) copy-start(bf16[512,256]{1,0:T(8,128)(2,1)} %get-tuple-element.44.refs_8_.refs_0_) | copy-start | bytes 786436
  178.5 53.1 %copy-start.7 = (bf16[512,256]{1,0:T(8,128)(2,1)S(1)}, bf16[512,256]{1,0:T(8,128)(2,1)}, u32[]{:S(2)}) copy-start(bf16[512,256]{1,0:T(8,128)(2,1)} %get-tuple-element.45.refs_9_.refs_1_) | copy-start | bytes 786436
  178.5 53.1 %copy-start.8 = (bf16[512,256]{1,0:T(8,128)(2,1)S(1)}, bf16[512,256]{1,0:T(8,128)(2,1)}, u32[]{:S(2)}) copy-start(bf16[512,256]{1,0:T(8,128)(2,1)} %get-tuple-element.46.refs_10_) | copy-start | bytes 786436
  178.5 23.4 %all-to-all-start.4 = ((bf16[8,320,128]{2,1,0:T(8,128)(2,1)}), bf16[8,320,128]{2,1,0:T(8,128)(2,1)S(1)}, u32[]{:S(2)}, u32[]{:S(2)}) async-start(bf16[8,320,128]{2,1,0:T(8,128)(2,1)} %get-tuple-element.63), calls=%async_computation.4 | async-start | bytes 1310720 | tf_op jit(solution)/shard_map/all_to_all | solution.py:423
  183.8 12.1 %collective-permute-start.15 = (bf16[128,512]{1,0:T(8,128)(2,1)}, bf16[128,512]{1,0:T(8,128)(2,1)S(1)}, u32[]{:S(2)}, u32[]{:S(2)}) collective-permute-start(bf16[128,512]{1,0:T(8,128)(2,1)} %get-tuple-element.64.refs_1_), channel_id=1, source_target_pairs={{0,24},{8,0},{16,8},{24,16},{1,25},{9,1},{17,9},{25,17},{2,26},{10... | collective-permute-start | bytes 393224 | tf_op jit(solution)/shard_map/ppermute | solution.py:507
  186.3 11.1 %collective-permute-start.16 = (bf16[128,512]{1,0:T(8,128)(2,1)}, bf16[128,512]{1,0:T(8,128)(2,1)S(1)}, u32[]{:S(2)}, u32[]{:S(2)}) collective-permute-start(bf16[128,512]{1,0:T(8,128)(2,1)} %get-tuple-element.64.refs_1_), channel_id=1, source_target_pairs={{0,16},{8,24},{16,0},{24,8},{1,17},{9,25},{17,1},{25,9},{2,18},{10... | collective-permute-start | bytes 393224 | tf_op jit(solution)/shard_map/ppermute | solution.py:507
  186.9 13.1 %collective-permute-start.17 = (bf16[128,512]{1,0:T(8,128)(2,1)}, bf16[128,512]{1,0:T(8,128)(2,1)S(1)}, u32[]{:S(2)}, u32[]{:S(2)}) collective-permute-start(bf16[128,512]{1,0:T(8,128)(2,1)} %get-tuple-element.64.refs_1_), channel_id=1, source_target_pairs={{0,8},{8,16},{16,24},{24,0},{1,9},{9,17},{17,25},{25,1},{2,10},{10... | collective-permute-start | bytes 393224 | tf_op jit(solution)/shard_map/ppermute | solution.py:507
  187.5 13.3 %collective-permute-start.18 = (bf16[128,512]{1,0:T(8,128)(2,1)}, bf16[128,512]{1,0:T(8,128)(2,1)S(1)}, u32[]{:S(2)}, u32[]{:S(2)}) collective-permute-start(bf16[128,512]{1,0:T(8,128)(2,1)} %get-tuple-element.64.refs_1_), channel_id=1, source_target_pairs={{0,4},{4,0},{1,5},{5,1},{2,6},{6,2},{3,7},{7,3},{8,12},{12,8},{9,1... | collective-permute-start | bytes 393224 | tf_op jit(solution)/shard_map/ppermute | solution.py:508
  195.9 6.6 %copy-start.13 = (bf16[128,512]{1,0:T(8,128)(2,1)}, bf16[128,512]{1,0:T(8,128)(2,1)S(1)}, u32[]{:S(2)}) copy-start(bf16[128,512]{1,0:T(8,128)(2,1)S(1)} %collective-permute-done.15.refs_2_) | copy-start | bytes 393220
  195.9 5.0 %collective-permute-start.19 = (bf16[128,512]{1,0:T(8,128)(2,1)S(1)}, bf16[128,512]{1,0:T(8,128)(2,1)S(1)}, u32[]{:S(2)}, u32[]{:S(2)}) collective-permute-start(bf16[128,512]{1,0:T(8,128)(2,1)S(1)} %collective-permute-done.15.refs_2_), channel_id=1, source_target_pairs={{0,4},{4,0},{1,5},{5,1},{2,6},{6,2},{3,7},{7,3},{8,12},{12,8},{9,1... | collective-permute-start | bytes 393224 | tf_op jit(solution)/shard_map/ppermute | solution.py:508
  197.4 5.0 %copy-start.14 = (bf16[128,512]{1,0:T(8,128)(2,1)}, bf16[128,512]{1,0:T(8,128)(2,1)S(1)}, u32[]{:S(2)}) copy-start(bf16[128,512]{1,0:T(8,128)(2,1)S(1)} %collective-permute-done.16.refs_3_) | copy-start | bytes 393220
  197.4 3.4 %collective-permute-start.20 = (bf16[128,512]{1,0:T(8,128)(2,1)S(1)}, bf16[128,512]{1,0:T(8,128)(2,1)S(1)}, u32[]{:S(2)}, u32[]{:S(2)}) collective-permute-start(bf16[128,512]{1,0:T(8,128)(2,1)S(1)} %collective-permute-done.16.refs_3_), channel_id=1, source_target_pairs={{0,4},{4,0},{1,5},{5,1},{2,6},{6,2},{3,7},{7,3},{8,12},{12,8},{9,1... | collective-permute-start | bytes 393224 | tf_op jit(solution)/shard_map/ppermute | solution.py:508
  200.0 2.4 %copy-start.15 = (bf16[128,512]{1,0:T(8,128)(2,1)}, bf16[128,512]{1,0:T(8,128)(2,1)S(1)}, u32[]{:S(2)}) copy-start(bf16[128,512]{1,0:T(8,128)(2,1)S(1)} %collective-permute-done.17.refs_4_) | copy-start | bytes 393220
  200.0 1.8 collective-permute-start.21
  200.8 1.6 copy-start.16
  200.8 1.0 copy-start.17
  226.6 13.4 %all-to-all-start.6 = ((bf16[8,64,128]{2,1,0:T(8,128)(2,1)}), bf16[8,64,128]{2,1,0:T(8,128)(2,1)S(1)}, u32[]{:S(2)}, u32[]{:S(2)}) async-start(bf16[8,64,128]{2,1,0:T(8,128)(2,1)} %get-tuple-element.71), calls=%async_computation.6 | async-start | bytes 262144 | tf_op jit(solution)/shard_map/all_to_all | solution.py:423
  231.6 6.4 %copy-start.5 = (bf16[128,2,256]{2,0,1:T(8,128)(2,1)S(1)}, bf16[128,2,256]{2,0,1:T(8,128)(2,1)}, u32[]{:S(2)}) copy-start(bf16[128,2,256]{2,0,1:T(8,128)(2,1)} %copy.28) | copy-start | bytes 393220
  231.6 6.4 %copy-start.9 = (f32[128,512]{1,0:T(8,128)S(1)}, f32[128,512]{1,0:T(8,128)}, u32[]{:S(2)}) copy-start(f32[128,512]{1,0:T(8,128)} %get-tuple-element.69.refs_0_) | copy-start | bytes 786436
  (2 other events, 1.6 us)
